TPU v7x, 256 devices: a 4x2x16 block of a 4x16x16 slice. The times are simulated.
256 devices in a mesh: grp: 2 (over y), sp: 16 (over z), tp: 8 (over x, core).
Axes of the slice: x: 4, y: 2, z: 16, core: 2. Of those that a mesh axis runs over, the one named last changes fastest.
The devices are a block of a 4x16x16 slice.
Arguments:
- tokens: bfloat16 [65536, 2048], P(('grp', 'sp')), parts along dimension 0, may hold values from -6 to 6
- in_gain: float32 [2048], replicated, may hold values from 0.1 to 1.9
- w_input: bfloat16 [2048, 2048], P(None, 'tp'), may hold values from -0.125 to 0.125
- w_gate: bfloat16 [2048, 2048], P(None, 'tp'), may hold values from -4 to 4
- conv_taps: float32 [4, 2048], P(None, 'tp'), may hold values from -3 to 3
- w_rate: bfloat16 [8, 256, 256], P('tp'), may hold values from -0.375 to 0.375
- w_inlet: bfloat16 [8, 256, 256], P('tp'), may hold values from -0.375 to 0.375
- decay_param: float32 [2048], P('tp'), may hold values from 3 to 25
- decay_bias: float32 [8, 65536], P('tp', ('grp', 'sp')), parts along dimension 1, may hold values from -1.5 to 0
- out_gain: float32 [2048], P('tp'), may hold values from 0.1 to 1.9
- w_out: bfloat16 [2048, 2048], P('sp'), may hold values from -0.125 to 0.125
Outputs:
- mixer_out: bfloat16 [65536, 2048], P(('grp', 'sp', 'tp')), parts along dimension 0
There are 2 independent parts, one for each index of `grp`. A program takes and returns all parts, laid end to end along the dimension named above; an argument that names none is the same for every part. Nothing has to cross between parts.
All inputs are finite; a program needn't handle non-finite values.
Results may differ from a plain program's by a relative error of at most 0.013.
Values may be sent and summed in bfloat16 or wider, within the bound.
No kernel may reach another device: no remote copies, remote signals or barrier semaphores. Data moves between devices by JAX's collectives and lax.ppermute only.
A program may use at most 128 MiB of HBM per device.

v0:
```python
import jax
import jax.numpy as jnp
from jax import lax
from jax.sharding import PartitionSpec as P


def from_behind(array, axis, by):
    peers = lax.axis_size(axis)
    pairs = [(i, i + by) for i in range(peers) if 0 <= i + by < peers]
    return lax.ppermute(array, axis, pairs)


def sent_to_all(array, axis):
    copies = jnp.broadcast_to(array, (lax.axis_size(axis), *array.shape))
    return lax.all_to_all(copies, axis, split_axis=0, concat_axis=0, tiled=True)


def collected_together(array, axis):
    leaves = jax.tree.leaves(array)
    sequence = sorted(range(len(leaves)), key=lambda k: -leaves[k].size)
    width = (1, *leaves[sequence[0]].shape)[-1]
    lines = [
        jnp.pad(leaves[k].reshape(-1), (0, -leaves[k].size % width)).reshape(-1, width)
        for k in sequence
    ]
    both, at, found = (sent_to_all(jnp.concatenate(lines), axis), 0, {})
    for k, line in zip(sequence, lines):
        piece = both[:, at : at + len(line)].reshape(len(both), -1)
        found[k] = piece[:, : leaves[k].size].reshape(-1, *leaves[k].shape)
        at += len(line)
    numbers = iter(range(len(leaves)))
    return jax.tree.map(lambda _: found[next(numbers)], array)


def joined_by_halves(pieces, combine):
    while len(jax.tree.leaves(pieces)[0]) > 1:
        pieces = jax.vmap(combine)(
            *(jax.tree.map(lambda part: part[side::2], pieces) for side in (0, 1))
        )
    return jax.tree.map(lambda part: part[0], pieces)


def entering(array, axis, combine, identity):
    peers, position = (lax.axis_size(axis), lax.axis_index(axis))
    passed = jnp.arange(peers) < position

    def kept(part, zero, own):
        part = jnp.where(
            passed.reshape(-1, *(1 for _ in own.shape)), part, jnp.asarray(zero, own.dtype)
        )
        return part

    pieces = collected_together(array, axis)
    return joined_by_halves(jax.tree.map(kept, pieces, identity, array), combine)


def of_everyone(array, axis):
    everything = sent_to_all(array, axis)
    return jnp.sum(everything, axis=0)


def combine_pairs(first_pair, second_pair):
    return (first_pair[0] * second_pair[0], second_pair[0] * first_pair[1] + second_pair[1])


def blocked_scan(decay_factor, drive_term):
    row_count, width = decay_factor.shape
    block_count = row_count // 8
    decay_blocks = decay_factor.reshape(block_count, 8, width)
    drive_blocks = drive_term.reshape(block_count, 8, width)
    running_prod = decay_blocks[:, 0]
    running_state = drive_blocks[:, 0]
    prod_list = [running_prod]
    state_list = [running_state]
    for inner in range(1, 8):
        factor = decay_blocks[:, inner]
        running_prod = factor * running_prod
        running_state = factor * running_state + drive_blocks[:, inner]
        prod_list.append(running_prod)
        state_list.append(running_state)
    prod_inner = jnp.stack(prod_list, axis=1)
    state_inner = jnp.stack(state_list, axis=1)
    total_prod = running_prod
    total_state = running_state
    stride = 1
    while stride < block_count:
        earlier_prod = jnp.concatenate(
            [jnp.ones((stride, width), jnp.float32), total_prod[: block_count - stride]], axis=0
        )
        earlier_state = jnp.concatenate(
            [jnp.zeros((stride, width), jnp.float32), total_state[: block_count - stride]], axis=0
        )
        total_prod, total_state = combine_pairs(
            (earlier_prod, earlier_state), (total_prod, total_state)
        )
        stride = stride * 2
    before_prod = jnp.concatenate(
        [jnp.ones((1, width), jnp.float32), total_prod[: block_count - 1]], axis=0
    )
    before_state = jnp.concatenate(
        [jnp.zeros((1, width), jnp.float32), total_state[: block_count - 1]], axis=0
    )
    full_prod = prod_inner * before_prod[:, None, :]
    full_local = state_inner + prod_inner * before_state[:, None, :]
    return (full_prod.reshape(row_count, width), full_local.reshape(row_count, width))


def body(
    tokens,
    in_gain,
    w_input,
    w_gate,
    conv_taps,
    w_rate,
    w_inlet,
    decay_param,
    decay_bias,
    out_gain,
    w_out,
):
    row_count = tokens.shape[0]
    channels = w_input.shape[1]
    heads_here = w_rate.shape[0]
    head_size = w_rate.shape[1]
    conv_reach = conv_taps.shape[0] - 1
    as_float = tokens.astype(jnp.float32)
    inv_norm = lax.rsqrt(jnp.mean(as_float * as_float, axis=1, keepdims=True) + 1e-06)
    normed = (as_float * inv_norm * in_gain).astype(jnp.bfloat16)
    projected = jnp.dot(normed, w_input, preferred_element_type=jnp.float32).astype(jnp.bfloat16)
    gate_raw = jnp.dot(normed, w_gate, preferred_element_type=jnp.float32).astype(jnp.bfloat16)
    prior_rows = from_behind(projected[row_count - conv_reach :], "sp", 1)
    padded = jnp.concatenate([prior_rows, projected], axis=0).astype(jnp.float32)
    summed = padded[0:row_count] * conv_taps[0]
    for offset in range(1, conv_reach + 1):
        summed = summed + padded[offset : offset + row_count] * conv_taps[offset]
    convolved = summed.astype(jnp.bfloat16)
    per_head = convolved.reshape(row_count, heads_here, head_size)
    rate_gate = jax.nn.sigmoid(
        jnp.einsum("shi,hij->shj", per_head, w_rate, preferred_element_type=jnp.float32)
    ).reshape(row_count, channels)
    input_gate = jax.nn.sigmoid(
        jnp.einsum("shi,hij->shj", per_head, w_inlet, preferred_element_type=jnp.float32)
    ).reshape(row_count, channels)
    head_bias = jnp.repeat(jnp.transpose(decay_bias), head_size, axis=1)
    log_decay = -8.0 * rate_gate * jax.nn.softplus(-decay_param) + head_bias
    decay_factor = jnp.exp(log_decay)
    drive_term = jnp.sqrt(-jnp.expm1(2.0 * log_decay)) * input_gate * convolved.astype(jnp.float32)
    unit_full = (jnp.ones((channels,), jnp.float32), jnp.zeros((channels,), jnp.float32))
    decay_prod, local_state = blocked_scan(decay_factor, drive_term)
    incoming_state = entering((decay_prod[-1], local_state[-1]), "sp", combine_pairs, unit_full)[1]
    full_state = local_state + decay_prod * incoming_state
    gated_out = full_state * jax.nn.gelu(gate_raw.astype(jnp.float32))
    square_total = of_everyone(jnp.sum(gated_out * gated_out, axis=1), "tp")
    out_scale = lax.rsqrt(square_total / (channels * lax.axis_size("tp")) + 1e-06)
    normed_out = (gated_out * out_scale[:, None] * out_gain).astype(jnp.bfloat16)
    token_matrix = lax.all_to_all(normed_out, "tp", split_axis=0, concat_axis=1, tiled=True)
    projected_out = jnp.dot(
        token_matrix,
        lax.all_gather(w_out, "sp", axis=0, tiled=True),
        preferred_element_type=jnp.float32,
    )
    return projected_out.astype(jnp.bfloat16)


def solution(mesh):
    return jax.shard_map(
        body,
        mesh=mesh,
        in_specs=(
            P(("grp", "sp"), None),
            P(),
            P(None, "tp"),
            P(None, "tp"),
            P(None, "tp"),
            P("tp", None, None),
            P("tp", None, None),
            P("tp"),
            P("tp", ("grp", "sp")),
            P("tp"),
            P("sp", None),
        ),
        out_specs=P(("grp", "sp", "tp"), None),
        check_vma=False,
    )
```

profile of v0, /device:TPU:33, one launch (start us, length us, event | category | flops | bytes accessed | tf_op | source)
XLA Modules:
  0.0 142.6 jit_solution(2775839110201704660)
XLA Ops:
  6.6 0.7 all-gather.2.cloned.1.call-update
  7.3 5.2 %fusion = f32[2048]{0:T(1024)S(1)} fusion(bf16[2048,2048]{1,0:T(8,128)(2,1)} %param.11), kind=kLoop, calls=%fused_computation.2 | loop fusion | flops 12580864 | bytes 8396800 | tf_op jit(solution)/shard_map/reduce_sum | solution.py:127
  12.6 0.5 copy-done.2
  13.1 4.0 %convolution_convert_fusion.2 = bf16[2048,256]{1,0:T(8,128)(2,1)S(1)} fusion(bf16[2048,256]{1,0:T(8,128)(2,1)} %param.13, bf16[2048,2048]{1,0:T(8,128)(2,1)S(1)} %copy-done.2, f32[2048]{0:T(1024)S(1)} %copy-done.9, f32[2048]{0:T(1024)S(1)} %add_rsqrt_fusion.1), kind=kOutput, calls=%fused_computation.21 | convolution fusion | flops 2164785152 | bytes 10502144 | tf_op jit(solution)/shard_map/dot_general | solution.py:129
  17.1 5.4 %collective-permute-start = (bf16[3,256]{1,0:T(4,128)(2,1)S(1)}, bf16[3,256]{1,0:T(4,128)(2,1)S(1)}, u32[]{:S(2)}, u32[]{:S(2)}) collective-permute-start(bf16[3,256]{1,0:T(4,128)(2,1)S(1)} %slice.253), channel_id=1, source_target_pairs={{0,8},{8,16},{16,24},{24,32},{32,40},{40,48},{48,56},{56,64},{64,7... | collective-permute-start | bytes 4616 | tf_op jit(solution)/shard_map/ppermute | solution.py:10
  22.6 0.5 broadcast.117
  23.1 0.7 reduce.4
  24.2 0.9 fusion.20
  25.1 0.7 fusion.8
  25.9 0.8 fusion.24
  26.7 2.0 %fusion.27 = f32[256,8,256]{2,1,0:T(8,128)S(1)} fusion(bf16[2048,256]{1,0:T(8,128)(2,1)S(1)} %fusion.20, f32[2048,256]{1,0:T(8,128)S(1)} %fusion.8, f32[2048]{0:T(1024)S(1)} %bitcast.74, f32[256]{0:T(256)S(1)} %fusion.34, bf16[1,256,256]{2,1,0:T(8,128)(2,1)S(1)} %copy-done.8), kind=kOutput, calls=%fused_computation.44 | convolution fusion | flops 273678336 | bytes 5383168 | tf_op jit(solution)/shard_map/shi,hij->shj/dot_general | solution.py:142
  28.7 1.2 fusion.35
  32.7 1.2 copy.142
  34.1 1.2 copy.143
  35.4 0.6 broadcast_in_dim.19
  36.0 22.4 %all-to-all-start = ((f32[16,2,256]{2,1,0:T(2,128)}), f32[16,2,256]{2,1,0:T(2,128)S(1)}, u32[]{:S(2)}, u32[]{:S(2)}) async-start(f32[16,2,256]{2,1,0:T(2,128)} %broadcast_in_dim.19), calls=%async_computation | async-start | bytes 65536 | tf_op jit(solution)/shard_map/all_to_all | solution.py:15
  58.4 11.8 %all-to-all-done = f32[16,2,256]{2,1,0:T(2,128)S(1)} async-done(((f32[16,2,256]{2,1,0:T(2,128)}), f32[16,2,256]{2,1,0:T(2,128)S(1)}, u32[]{:S(2)}, u32[]{:S(2)}) %all-to-all-start) | async-done | bytes 32800 | tf_op jit(solution)/shard_map/all_to_all | solution.py:15
  70.6 10.5 %multiply_reduce_fusion = (f32[2048]{0:T(1024)S(1)}, f32[2048,256]{1,0:T(8,128)}) fusion(bf16[2048,256]{1,0:T(8,128)(2,1)S(1)} %copy-done, bf16[2048,2048]{1,0:T(8,128)(2,1)} %param.11, f32[2048]{0:T(1024)S(1)} %copy-done.9, f32[2048]{0:T(1024)S(1)} %add_rsqrt_fusion.1, f32[256]{0:T(256)S(1)} %bitcast.79, f32[256,8,256]{2,0,1:T(8,128)S(1)} %get-tuple-element.25, ...), kind=kOutput, calls=%fused_computation.42 | convolution fusion | flops 2172123136 | bytes 15754240 | tf_op jit(solution)/shard_map/dot_general | solution.py:130
  81.1 12.3 %all_to_all.30 = f32[8,1,2048]{2,1,0:T(1,128)S(1)} all-to-all(f32[8,1,2048]{2,1,0:T(1,128)S(1)} %broadcast_in_dim.22), channel_id=1, replica_groups=mesh['grp'=2,'sp'=16,'tp'=8] {'tp'}, dimensions={0} | all-to-all | bytes 131072 | tf_op jit(solution)/shard_map/all_to_all | solution.py:15
  93.4 2.0 %multiply_convert_fusion = bf16[2048,256]{1,0:T(8,128)(2,1)S(1)} fusion(f32[2048,256]{1,0:T(8,128)} %get-tuple-element.55, f32[256]{0:T(256)S(1)} %copy-done.5, f32[2048]{0:T(1024)S(1)} %add_rsqrt_fusion), kind=kLoop, calls=%fused_computation.41 | loop fusion | flops 1572864 | bytes 3154944 | tf_op jit(solution)/shard_map/convert_element_type | solution.py:155
  95.4 0.5 copy.84
  96.0 18.2 %all_to_all.31 = bf16[8,256,256]{1,2,0:T(8,128)(2,1)S(1)} all-to-all(bf16[8,256,256]{1,2,0:T(8,128)(2,1)S(1)} %copy.84), channel_id=1, replica_groups=mesh['grp'=2,'sp'=16,'tp'=8] {'tp'}, dimensions={0} | all-to-all | bytes 2097152 | tf_op jit(solution)/shard_map/all_to_all | solution.py:156
  114.1 14.9 %all-gather.2.cloned.1.call-done = bf16[2048,2048]{1,0:T(8,128)(2,1)} async-done(((bf16[128,2048]{1,0:T(8,128)(2,1)}), bf16[2048,2048]{1,0:T(8,128)(2,1)}) %all-gather.2.cloned.1.call-update) | async-done | bytes 8388624 | tf_op jit(solution)/shard_map/all_gather | solution.py:159
  129.0 6.7 %convolution_convert_fusion = bf16[256,2048]{1,0:T(8,128)(2,1)} fusion(bf16[256,2048]{0,1:T(8,128)(2,1)S(1)} %bitcast.64, bf16[2048,2048]{1,0:T(8,128)(2,1)} %all-gather.2.cloned.1.call-done), kind=kOutput, calls=%fused_computation.19 | convolution fusion | flops 2148007936 | bytes 10485760 | tf_op jit(solution)/shard_map/dot_general | solution.py:157
  (91 shorter events, 3.7 us)
Async XLA Ops:
  6.5 64.0 %copy-start = (bf16[2048,256]{1,0:T(8,128)(2,1)S(1)}, bf16[2048,256]{1,0:T(8,128)(2,1)}, u32[]{:S(2)}) copy-start(bf16[2048,256]{1,0:T(8,128)(2,1)} %param.14) | copy-start | bytes 3145732
  6.6 122.5 %all-gather.2.cloned.1.call-start = ((), (), s32[]{:S(2)}) async-start(), calls=%async_computation.3 | async-start | bytes 8912896 | tf_op jit(solution)/shard_map/all_gather | solution.py:159
  7.3 5.8 %copy-start.2 = (bf16[2048,2048]{1,0:T(8,128)(2,1)S(1)}, bf16[2048,2048]{1,0:T(8,128)(2,1)}, u32[]{:S(2)}) copy-start(bf16[2048,2048]{1,0:T(8,128)(2,1)} %param.11) | copy-start | bytes 25165828
  7.3 5.8 %copy-start.9 = (f32[2048]{0:T(1024)S(1)}, f32[2048]{0:T(1024)}, u32[]{:S(2)}) copy-start(f32[2048]{0:T(1024)} %param.12) | copy-start | bytes 24580
  13.1 9.4 %copy-start.4 = (f32[4,256]{1,0:T(4,128)S(1)}, f32[4,256]{1,0:T(4,128)}, u32[]{:S(2)}) copy-start(f32[4,256]{1,0:T(4,128)} %param.15) | copy-start | bytes 12292
  13.1 9.5 %copy-start.6 = (f32[256]{0:T(256)S(1)}, f32[256]{0:T(256)}, u32[]{:S(2)}) copy-start(f32[256]{0:T(256)} %param.18) | copy-start | bytes 3076
  13.1 10.0 %copy-start.3 = (f32[1,2048]{1,0:T(1,128)S(1)}, f32[1,2048]{1,0:T(1,128)}, u32[]{:S(2)}) copy-start(f32[1,2048]{1,0:T(1,128)} %param.19) | copy-start | bytes 24580
  17.1 6.8 %collective-permute-start = (bf16[3,256]{1,0:T(4,128)(2,1)S(1)}, bf16[3,256]{1,0:T(4,128)(2,1)S(1)}, u32[]{:S(2)}, u32[]{:S(2)}) collective-permute-start(bf16[3,256]{1,0:T(4,128)(2,1)S(1)} %slice.253), channel_id=1, source_target_pairs={{0,8},{8,16},{16,24},{24,32},{32,40},{40,48},{48,56},{56,64},{64,7... | collective-permute-start | bytes 4616 | tf_op jit(solution)/shard_map/ppermute | solution.py:10
  24.2 0.9 copy-start.7
  25.8 0.9 copy-start.8
  32.7 1.4 copy-start.1
  36.0 34.2 %all-to-all-start = ((f32[16,2,256]{2,1,0:T(2,128)}), f32[16,2,256]{2,1,0:T(2,128)S(1)}, u32[]{:S(2)}, u32[]{:S(2)}) async-start(f32[16,2,256]{2,1,0:T(2,128)} %broadcast_in_dim.19), calls=%async_computation | async-start | bytes 65536 | tf_op jit(solution)/shard_map/all_to_all | solution.py:15
  70.6 22.8 %copy-start.5 = (f32[256]{0:T(256)S(1)}, f32[256]{0:T(256)}, u32[]{:S(2)}) copy-start(f32[256]{0:T(256)} %param.20) | copy-start | bytes 3076
Sparse Core Ops, SparseCore 0:
  9.1 119.8 all-gather.1
where the time goes:
time: 143 us
  blocking collectives  30.4 us (21%)
  starting transfers between devices  27.8 us (19%)
  waiting for transfers between devices  27.4 us (19%)
  matrix products  23.8 us (17%)
  between operations  14 us (10%)
  other arithmetic  12 us (8%)
  local copies, waits for them, and re-layouts  7.12 us (5%)
    all_to_all x1, starting transfers between devices, sent_to_all(): return lax.all_to_all(copies, axis, split_axis=0, concat_axis=0, tiled=True)  22.4 us
    all_to_all x1, blocking collectives, body(): lax.all_to_all(normed_out, 'tp', split_axis=0, concat_axis=1, tiled=True)  18.2 us
    all_gather x1, waiting for transfers between devices, body(): lax.all_gather(w_out, 'sp', axis=0, tiled=True)  14.9 us
    all_to_all x1, blocking collectives, sent_to_all(): return lax.all_to_all(copies, axis, split_axis=0, concat_axis=0, tiled=True)  12.3 us
    all_to_all x1, waiting for transfers between devices, sent_to_all(): return lax.all_to_all(copies, axis, split_axis=0, concat_axis=0, tiled=True)  11.8 us
    dot_general x1, matrix products, body(): jnp.dot(normed, w_gate, preferred_element_type=jnp.float32)  10.5 us
    dot_general x1, matrix products, body(): jnp.dot(token_matrix, lax.all_gather(w_out, 'sp', axis=0, tiled=True), pr...  6.7 us
    ppermute x1, starting transfers between devices, from_behind(): return lax.ppermute(array, axis, pairs)  5.42 us
  transfers between devices with their start and end apart: 3, of which 2 were waited for; matrix products, arithmetic and copies ran while one was open for 25% of the time, Pallas kernels for 0%

commit v1 on v0

v1 whole, which is shorter than its diff:
```python
import functools

import jax
import jax.numpy as jnp
from jax import lax
from jax.experimental import pallas as pl
from jax.experimental.pallas import tpu as pltpu
from jax.sharding import PartitionSpec as P

F32 = jnp.float32
BF16 = jnp.bfloat16
BLOCK = 256
SEG = 8
EXTRA = 16
EPS = 1e-06


def normed_rows(rows, gain):
    wide = rows.astype(F32)
    inv = lax.rsqrt(jnp.mean(wide * wide, axis=1, keepdims=True) + EPS)
    return (wide * inv * gain).astype(BF16)


def minus_expm1(y, exp_y):
    series = 1.0 / 120.0 + y * (1.0 / 720.0)
    series = 1.0 / 24.0 + y * series
    series = 1.0 / 6.0 + y * series
    series = 0.5 + y * series
    series = -y * (1.0 + y * series)
    return jnp.where(y > -0.25, series, 1.0 - exp_y)


def gelu(x):
    inner = 0.7978845608028654 * (x + 0.044715 * (x * x * x))
    return 0.5 * x * (1.0 + jnp.tanh(inner))


def logistic(x):
    return 1.0 / (1.0 + jnp.exp(-x))


def shifted_down(x, by, fill):
    rows = lax.broadcasted_iota(jnp.int32, x.shape, 0)
    return jnp.where(rows < by, fill, pltpu.roll(x, by, 0))


def input_kernel(tokens, gain, w_input, projected):
    normed = normed_rows(tokens[...], gain[...])
    projected[...] = jnp.dot(normed, w_input[...], preferred_element_type=F32).astype(BF16)


def gate_kernel(tokens, gain, w_gate, gate):
    normed = normed_rows(tokens[...], gain[...])
    gate_raw = jnp.dot(normed, w_gate[...], preferred_element_type=F32).astype(BF16)
    gate[...] = gelu(gate_raw.astype(F32))


def thirds(x):
    top = x.astype(BF16)
    rest = x - top.astype(F32)
    middle = rest.astype(BF16)
    return [top, middle, (rest - middle.astype(F32)).astype(BF16)]


def recur_kernel(projected, taps, w_rate, w_inlet, soft, bias, *refs, first):
    early, refs = refs[:3] if first else refs[:4], refs[3:] if first else refs[4:]
    state, prod, ends, conv_buf, decay_buf, drive_buf, carry = refs
    step = pl.program_id(0)

    @pl.when(step == 0)
    def _():
        if first:
            halo, gain, w_input = early
            edge = jnp.dot(normed_rows(halo[...], gain[...]), w_input[...], preferred_element_type=F32)
            conv_buf[0:8, :] = edge.astype(BF16).astype(F32)[8:16]
            head_row = lax.broadcasted_iota(jnp.int32, carry.shape, 0) == 0
            carry[...] = jnp.where(head_row, 1.0, 0.0)
        else:
            before, begun = early[0], early[1]
            conv_buf[0:8, :] = before[...].astype(F32)[8:16]
            carry[...] = begun[0]

    @pl.when(step > 0)
    def _():
        conv_buf[0:8, :] = conv_buf[BLOCK : BLOCK + 8, :]

    conv_buf[8 : BLOCK + 8, :] = projected[...].astype(F32)
    summed = conv_buf[5 : BLOCK + 5, :] * taps[0:1, :]
    for k in range(1, 4):
        summed = summed + conv_buf[5 + k : BLOCK + 5 + k, :] * taps[k : k + 1, :]
    convolved = summed.astype(BF16)
    rate = logistic(jnp.dot(convolved, w_rate[0], preferred_element_type=F32))
    inlet = logistic(jnp.dot(convolved, w_inlet[0], preferred_element_type=F32))
    row_bias = bias[...]
    pieces = thirds(row_bias) + [jnp.zeros((13, BLOCK), BF16)]
    bias_col = lax.dot_general(
        jnp.concatenate(pieces, 0), jnp.ones((16, rate.shape[1]), BF16), (((0,), (0,)), ((), ())),
        preferred_element_type=F32,
    )
    log_decay = -8.0 * rate * soft[...] + bias_col
    decay = jnp.exp(log_decay)
    drive = jnp.sqrt(minus_expm1(2.0 * log_decay, decay * decay)) * inlet * convolved.astype(F32)
    segs = BLOCK // SEG
    for half in range(2):
        lanes = slice(half * 128, half * 128 + 128)
        decay_buf[half] = decay[:, lanes]
        drive_buf[half] = drive[:, lanes]
        row = [(half, pl.ds(r, segs, stride=SEG), slice(None)) for r in range(SEG)]
        p, h = decay_buf[row[0]], drive_buf[row[0]]
        inner = [(p, h)]
        for r in range(1, SEG):
            a = decay_buf[row[r]]
            h = a * h + drive_buf[row[r]]
            p = a * p
            inner.append((p, h))
        by = 1
        while by < segs:
            h = h + p * shifted_down(h, by, 0.0)
            p = p * shifted_down(p, by, 1.0)
            by *= 2
        before_p = shifted_down(p, 1, 1.0)
        before_h = shifted_down(h, 1, 0.0)
        start_h = before_h + before_p * carry[1:2, lanes]
        start_p = before_p * carry[0:1, lanes]
        for r in range(SEG):
            p, h = inner[r]
            state[row[r]] = h + p * start_h
            prod[row[r]] = p * start_p
        carry[0:1, lanes] = prod[half, BLOCK - 1 : BLOCK, :]
        carry[1:2, lanes] = state[half, BLOCK - 1 : BLOCK, :]
    ends[...] = jnp.broadcast_to(carry[...][None], ends.shape)


def gated_kernel(state, prod, gate, ends, gain, sent, incoming):
    @pl.when(pl.program_id(0) == 0)
    def _():
        span = lax.axis_index("sp")
        total = jnp.zeros((1, gain.shape[1]), F32)
        for k in range(ends.shape[0]):
            total = jnp.where(k < span, ends[k, 0:1, :] * total + ends[k, 1:2, :], total)
        incoming[...] = jnp.broadcast_to(total, incoming.shape)

    ones = jnp.ones((8, 128), BF16)
    over = (((1,), (1,)), ((), ()))
    for d in range(sent.shape[0]):
        rows = slice(d * BLOCK, d * BLOCK + BLOCK)
        total = jnp.zeros((8, BLOCK), F32)
        for half in range(2):
            lanes = slice(half * 128, half * 128 + 128)
            gated = (state[half, rows, :] + prod[half, rows, :] * incoming[0:1, lanes]) * gate[rows, lanes]
            sent[d, half, 0:BLOCK, :] = (gated * gain[:, lanes]).astype(BF16)
            square = gated * gated
            high = square.astype(BF16)
            low = (square - high.astype(F32)).astype(BF16)
            total = total + lax.dot_general(ones, high, over, preferred_element_type=F32)
            total = total + lax.dot_general(ones, low, over, preferred_element_type=F32)
        top = total.astype(BF16).astype(F32)
        row = lax.broadcasted_iota(jnp.int32, total.shape, 0)
        lines = jnp.where(row == 0, top, jnp.where(row == 1, total - top, 0.0))
        lines = jnp.concatenate([lines, jnp.zeros_like(lines)], 0).astype(BF16)
        for half in range(2):
            sent[d, half, BLOCK : BLOCK + EXTRA, :] = lines[:, half * 128 : half * 128 + 128]


def product(arrived, places, blocks, low, step):
    mixed = jnp.concatenate([arrived[place, 0:BLOCK, :] for place in places], 1)
    weights = jnp.concatenate([block[:, low : low + step] for block in blocks], 0)
    return jnp.dot(mixed, weights, preferred_element_type=F32)


def places_of(offsets, spans):
    span, core = lax.axis_index("sp"), lax.axis_index("tp") % 2
    return [lax.rem(span + spans + jnp.where(core == 0, k, -k), spans) for k in offsets]


def early_kernel(arrived, *refs, offsets, spans):
    blocks, out = refs[:-1], refs[-1]
    places = places_of(offsets, spans)
    step = 512
    for low in range(0, out.shape[1], step):
        out[:, low : low + step] = product(arrived, places, blocks, low, step)


def late_kernel(arrived, sums, *refs, offsets, spans, channels):
    blocks, out = refs[:-1], refs[-1]
    places = places_of(offsets, spans)
    ones = jnp.ones((arrived.shape[0] // 2 * EXTRA, 128), BF16)
    square = []
    for half in range(2):
        lines = [arrived[k, BLOCK : BLOCK + EXTRA, :] for k in range(half, arrived.shape[0], 2)]
        square.append(
            lax.dot_general(
                jnp.concatenate(lines, 0), ones, (((0,), (0,)), ((), ())), preferred_element_type=F32
            )
        )
    scale = lax.rsqrt(jnp.concatenate(square, 0)[:, 0:1] / channels + EPS)
    step = 512
    for low in range(0, out.shape[1], step):
        acc = sums[:, low : low + step] + product(arrived, places, blocks, low, step)
        out[:, low : low + step] = (acc * scale).astype(BF16)


def tie(*values):
    return lax.optimization_barrier(values)


def body(
    tokens, in_gain, w_input, w_gate, conv_taps, w_rate, w_inlet, decay_param, decay_bias, out_gain, w_out
):
    rows, width = tokens.shape
    head = w_input.shape[1]
    spans, heads = lax.axis_size("sp"), lax.axis_size("tp")
    _, out_width = w_out.shape
    reach = spans // 2

    around = []
    swap = []
    for z in range(spans):
        for t in range(heads):
            ahead = (z + 1) % spans if t % 2 == 0 else (z - 1) % spans
            around.append((z * heads + t, ahead * heads + t))
            swap.append((z * heads + t, z * heads + t + 1 - 2 * (t % 2)))

    moved, swapped = [], []

    def onward(x):
        moved.append(lax.ppermute(x, ("sp", "tp"), around))

    def across(x):
        swapped.append(lax.ppermute(x, ("sp", "tp"), swap))

    def advance(value):
        if swapped:
            value, moved[-1], swapped[-1] = tie(value, moved[-1], swapped[-1])
        else:
            value, moved[-1] = tie(value, moved[-1])
        if len(moved) < reach:
            across(moved[-1])
            onward(moved[-1])
        return value

    fixed = lambda *shape: pl.BlockSpec(shape, lambda i: (0,) * len(shape))
    halves = lambda n, at: pl.BlockSpec((2, n, head // 2), lambda i: (0, i + at, 0))
    moving = lambda n, cols, at=0: pl.BlockSpec((n, cols), lambda i: (i + at, 0))
    hbm = pl.BlockSpec(memory_space=pl.ANY)
    vmem = pl.BlockSpec(memory_space=pltpu.VMEM)

    onward(w_out)
    halo = lax.ppermute(tokens[rows - 16 :], "sp", [(i, i + 1) for i in range(spans - 1)])
    soft = jax.nn.softplus(-decay_param).reshape(1, head)
    gain_row = in_gain.reshape(1, width)

    big = 2 * BLOCK
    projected = pl.pallas_call(
        input_kernel,
        grid=(rows // big,),
        in_specs=[moving(big, width), fixed(1, width), fixed(width, head)],
        out_specs=moving(big, head),
        out_shape=jax.ShapeDtypeStruct((rows, head), BF16),
        name="input",
    )(tokens, gain_row, w_input)

    half_rows = rows // 2
    steps = half_rows // BLOCK
    state_shape = jax.ShapeDtypeStruct((2, rows, head // 2), F32)

    def recur(first, *extra):
        at = 0 if first else steps
        specs = [
            moving(BLOCK, head, at), fixed(4, head), fixed(1, head, head), fixed(1, head, head), fixed(1, head),
            pl.BlockSpec((1, BLOCK), lambda i: (0, i + at)),
        ]
        if first:
            specs += [fixed(16, width), fixed(1, width), fixed(width, head)]
        else:
            specs += [
                pl.BlockSpec((16, head), lambda i: (half_rows // 16 - 1, 0)),
                pl.BlockSpec((1, 8, head), lambda i: (0, 0, 0)), hbm, hbm,
            ]
        many = 1 if first else spans
        return pl.pallas_call(
            functools.partial(recur_kernel, first=first),
            grid=(steps,),
            in_specs=specs,
            out_specs=[halves(BLOCK, at), halves(BLOCK, at), fixed(many, 8, head)],
            out_shape=[state_shape, state_shape, jax.ShapeDtypeStruct((many, 8, head), F32)],
            scratch_shapes=[
                pltpu.VMEM((BLOCK + 8, head), F32), pltpu.VMEM((2, BLOCK, head // 2), F32),
                pltpu.VMEM((2, BLOCK, head // 2), F32), pltpu.VMEM((8, head), F32),
            ],
            input_output_aliases={} if first else {8: 0, 9: 1},
            name="recur",
        )(projected, conv_taps, w_rate, w_inlet, soft, decay_bias, *extra)

    state, prod, begun = recur(True, halo, gain_row, w_input)
    begun = advance(begun)
    state, prod, ends = recur(False, projected, begun, state, prod)
    all_ends = lax.all_to_all(ends, "sp", split_axis=0, concat_axis=0, tiled=True)
    gate_tokens = advance(tokens)
    gate_tokens, _ = tie(gate_tokens, ends)
    gate = pl.pallas_call(
        gate_kernel,
        grid=(rows // big,),
        in_specs=[moving(big, width), fixed(1, width), fixed(width, head)],
        out_specs=moving(big, head),
        out_shape=jax.ShapeDtypeStruct((rows, head), F32),
        name="gate",
    )(gate_tokens, gain_row, w_gate)
    gate = advance(gate)

    sent = pl.pallas_call(
        gated_kernel,
        grid=(heads // 2,),
        in_specs=[halves(big, 0), halves(big, 0), moving(big, head), fixed(spans, 8, head), fixed(1, head)],
        out_specs=pl.BlockSpec((2, 2, BLOCK + EXTRA, head // 2), lambda i: (i, 0, 0, 0)),
        out_shape=jax.ShapeDtypeStruct((heads, 2, BLOCK + EXTRA, head // 2), BF16),
        scratch_shapes=[pltpu.VMEM((8, head), F32)],
        name="gated",
    )(state, prod, gate, all_ends, out_gain.reshape(1, head))
    arrived = lax.all_to_all(sent, "tp", split_axis=0, concat_axis=0, tiled=True)
    holding = sent
    while len(moved) < reach - 2:
        holding = advance(holding)
    arrived = arrived.reshape(2 * heads, BLOCK + EXTRA, head // 2)
    arrived = advance(arrived)
    done = len(swapped) - 1
    offsets = [0] + [-k for k in range(1, done + 1)] + list(range(1, done + 1))
    sums = pl.pallas_call(
        functools.partial(early_kernel, offsets=offsets, spans=spans),
        in_specs=[vmem] * (2 + 2 * done),
        out_specs=vmem,
        out_shape=jax.ShapeDtypeStruct((BLOCK, out_width), F32),
        name="early",
    )(arrived, w_out, *moved[:done], *swapped[:done])
    while len(moved) < reach:
        sums = advance(sums)
    offsets = [-k for k in range(done + 1, reach + 1)] + list(range(done + 1, reach))
    return pl.pallas_call(
        functools.partial(late_kernel, offsets=offsets, spans=spans, channels=heads * head),
        in_specs=[vmem] * (2 + len(offsets)),
        out_specs=vmem,
        out_shape=jax.ShapeDtypeStruct((BLOCK, out_width), BF16),
        name="late",
    )(arrived, sums, *moved[done:], *swapped[done:])


def solution(mesh):
    return jax.shard_map(
        body,
        mesh=mesh,
        in_specs=(
            P(("grp", "sp"), None), P(), P(None, "tp"), P(None, "tp"), P(None, "tp"),
            P("tp", None, None), P("tp", None, None), P("tp"), P("tp", ("grp", "sp")), P("tp"), P("sp", None),
        ),
        out_specs=P(("grp", "sp", "tp"), None),
        check_vma=False,
    )
```

time: 143 us -> 144 us (level)
  Pallas kernels: 0 us -> 44.1 us
  matrix products: 23.8 us -> 0 us
  starting transfers between devices: 27.8 us -> 47.6 us
  between operations: 14 us -> 0.16 us
  blocking collectives: 30.4 us -> 16.8 us
  other arithmetic: 12 us -> 1.29 us
  local copies, waits for them, and re-layouts: 7.12 us -> 2.3 us
  waiting for transfers between devices: 27.4 us -> 30.3 us
    pallas_call x0 -> x7, Pallas kernels: none -> 44.1 us  [the longest x2 12.2 us: recur(): pl.pallas_call(functools.partial(recur_kernel, first=first), grid=(steps,...]
    ppermute x1 -> x16, starting transfers between devices: 5.42 us -> 42.8 us  [the longest x8 29.5 us: onward(): moved.append(lax.ppermute(x, ('sp', 'tp'), around))]
    dot_general x5 -> x0, matrix products: 23.8 us -> none  [the longest x1 10.5 us: body(): jnp.dot(normed, w_gate, preferred_element_type=jnp.float32)]
    ppermute x1 -> x16, waiting for transfers between devices: 0.01 us -> 19.1 us  [the longest x8 16.5 us: onward(): moved.append(lax.ppermute(x, ('sp', 'tp'), around))]
    all_to_all x1, starting transfers between devices: 22.4 us -> 4.86 us  [body(): lax.all_to_all(sent, 'tp', split_axis=0, concat_axis=0, tiled=True)]
    all_gather x1 -> x0, waiting for transfers between devices: 14.9 us -> none  [body(): lax.all_gather(w_out, 'sp', axis=0, tiled=True)]
    all_to_all x2 -> x1, blocking collectives: 30.4 us -> 16.8 us  [body(): lax.all_to_all(ends, 'sp', split_axis=0, concat_axis=0, tiled=True)]
    reduce_sum x2 -> x0, other arithmetic: 5.29 us -> none  [the longest x1 5.23 us: body(): jnp.mean(as_float * as_float, axis=1, keepdims=True) + 1e-06]
  transfers between devices with their start and end apart: 3 -> 17, of which waited for: 2 -> 7; matrix products, arithmetic and copies ran while one was open for 25% -> 1% of each run, Pallas kernels for 0% -> 28%
where the time goes in v1:
time: 144 us; the launch traced here: 143 us
  starting transfers between devices  47.6 us (33%)
  Pallas kernels  44.1 us (31%)
  waiting for transfers between devices  30.3 us (21%)
  blocking collectives  16.8 us (12%)
  local copies, waits for them, and re-layouts  2.3 us (2%)
    ppermute x8, starting transfers between devices, onward(): moved.append(lax.ppermute(x, ('sp', 'tp'), around))  29.5 us
    all_to_all x1, blocking collectives, body(): lax.all_to_all(ends, 'sp', split_axis=0, concat_axis=0, tiled=True)  16.8 us
    ppermute x8, waiting for transfers between devices, onward(): moved.append(lax.ppermute(x, ('sp', 'tp'), around))  16.5 us
    pallas_call x2, Pallas kernels, recur(): pl.pallas_call(functools.partial(recur_kernel, first=first), grid=(steps,...  12.2 us
    ppermute x7, starting transfers between devices, across(): swapped.append(lax.ppermute(x, ('sp', 'tp'), swap))  12 us
    all_to_all x1, waiting for transfers between devices, body(): lax.all_to_all(sent, 'tp', split_axis=0, concat_axis=0, tiled=True)  11.2 us
    pallas_call x1, Pallas kernels, body(): pl.pallas_call(gate_kernel, grid=(rows // big,), in_specs=[moving(big, wi...  8.32 us
    pallas_call x1, Pallas kernels, body(): pl.pallas_call(input_kernel, grid=(rows // big,), in_specs=[moving(big, w...  7.8 us
  transfers between devices with their start and end apart: 17, of which 7 were waited for; matrix products, arithmetic and copies ran while one was open for 1% of the time, Pallas kernels for 28%

profile of v1, /device:TPU:33, one launch (start us, length us, event | category | flops | bytes accessed | tf_op | source)
XLA Modules:
  0.0 142.6 jit_solution(12424292090960970949)
XLA Ops:
  0.0 22.9 %collective-permute-start.1 = (bf16[128,2048]{1,0:T(8,128)(2,1)}, bf16[128,2048]{1,0:T(8,128)(2,1)S(1)}, u32[]{:S(2)}, u32[]{:S(2)}) collective-permute-start(bf16[128,2048]{1,0:T(8,128)(2,1)} %refs_0_.1), channel_id=1, source_target_pairs={{0,8},{1,121},{2,10},{3,123},{4,12},{5,125},{6,14},{7,127},{8,16},... | collective-permute-start | bytes 1572872 | tf_op jit(solution)/shard_map/ppermute | solution.py:227
  23.8 1.3 collective-permute-start
  25.1 1.3 compare_select_fusion
  26.4 7.8 %input.1.projected.refs_0_ = bf16[2048,256]{1,0:T(8,128)(2,1)} custom-call(bf16[2048,2048]{1,0:T(8,128)(2,1)} %tokens.2, f32[1,2048]{1,0:T(1,128)} %bitcast.6, bf16[2048,256]{1,0:T(8,128)(2,1)} %refs_2_.1), custom_call_target="tpu_custom_call" | custom-call | tf_op jit(solution)/shard_map/input/pallas_call | solution.py:254
  34.8 6.5 %recur.2 = (f32[2,2048,128]{2,1,0:T(8,128)}, f32[2,2048,128]{2,1,0:T(8,128)}, f32[1,8,256]{2,1,0:T(8,128)}) custom-call(bf16[2048,256]{1,0:T(8,128)(2,1)} %input.1.projected.refs_0_, f32[4,256]{1,0:T(4,128)} %taps.3, bf16[1,256,256]{2,1,0:T(8,128)(2,1)} %w_rate.3, bf16[1,256,256]{2,1,0:T(8,128)(2,1)} %w_inlet.3, f32[1,256]{1,0:T(1,128)} %bitcast.9, ...), custom_call_target="tpu_custom_call" | custom-call | tf_op jit(solution)/shard_map/recur/pallas_call | solution.py:281
  42.0 1.3 collective-permute-done.3.refs_6_
  43.3 6.6 %collective-permute-done.2.refs_2_ = bf16[128,2048]{1,0:T(8,128)(2,1)S(1)} collective-permute-done((bf16[128,2048]{1,0:T(8,128)(2,1)S(1)}, bf16[128,2048]{1,0:T(8,128)(2,1)S(1)}, u32[]{:S(2)}, u32[]{:S(2)}) %collective-permute-start.2) | collective-permute-done | bytes 524320 | tf_op jit(solution)/shard_map/ppermute | solution.py:227
  49.9 2.4 %collective-permute-start.5 = (bf16[128,2048]{1,0:T(8,128)(2,1)S(1)}, bf16[128,2048]{1,0:T(8,128)(2,1)S(1)}, u32[]{:S(2)}, u32[]{:S(2)}) collective-permute-start(bf16[128,2048]{1,0:T(8,128)(2,1)S(1)} %collective-permute-done.2.refs_2_), channel_id=1, source_target_pairs={{0,1},{1,0},{2,3},{3,2},{4,5},{5,4},{6,7},{7,6},{8,9},{9,8},{10,11... | collective-permute-start | bytes 1572872 | tf_op jit(solution)/shard_map/ppermute | solution.py:230
  52.3 5.8 %recur.3 = (f32[2,2048,128]{2,1,0:T(8,128)}, f32[2,2048,128]{2,1,0:T(8,128)}, f32[16,8,256]{2,1,0:T(8,128)}) custom-call(bf16[2048,256]{1,0:T(8,128)(2,1)} %input.1.projected.refs_0_, f32[4,256]{1,0:T(4,128)} %taps.3, bf16[1,256,256]{2,1,0:T(8,128)(2,1)} %w_rate.3, bf16[1,256,256]{2,1,0:T(8,128)(2,1)} %w_inlet.3, ...), custom_call_target="tpu_custom_call", output_to_operand_aliasing={{0}: (8, {}), {1}: (9, {})} | custom-call | tf_op jit(solution)/shard_map/recur/pallas_call | solution.py:281
  58.1 8.3 %gate.1 = f32[2048,256]{1,0:T(8,128)} custom-call(bf16[2048,2048]{1,0:T(8,128)(2,1)} %tokens.2, f32[1,2048]{1,0:T(1,128)} %bitcast.8, bf16[2048,256]{1,0:T(8,128)(2,1)} %w_gate.1), custom_call_target="tpu_custom_call" | custom-call | tf_op jit(solution)/shard_map/gate/pallas_call | solution.py:301
  66.8 2.8 %collective-permute-start.6 = (bf16[128,2048]{1,0:T(8,128)(2,1)S(1)}, bf16[128,2048]{1,0:T(8,128)(2,1)S(1)}, u32[]{:S(2)}, u32[]{:S(2)}) collective-permute-start(bf16[128,2048]{1,0:T(8,128)(2,1)S(1)} %collective-permute-done.4.refs_3_), channel_id=1, source_target_pairs={{0,8},{1,121},{2,10},{3,123},{4,12},{5,125},{6,14},{7,127},{8,16},... | collective-permute-start | bytes 1572872 | tf_op jit(solution)/shard_map/ppermute | solution.py:227
  69.5 16.8 %all_to_all.10.ends = f32[16,8,256]{2,1,0:T(8,128)} all-to-all(f32[16,8,256]{2,1,0:T(8,128)S(1)} %copy-done.12), channel_id=1, replica_groups=mesh['grp'=2,'sp'=16,'tp'=8] {'sp'}, dimensions={0} | all-to-all | bytes 262144 | tf_op jit(solution)/shard_map/all_to_all | solution.py:298
  86.3 4.9 %gated.1 = bf16[8,2,272,128]{3,2,1,0:T(8,128)(2,1)} custom-call(f32[2,2048,128]{2,1,0:T(8,128)} %get-tuple-element.34.state, f32[2,2048,128]{2,1,0:T(8,128)} %get-tuple-element.35.prod, f32[2048,256]{1,0:T(8,128)} %gate.1, f32[16,8,256]{2,1,0:T(8,128)} %all_to_all.10.ends, f32[1,256]{1,0:T(1,128)} %bitcast.11), custom_call_target="tpu_custom_call" | custom-call | tf_op jit(solution)/shard_map/gated/pallas_call | solution.py:311
  91.3 3.6 %collective-permute-start.9 = (bf16[128,2048]{1,0:T(8,128)(2,1)S(1)}, bf16[128,2048]{1,0:T(8,128)(2,1)S(1)}, u32[]{:S(2)}, u32[]{:S(2)}) collective-permute-start(bf16[128,2048]{1,0:T(8,128)(2,1)S(1)} %collective-permute-done.6.refs_4_), channel_id=1, source_target_pairs={{0,1},{1,0},{2,3},{3,2},{4,5},{5,4},{6,7},{7,6},{8,9},{9,8},{10,11... | collective-permute-start | bytes 1572872 | tf_op jit(solution)/shard_map/ppermute | solution.py:230
  96.1 4.9 %all-to-all-start.1 = ((bf16[8,2,272,128]{3,2,1,0:T(8,128)(2,1)}), bf16[8,2,272,128]{3,2,1,0:T(8,128)(2,1)S(1)}, u32[]{:S(2)}, u32[]{:S(2)}) async-start(bf16[8,2,272,128]{3,2,1,0:T(8,128)(2,1)} %gated.1), calls=%async_computation.1 | async-start | bytes 2228224 | tf_op jit(solution)/shard_map/all_to_all | solution.py:320
  101.0 2.3 %collective-permute-done.8.refs_5_ = bf16[128,2048]{1,0:T(8,128)(2,1)S(1)} collective-permute-done((bf16[128,2048]{1,0:T(8,128)(2,1)S(1)}, bf16[128,2048]{1,0:T(8,128)(2,1)S(1)}, u32[]{:S(2)}, u32[]{:S(2)}) %collective-permute-start.8) | collective-permute-done | bytes 524320 | tf_op jit(solution)/shard_map/ppermute | solution.py:227
  103.2 2.2 %collective-permute-start.11 = (bf16[128,2048]{1,0:T(8,128)(2,1)S(1)}, bf16[128,2048]{1,0:T(8,128)(2,1)}, u32[]{:S(2)}, u32[]{:S(2)}) collective-permute-start(bf16[128,2048]{1,0:T(8,128)(2,1)S(1)} %collective-permute-done.8.refs_5_), channel_id=1, source_target_pairs={{0,1},{1,0},{2,3},{3,2},{4,5},{5,4},{6,7},{7,6},{8,9},{9,8},{10,11... | collective-permute-start | bytes 1572872 | tf_op jit(solution)/shard_map/ppermute | solution.py:230
  105.4 11.2 %all-to-all-done.1 = bf16[8,2,272,128]{3,2,1,0:T(8,128)(2,1)S(1)} async-done(((bf16[8,2,272,128]{3,2,1,0:T(8,128)(2,1)}), bf16[8,2,272,128]{3,2,1,0:T(8,128)(2,1)S(1)}, u32[]{:S(2)}, u32[]{:S(2)}) %all-to-all-start.1) | async-done | bytes 1114144 | tf_op jit(solution)/shard_map/all_to_all | solution.py:320
  117.7 1.6 %collective-permute-start.12 = (bf16[128,2048]{1,0:T(8,128)(2,1)}, bf16[128,2048]{1,0:T(8,128)(2,1)}, u32[]{:S(2)}, u32[]{:S(2)}) collective-permute-start(bf16[128,2048]{1,0:T(8,128)(2,1)} %collective-permute-done.10.refs_0_), channel_id=1, source_target_pairs={{0,8},{1,121},{2,10},{3,123},{4,12},{5,125},{6,14},{7,127},{8,16},... | collective-permute-start | bytes 1572872 | tf_op jit(solution)/shard_map/ppermute | solution.py:227
  119.4 6.1 %early.1.sums = f32[256,2048]{1,0:T(8,128)} custom-call(bf16[16,272,128]{2,1,0:T(8,128)(2,1)} %bitcast.4, bf16[128,2048]{1,0:T(8,128)(2,1)} %refs_0_.1, bf16[128,2048]{1,0:T(8,128)(2,1)} %copy-done.1, bf16[128,2048]{1,0:T(8,128)(2,1)} %copy-done.3, bf16[128,2048]{1,0:T(8,128)(2,1)} %copy-done.5, bf16[128,2048]{1,0:T(8,128)(2,1)} %copy-done.7, ...), custom_call_target="tpu_custom_call" | custom-call | tf_op jit(solution)/shard_map/early/pallas_call | solution.py:328
  126.4 2.2 %collective-permute-start.15 = (bf16[128,2048]{1,0:T(8,128)(2,1)}, bf16[128,2048]{1,0:T(8,128)(2,1)S(1)}, u32[]{:S(2)}, u32[]{:S(2)}) collective-permute-start(bf16[128,2048]{1,0:T(8,128)(2,1)} %collective-permute-done.12.refs_1_), channel_id=1, source_target_pairs={{0,1},{1,0},{2,3},{3,2},{4,5},{5,4},{6,7},{7,6},{8,9},{9,8},{10,11... | collective-permute-start | bytes 1572872 | tf_op jit(solution)/shard_map/ppermute | solution.py:230
  129.0 1.3 collective-permute-done.15.refs_4_
  130.3 6.8 %collective-permute-done.14.refs_2_ = bf16[128,2048]{1,0:T(8,128)(2,1)S(1)} collective-permute-done((bf16[128,2048]{1,0:T(8,128)(2,1)}, bf16[128,2048]{1,0:T(8,128)(2,1)S(1)}, u32[]{:S(2)}, u32[]{:S(2)}) %collective-permute-start.14) | collective-permute-done | bytes 524320 | tf_op jit(solution)/shard_map/ppermute | solution.py:227
  137.9 4.7 %late.1 = bf16[256,2048]{1,0:T(8,128)(2,1)} custom-call(bf16[16,272,128]{2,1,0:T(8,128)(2,1)} %bitcast.5, f32[256,2048]{1,0:T(8,128)} %early.1.sums, bf16[128,2048]{1,0:T(8,128)(2,1)} %collective-permute-done.10.refs_0_, bf16[128,2048]{1,0:T(8,128)(2,1)} %collective-permute-done.12.refs_1_, bf16[128,2048]{1,0:T(8,128)(2,1)} %copy-done.11, ...), custom_call_target="tpu_custom_call" | custom-call | tf_op jit(solution)/shard_map/late/pallas_call | solution.py:338
  (48 shorter events, 6.9 us)
Async XLA Ops:
  0.0 41.2 %collective-permute-start.1 = (bf16[128,2048]{1,0:T(8,128)(2,1)}, bf16[128,2048]{1,0:T(8,128)(2,1)S(1)}, u32[]{:S(2)}, u32[]{:S(2)}) collective-permute-start(bf16[128,2048]{1,0:T(8,128)(2,1)} %refs_0_.1), channel_id=1, source_target_pairs={{0,8},{1,121},{2,10},{3,123},{4,12},{5,125},{6,14},{7,127},{8,16},... | collective-permute-start | bytes 1572872 | tf_op jit(solution)/shard_map/ppermute | solution.py:227
  23.8 10.4 %collective-permute-start = (bf16[16,2048]{1,0:T(8,128)(2,1)S(1)}, bf16[16,2048]{1,0:T(8,128)(2,1)S(1)}, u32[]{:S(2)}, u32[]{:S(2)}) collective-permute-start(bf16[16,2048]{1,0:T(8,128)(2,1)S(1)} %slice.3), channel_id=1, source_target_pairs={{0,8},{8,16},{16,24},{24,32},{32,40},{40,48},{48,56},{56,64},{64,7... | collective-permute-start | bytes 196616 | tf_op jit(solution)/shard_map/ppermute | solution.py:249
  41.3 16.8 %copy-start.1 = (bf16[128,2048]{1,0:T(8,128)(2,1)}, bf16[128,2048]{1,0:T(8,128)(2,1)S(1)}, u32[]{:S(2)}) copy-start(bf16[128,2048]{1,0:T(8,128)(2,1)S(1)} %collective-permute-done.1.refs_1_) | copy-start | bytes 1572868
  41.3 2.0 %collective-permute-start.3 = (bf16[128,2048]{1,0:T(8,128)(2,1)S(1)}, bf16[128,2048]{1,0:T(8,128)(2,1)S(1)}, u32[]{:S(2)}, u32[]{:S(2)}) collective-permute-start(bf16[128,2048]{1,0:T(8,128)(2,1)S(1)} %collective-permute-done.1.refs_1_), channel_id=1, source_target_pairs={{0,1},{1,0},{2,3},{3,2},{4,5},{5,4},{6,7},{7,6},{8,9},{9,8},{10,11... | collective-permute-start | bytes 1572872 | tf_op jit(solution)/shard_map/ppermute | solution.py:230
  41.4 8.4 %collective-permute-start.2 = (bf16[128,2048]{1,0:T(8,128)(2,1)S(1)}, bf16[128,2048]{1,0:T(8,128)(2,1)S(1)}, u32[]{:S(2)}, u32[]{:S(2)}) collective-permute-start(bf16[128,2048]{1,0:T(8,128)(2,1)S(1)} %collective-permute-done.1.refs_1_), channel_id=1, source_target_pairs={{0,8},{1,121},{2,10},{3,123},{4,12},{5,125},{6,14},{7,127},{8,16},... | collective-permute-start | bytes 1572872 | tf_op jit(solution)/shard_map/ppermute | solution.py:227
  49.9 16.6 %collective-permute-start.5 = (bf16[128,2048]{1,0:T(8,128)(2,1)S(1)}, bf16[128,2048]{1,0:T(8,128)(2,1)S(1)}, u32[]{:S(2)}, u32[]{:S(2)}) collective-permute-start(bf16[128,2048]{1,0:T(8,128)(2,1)S(1)} %collective-permute-done.2.refs_2_), channel_id=1, source_target_pairs={{0,1},{1,0},{2,3},{3,2},{4,5},{5,4},{6,7},{7,6},{8,9},{9,8},{10,11... | collective-permute-start | bytes 1572872 | tf_op jit(solution)/shard_map/ppermute | solution.py:230
  52.3 14.1 %collective-permute-start.4 = (bf16[128,2048]{1,0:T(8,128)(2,1)S(1)}, bf16[128,2048]{1,0:T(8,128)(2,1)S(1)}, u32[]{:S(2)}, u32[]{:S(2)}) collective-permute-start(bf16[128,2048]{1,0:T(8,128)(2,1)S(1)} %collective-permute-done.2.refs_2_), channel_id=1, source_target_pairs={{0,8},{1,121},{2,10},{3,123},{4,12},{5,125},{6,14},{7,127},{8,16},... | collective-permute-start | bytes 1572872 | tf_op jit(solution)/shard_map/ppermute | solution.py:227
  66.4 24.8 %copy-start.4 = (bf16[128,2048]{1,0:T(8,128)(2,1)}, bf16[128,2048]{1,0:T(8,128)(2,1)S(1)}, u32[]{:S(2)}) copy-start(bf16[128,2048]{1,0:T(8,128)(2,1)S(1)} %collective-permute-done.5.refs_7_) | copy-start | bytes 1572868
  66.4 24.8 %copy-start.5 = (bf16[128,2048]{1,0:T(8,128)(2,1)}, bf16[128,2048]{1,0:T(8,128)(2,1)S(1)}, u32[]{:S(2)}) copy-start(bf16[128,2048]{1,0:T(8,128)(2,1)S(1)} %collective-permute-done.4.refs_3_) | copy-start | bytes 1572868
  66.4 24.8 %collective-permute-start.7 = (bf16[128,2048]{1,0:T(8,128)(2,1)S(1)}, bf16[128,2048]{1,0:T(8,128)(2,1)S(1)}, u32[]{:S(2)}, u32[]{:S(2)}) collective-permute-start(bf16[128,2048]{1,0:T(8,128)(2,1)S(1)} %collective-permute-done.4.refs_3_), channel_id=1, source_target_pairs={{0,1},{1,0},{2,3},{3,2},{4,5},{5,4},{6,7},{7,6},{8,9},{9,8},{10,11... | collective-permute-start | bytes 1572872 | tf_op jit(solution)/shard_map/ppermute | solution.py:230
  66.8 24.5 %collective-permute-start.6 = (bf16[128,2048]{1,0:T(8,128)(2,1)S(1)}, bf16[128,2048]{1,0:T(8,128)(2,1)S(1)}, u32[]{:S(2)}, u32[]{:S(2)}) collective-permute-start(bf16[128,2048]{1,0:T(8,128)(2,1)S(1)} %collective-permute-done.4.refs_3_), channel_id=1, source_target_pairs={{0,8},{1,121},{2,10},{3,123},{4,12},{5,125},{6,14},{7,127},{8,16},... | collective-permute-start | bytes 1572872 | tf_op jit(solution)/shard_map/ppermute | solution.py:227
  91.3 28.1 %copy-start.6 = (bf16[128,2048]{1,0:T(8,128)(2,1)}, bf16[128,2048]{1,0:T(8,128)(2,1)S(1)}, u32[]{:S(2)}) copy-start(bf16[128,2048]{1,0:T(8,128)(2,1)S(1)} %collective-permute-done.7.refs_8_) | copy-start | bytes 1572868
  91.3 28.1 %copy-start.7 = (bf16[128,2048]{1,0:T(8,128)(2,1)}, bf16[128,2048]{1,0:T(8,128)(2,1)S(1)}, u32[]{:S(2)}) copy-start(bf16[128,2048]{1,0:T(8,128)(2,1)S(1)} %collective-permute-done.6.refs_4_) | copy-start | bytes 1572868
  91.3 9.7 %collective-permute-start.9 = (bf16[128,2048]{1,0:T(8,128)(2,1)S(1)}, bf16[128,2048]{1,0:T(8,128)(2,1)S(1)}, u32[]{:S(2)}, u32[]{:S(2)}) collective-permute-start(bf16[128,2048]{1,0:T(8,128)(2,1)S(1)} %collective-permute-done.6.refs_4_), channel_id=1, source_target_pairs={{0,1},{1,0},{2,3},{3,2},{4,5},{5,4},{6,7},{7,6},{8,9},{9,8},{10,11... | collective-permute-start | bytes 1572872 | tf_op jit(solution)/shard_map/ppermute | solution.py:230
  94.9 8.3 %collective-permute-start.8 = (bf16[128,2048]{1,0:T(8,128)(2,1)S(1)}, bf16[128,2048]{1,0:T(8,128)(2,1)S(1)}, u32[]{:S(2)}, u32[]{:S(2)}) collective-permute-start(bf16[128,2048]{1,0:T(8,128)(2,1)S(1)} %collective-permute-done.6.refs_4_), channel_id=1, source_target_pairs={{0,8},{1,121},{2,10},{3,123},{4,12},{5,125},{6,14},{7,127},{8,16},... | collective-permute-start | bytes 1572872 | tf_op jit(solution)/shard_map/ppermute | solution.py:227
  96.1 20.5 %all-to-all-start.1 = ((bf16[8,2,272,128]{3,2,1,0:T(8,128)(2,1)}), bf16[8,2,272,128]{3,2,1,0:T(8,128)(2,1)S(1)}, u32[]{:S(2)}, u32[]{:S(2)}) async-start(bf16[8,2,272,128]{3,2,1,0:T(8,128)(2,1)} %gated.1), calls=%async_computation.1 | async-start | bytes 2228224 | tf_op jit(solution)/shard_map/all_to_all | solution.py:320
  101.0 18.4 %copy-start.8 = (bf16[128,2048]{1,0:T(8,128)(2,1)}, bf16[128,2048]{1,0:T(8,128)(2,1)S(1)}, u32[]{:S(2)}) copy-start(bf16[128,2048]{1,0:T(8,128)(2,1)S(1)} %collective-permute-done.9.refs_9_) | copy-start | bytes 1572868
  103.2 16.1 %copy-start.9 = (bf16[128,2048]{1,0:T(8,128)(2,1)}, bf16[128,2048]{1,0:T(8,128)(2,1)S(1)}, u32[]{:S(2)}) copy-start(bf16[128,2048]{1,0:T(8,128)(2,1)S(1)} %collective-permute-done.8.refs_5_) | copy-start | bytes 1572868
  103.2 13.4 %collective-permute-start.11 = (bf16[128,2048]{1,0:T(8,128)(2,1)S(1)}, bf16[128,2048]{1,0:T(8,128)(2,1)}, u32[]{:S(2)}, u32[]{:S(2)}) collective-permute-start(bf16[128,2048]{1,0:T(8,128)(2,1)S(1)} %collective-permute-done.8.refs_5_), channel_id=1, source_target_pairs={{0,1},{1,0},{2,3},{3,2},{4,5},{5,4},{6,7},{7,6},{8,9},{9,8},{10,11... | collective-permute-start | bytes 1572872 | tf_op jit(solution)/shard_map/ppermute | solution.py:230
  105.4 11.2 %collective-permute-start.10 = (bf16[128,2048]{1,0:T(8,128)(2,1)S(1)}, bf16[128,2048]{1,0:T(8,128)(2,1)}, u32[]{:S(2)}, u32[]{:S(2)}) collective-permute-start(bf16[128,2048]{1,0:T(8,128)(2,1)S(1)} %collective-permute-done.8.refs_5_), channel_id=1, source_target_pairs={{0,8},{1,121},{2,10},{3,123},{4,12},{5,125},{6,14},{7,127},{8,16},... | collective-permute-start | bytes 1572872 | tf_op jit(solution)/shard_map/ppermute | solution.py:227
  116.6 8.9 %collective-permute-start.13 = (bf16[128,2048]{1,0:T(8,128)(2,1)}, bf16[128,2048]{1,0:T(8,128)(2,1)}, u32[]{:S(2)}, u32[]{:S(2)}) collective-permute-start(bf16[128,2048]{1,0:T(8,128)(2,1)} %collective-permute-done.10.refs_0_), channel_id=1, source_target_pairs={{0,1},{1,0},{2,3},{3,2},{4,5},{5,4},{6,7},{7,6},{8,9},{9,8},{10,11... | collective-permute-start | bytes 1572872 | tf_op jit(solution)/shard_map/ppermute | solution.py:230
  117.7 8.6 %collective-permute-start.12 = (bf16[128,2048]{1,0:T(8,128)(2,1)}, bf16[128,2048]{1,0:T(8,128)(2,1)}, u32[]{:S(2)}, u32[]{:S(2)}) collective-permute-start(bf16[128,2048]{1,0:T(8,128)(2,1)} %collective-permute-done.10.refs_0_), channel_id=1, source_target_pairs={{0,8},{1,121},{2,10},{3,123},{4,12},{5,125},{6,14},{7,127},{8,16},... | collective-permute-start | bytes 1572872 | tf_op jit(solution)/shard_map/ppermute | solution.py:227
  126.4 4.0 %collective-permute-start.15 = (bf16[128,2048]{1,0:T(8,128)(2,1)}, bf16[128,2048]{1,0:T(8,128)(2,1)S(1)}, u32[]{:S(2)}, u32[]{:S(2)}) collective-permute-start(bf16[128,2048]{1,0:T(8,128)(2,1)} %collective-permute-done.12.refs_1_), channel_id=1, source_target_pairs={{0,1},{1,0},{2,3},{3,2},{4,5},{5,4},{6,7},{7,6},{8,9},{9,8},{10,11... | collective-permute-start | bytes 1572872 | tf_op jit(solution)/shard_map/ppermute | solution.py:230
  128.6 8.5 %collective-permute-start.14 = (bf16[128,2048]{1,0:T(8,128)(2,1)}, bf16[128,2048]{1,0:T(8,128)(2,1)S(1)}, u32[]{:S(2)}, u32[]{:S(2)}) collective-permute-start(bf16[128,2048]{1,0:T(8,128)(2,1)} %collective-permute-done.12.refs_1_), channel_id=1, source_target_pairs={{0,8},{1,121},{2,10},{3,123},{4,12},{5,125},{6,14},{7,127},{8,16},... | collective-permute-start | bytes 1572872 | tf_op jit(solution)/shard_map/ppermute | solution.py:227
  (7 other events, 45.4 us)

commit v2 on v1

v2 whole, which is shorter than its diff:
```python
import functools

import jax
import jax.numpy as jnp
from jax import lax
from jax.experimental import pallas as pl
from jax.experimental.pallas import tpu as pltpu
from jax.sharding import PartitionSpec as P

F32 = jnp.float32
BF16 = jnp.bfloat16
BLOCK = 256
SEG = 8
EXTRA = 16
EPS = 1e-06
STREAMS = 2
EXCHANGE = (2, 1, 3, 0)


def on_chip(x):
    return pltpu.with_memory_space_constraint(x, pltpu.VMEM)


def limit(mebibytes):
    return pltpu.CompilerParams(vmem_limit_bytes=mebibytes << 20)


def inverse_norm(rows):
    wide = rows.astype(F32)
    return lax.rsqrt(jnp.mean(wide * wide, axis=1, keepdims=True) + EPS)


def thirds(x):
    top = x.astype(BF16)
    rest = x - top.astype(F32)
    middle = rest.astype(BF16)
    return [top, middle, (rest - middle.astype(F32)).astype(BF16)]


def as_column(row, width):
    pieces = thirds(row) + [jnp.zeros((13, row.shape[1]), BF16)]
    return lax.dot_general(
        jnp.concatenate(pieces, 0), jnp.ones((16, width), BF16), (((0,), (0,)), ((), ())),
        preferred_element_type=F32,
    )


def softplus(x):
    e = jnp.exp(-jnp.abs(x))
    series = 1.0 / 6.0 - e * (1.0 / 7.0)
    for k in (5, 4, 3, 2):
        series = 1.0 / k - e * series
    small = e * (1.0 - e * series)
    return jnp.maximum(x, 0.0) + jnp.where(e < 0.06, small, jnp.log(1.0 + e))


def minus_expm1(y, exp_y):
    series = 1.0 / 120.0 + y * (1.0 / 720.0)
    series = 1.0 / 24.0 + y * series
    series = 1.0 / 6.0 + y * series
    series = 0.5 + y * series
    series = -y * (1.0 + y * series)
    return jnp.where(y > -0.25, series, 1.0 - exp_y)


def gelu(x):
    inner = 0.7978845608028654 * (x + 0.044715 * (x * x * x))
    return 0.5 * x * (1.0 + jnp.tanh(inner))


def logistic(x):
    return 1.0 / (1.0 + jnp.exp(-x))


def shifted_down(x, by, fill):
    rows = lax.broadcasted_iota(jnp.int32, x.shape, 0)
    return jnp.where(rows < by, fill, pltpu.roll(x, by, 0))


def branch_product(rows, weights):
    product = jnp.dot(rows, weights, preferred_element_type=F32)
    return (product * inverse_norm(rows)).astype(BF16)


def scaled_weights(weights, gain):
    return (weights[...].astype(F32) * as_column(gain[...], weights.shape[1])).astype(BF16)


def chunk_copy(source, target, sems, k):
    chunk = source.shape[0] // sems.shape[0]
    at = pl.ds(pl.multiple_of(k * chunk, chunk), chunk)
    return at, pltpu.make_async_copy(source.at[at, :], target.at[at, :], sems.at[k])


def input_kernel(tokens, gain, w_input, projected, scaled, kept, sems):
    count = sems.shape[0]
    for k in range(count):
        chunk_copy(tokens, kept, sems, k)[1].start()
    scaled[...] = scaled_weights(w_input, gain)

    def part(k, _):
        at, copy = chunk_copy(tokens, kept, sems, k)
        copy.wait()
        projected[at, :] = branch_product(kept[at, :], scaled[...])
        return 0

    lax.fori_loop(0, count, part, 0)


def gate_kernel(tokens, gain, w_gate, gate, scaled, kept, made, sems, out_sems):
    count = sems.shape[0]
    for k in range(count):
        chunk_copy(tokens, kept, sems, k)[1].start()
    scaled[...] = scaled_weights(w_gate, gain)

    def part(k, _):
        at, copy = chunk_copy(tokens, kept, sems, k)
        copy.wait()
        made[at, :] = gelu(branch_product(kept[at, :], scaled[...]).astype(F32))
        chunk_copy(made, gate, out_sems, k)[1].start()
        return 0

    lax.fori_loop(0, count, part, 0)
    for k in range(count):
        chunk_copy(made, gate, out_sems, k)[1].wait()


def recur_kernel(projected, taps, w_rate, w_inlet, decay_param, bias, *refs, first):
    if first:
        halo, scaled, refs = *refs[:2], refs[2:]
    else:
        begun, refs = refs[0], refs[1:]
    state_out, prod_out, ends, conv_buf, decay_buf, drive_buf, carry, state, prod, sems = refs
    if first:
        conv_buf[0:8, :] = branch_product(halo[...], scaled[...]).astype(F32)[8:16]
        head_row = lax.broadcasted_iota(jnp.int32, carry.shape, 0) == 0
        carry[...] = jnp.where(head_row, 1.0, 0.0)
    else:
        middle = projected.shape[0] // 2
        conv_buf[0:8, :] = projected[middle - 16 : middle, :].astype(F32)[8:16]
        carry[...] = begun[0]
    soft = softplus(-decay_param[...])
    blocks = projected.shape[0] // 2 // BLOCK
    segs = BLOCK // SEG

    def leaving(k):
        at = (slice(None), pl.ds(pl.multiple_of(k * BLOCK, BLOCK), BLOCK), slice(None))
        return [
            pltpu.make_async_copy(ref.at[at], out.at[at], sems.at[n, k])
            for n, (ref, out) in enumerate(((state, state_out), (prod, prod_out)))
        ]

    def part(k, _):
        block = k + (0 if first else blocks)
        start = pl.multiple_of(block * BLOCK, BLOCK)
        conv_buf[8 : BLOCK + 8, :] = projected[pl.ds(start, BLOCK), :].astype(F32)
        summed = conv_buf[5 : BLOCK + 5, :] * taps[0:1, :]
        for tap in range(1, 4):
            summed = summed + conv_buf[5 + tap : BLOCK + 5 + tap, :] * taps[tap : tap + 1, :]
        conv_buf[0:8, :] = conv_buf[BLOCK : BLOCK + 8, :]
        convolved = summed.astype(BF16)
        rate = logistic(jnp.dot(convolved, w_rate[0], preferred_element_type=F32))
        inlet = logistic(jnp.dot(convolved, w_inlet[0], preferred_element_type=F32))
        log_decay = -8.0 * rate * soft + as_column(bias[0:1, pl.ds(start, BLOCK)], rate.shape[1])
        decay = jnp.exp(log_decay)
        drive = jnp.sqrt(minus_expm1(2.0 * log_decay, decay * decay)) * inlet * convolved.astype(F32)
        for half in range(2):
            lanes = slice(half * 128, half * 128 + 128)
            decay_buf[half] = decay[:, lanes]
            drive_buf[half] = drive[:, lanes]
            row = [(half, pl.ds(r, segs, stride=SEG), slice(None)) for r in range(SEG)]
            p, h = decay_buf[row[0]], drive_buf[row[0]]
            inner = [(p, h)]
            for r in range(1, SEG):
                a = decay_buf[row[r]]
                h = a * h + drive_buf[row[r]]
                p = a * p
                inner.append((p, h))
            by = 1
            while by < segs:
                h = h + p * shifted_down(h, by, 0.0)
                p = p * shifted_down(p, by, 1.0)
                by *= 2
            carry_p, carry_h = carry[0:1, lanes], carry[1:2, lanes]
            start_h = shifted_down(h, 1, 0.0) + shifted_down(p, 1, 1.0) * carry_h
            start_p = shifted_down(p, 1, 1.0) * carry_p
            carry[1:2, lanes] = h[segs - 1 : segs, :] + p[segs - 1 : segs, :] * carry_h
            carry[0:1, lanes] = p[segs - 1 : segs, :] * carry_p
            for r in range(SEG):
                p, h = inner[r]
                at = (half, pl.ds(pl.multiple_of(k * BLOCK, BLOCK) + r, segs, stride=SEG), slice(None))
                state[at] = h + p * start_h
                prod[at] = p * start_p
        for copy in leaving(k):
            copy.start()
        return 0

    lax.fori_loop(0, blocks, part, 0)
    for k in range(blocks):
        for copy in leaving(k):
            copy.wait()
    ends[...] = jnp.broadcast_to(carry[...][None], ends.shape)


def gated_kernel(state_1, state_2, prod_1, prod_2, gate, ends, gain, sent, incoming, states, prods, gates, sems):
    count = sent.shape[0]
    copies = []
    for d in range(count):
        state, prod = (state_1, prod_1) if d < count // 2 else (state_2, prod_2)
        near = pl.ds(d % (count // 2) * BLOCK, BLOCK)
        at = pl.ds(d * BLOCK, BLOCK)
        copies.append(
            [
                pltpu.make_async_copy(state.at[:, near, :], states.at[:, at, :], sems.at[0, d]),
                pltpu.make_async_copy(prod.at[:, near, :], prods.at[:, at, :], sems.at[1, d]),
                pltpu.make_async_copy(gate.at[at, :], gates.at[at, :], sems.at[2, d]),
            ]
        )
        for copy in copies[-1]:
            copy.start()
    span = lax.axis_index("sp")
    total = jnp.zeros((1, gain.shape[1]), F32)
    for k in range(ends.shape[0]):
        total = jnp.where(k < span, ends[k, 0:1, :] * total + ends[k, 1:2, :], total)
    incoming[...] = jnp.broadcast_to(total, incoming.shape)

    ones = jnp.ones((8, 128), BF16)
    over = (((1,), (1,)), ((), ()))
    for d in range(count):
        for copy in copies[d]:
            copy.wait()
        rows = slice(d * BLOCK, d * BLOCK + BLOCK)
        total = jnp.zeros((8, BLOCK), F32)
        for half in range(2):
            lanes = slice(half * 128, half * 128 + 128)
            gated = (states[half, rows, :] + prods[half, rows, :] * incoming[0:1, lanes]) * gates[rows, lanes]
            sent[d, half, 0:BLOCK, :] = (gated * gain[:, lanes]).astype(BF16)
            square = gated * gated
            high = square.astype(BF16)
            low = (square - high.astype(F32)).astype(BF16)
            total = total + lax.dot_general(ones, high, over, preferred_element_type=F32)
            total = total + lax.dot_general(ones, low, over, preferred_element_type=F32)
        top = total.astype(BF16).astype(F32)
        row = lax.broadcasted_iota(jnp.int32, total.shape, 0)
        lines = jnp.where(row == 0, top, jnp.where(row == 1, total - top, 0.0))
        lines = jnp.concatenate([lines, jnp.zeros_like(lines)], 0).astype(BF16)
        for half in range(2):
            sent[d, half, BLOCK : BLOCK + EXTRA, :] = lines[:, half * 128 : half * 128 + 128]


def product(arrived, places, blocks, low, step):
    mixed = jnp.concatenate([arrived[place, 0:BLOCK, :] for place in places], 1)
    weights = jnp.concatenate([block[:, low : low + step] for block in blocks], 0)
    return jnp.dot(mixed, weights, preferred_element_type=F32)


def places_of(offsets, spans):
    span, core = lax.axis_index("sp"), lax.axis_index("tp") % 2
    return [lax.rem(span + spans + jnp.where(core == 0, k, -k), spans) for k in offsets]


def joined(blocks, depth):
    whole, parts = [], []
    for block in blocks:
        parts.append(block)
        if sum(part.shape[0] for part in parts) == depth:
            whole.append(parts)
            parts = []
    return whole


def product(arrived, places, groups, low, step):
    mixed = jnp.concatenate([arrived[place, 0:BLOCK, :] for place in places], 1)
    weights = jnp.concatenate([part[:, low : low + step] for parts in groups for part in parts], 0)
    return jnp.dot(mixed, weights, preferred_element_type=F32)


def early_kernel(arrived, *refs, offsets, spans, depth):
    groups, out = joined(refs[:-1], depth), refs[-1]
    places = places_of(offsets, spans)
    step = 512
    for low in range(0, out.shape[1], step):
        out[:, low : low + step] = product(arrived, places, groups, low, step)


def late_kernel(arrived, sums, *refs, offsets, spans, depth, channels):
    groups, out = joined(refs[:-1], depth), refs[-1]
    places = places_of(offsets, spans)
    ones = jnp.ones((arrived.shape[0] // 2 * EXTRA, 128), BF16)
    square = []
    for half in range(2):
        lines = [arrived[k, BLOCK : BLOCK + EXTRA, :] for k in range(half, arrived.shape[0], 2)]
        square.append(
            lax.dot_general(
                jnp.concatenate(lines, 0), ones, (((0,), (0,)), ((), ())), preferred_element_type=F32
            )
        )
    scale = lax.rsqrt(jnp.concatenate(square, 0)[:, 0:1] / channels + EPS)
    step = 512
    for low in range(0, out.shape[1], step):
        acc = sums[:, low : low + step] + product(arrived, places, groups, low, step)
        out[:, low : low + step] = (acc * scale).astype(BF16)


def tie(*values):
    return lax.optimization_barrier(values)


def body(
    tokens, in_gain, w_input, w_gate, conv_taps, w_rate, w_inlet, decay_param, decay_bias, out_gain, w_out
):
    rows, width = tokens.shape
    head = w_input.shape[1]
    spans, heads = lax.axis_size("sp"), lax.axis_size("tp")
    depth, out_width = w_out.shape
    reach = spans // 2

    around = []
    swap = []
    for z in range(spans):
        for t in range(heads):
            ahead = (z + 1) % spans if t % 2 == 0 else (z - 1) % spans
            around.append((z * heads + t, ahead * heads + t))
            swap.append((z * heads + t, z * heads + t + 1 - 2 * (t % 2)))

    moved, swapped = [], []

    def onward(parts):
        moved.append([lax.ppermute(part, ("sp", "tp"), around) for part in parts])

    def across(parts):
        swapped.append([lax.ppermute(part, ("sp", "tp"), swap) for part in parts])

    def advance(value, pieces=1):
        before = swapped[-1] if swapped else []
        value, *rest = tie(value, *before, *moved[-1][:1])
        if swapped:
            swapped[-1] = rest[:-1]
        moved[-1] = rest[-1:] + moved[-1][1:]
        if len(moved) < reach:
            parts = moved[-1]
            if len(parts) < pieces:
                cut = depth // pieces
                parts = [parts[0][k * cut : k * cut + cut] for k in range(pieces)]
            onward(parts)
            across(moved[-2])
        return value

    fixed = pl.BlockSpec(memory_space=pltpu.VMEM)
    hbm = pl.BlockSpec(memory_space=pltpu.HBM)
    onward([w_out])
    halo = lax.ppermute(tokens[rows - 16 :], "sp", [(i, i + 1) for i in range(spans - 1)])
    gain_row = in_gain.reshape(1, width)

    in_hbm = lambda x: pltpu.with_memory_space_constraint(x, pltpu.HBM)
    projected, scaled = pl.pallas_call(
        input_kernel,
        in_specs=[hbm, fixed, fixed],
        out_specs=[fixed] * 2,
        out_shape=[pltpu.VMEM((rows, head), BF16), pltpu.VMEM((width, head), BF16)],
        scratch_shapes=[pltpu.VMEM((rows, width), BF16), pltpu.SemaphoreType.DMA((4,))],
        compiler_params=limit(16),
        name="input",
    )(in_hbm(tokens), gain_row, w_input)

    half_rows = rows // 2

    def recur(first, *extra):
        many = 1 if first else spans
        half_shape = (2, half_rows, head // 2)
        return pl.pallas_call(
            functools.partial(recur_kernel, first=first),
            in_specs=[fixed] * (6 + len(extra)),
            out_specs=[hbm, hbm, fixed],
            out_shape=[
                pltpu.HBM(half_shape, F32), pltpu.HBM(half_shape, F32),
                jax.ShapeDtypeStruct((many, 8, head), F32),
            ],
            scratch_shapes=[
                pltpu.VMEM((BLOCK + 8, head), F32), pltpu.VMEM((2, BLOCK, head // 2), F32),
                pltpu.VMEM((2, BLOCK, head // 2), F32), pltpu.VMEM((8, head), F32),
                pltpu.VMEM(half_shape, F32), pltpu.VMEM(half_shape, F32),
                pltpu.SemaphoreType.DMA((2, half_rows // BLOCK)),
            ],
            compiler_params=limit(12),
            name="recur",
        )(on_chip(projected), conv_taps, w_rate, w_inlet, decay_param.reshape(1, head), decay_bias, *extra)

    projected = advance(projected)
    state_1, prod_1, begun = recur(True, halo, on_chip(scaled))
    state_2, prod_2, ends = recur(False, begun)
    ends = advance(ends)
    all_ends = lax.all_to_all(ends, "sp", split_axis=0, concat_axis=0, tiled=True)
    late_tokens, _ = tie(tokens, ends)
    gate = pl.pallas_call(
        gate_kernel,
        in_specs=[hbm, fixed, fixed],
        out_specs=hbm,
        out_shape=pltpu.HBM((rows, head), F32),
        scratch_shapes=[
            pltpu.VMEM((width, head), BF16), pltpu.VMEM((rows, width), BF16), pltpu.VMEM((rows, head), F32),
            pltpu.SemaphoreType.DMA((4,)), pltpu.SemaphoreType.DMA((4,)),
        ],
        compiler_params=limit(20),
        name="gate",
    )(in_hbm(late_tokens), gain_row, w_gate)
    gate = advance(gate)

    sent = pl.pallas_call(
        gated_kernel,
        in_specs=[hbm] * 5 + [fixed] * 2,
        out_specs=fixed,
        out_shape=pltpu.VMEM((heads, 2, BLOCK + EXTRA, head // 2), BF16),
        scratch_shapes=[
            pltpu.VMEM((8, head), F32), pltpu.VMEM((2, rows, head // 2), F32),
            pltpu.VMEM((2, rows, head // 2), F32), pltpu.VMEM((rows, head), F32),
            pltpu.SemaphoreType.DMA((3, heads)),
        ],
        compiler_params=limit(12),
        name="gated",
    )(*map(in_hbm, (state_1, state_2, prod_1, prod_2, gate)), all_ends, out_gain.reshape(1, head))
    seat = lax.axis_index("tp")
    chips = heads // 2
    arrived = lax.dynamic_slice_in_dim(sent, seat, 1, 0)
    arrived = lax.dynamic_update_slice_in_dim(jnp.zeros_like(sent), arrived, seat, 0)
    order = [(dx, dc) for dx in EXCHANGE for dc in range(2) if (dx, dc) != (0, 0)]
    moves = []
    for dx, dc in order:
        to = lambda t: (t // 2 + dx) % chips * 2 + (t % 2 + dc) % 2
        part = lax.dynamic_slice_in_dim(sent, to(seat), 1, 0)
        moves.append(lax.ppermute(part, "tp", [(t, to(t)) for t in range(heads)]))
    for (dx, dc), part in zip(order, moves):
        source = (seat // 2 - dx + chips) % chips * 2 + (seat % 2 + dc) % 2
        arrived = lax.dynamic_update_slice_in_dim(arrived, part, source, 0)
    holding = sent
    while len(moved) < reach - 2:
        holding = advance(holding, STREAMS)
    arrived = arrived.reshape(2 * heads, BLOCK + EXTRA, head // 2)
    arrived = advance(arrived, STREAMS)
    flat = lambda groups: [on_chip(part) for parts in groups for part in parts]
    done = len(swapped) - 1
    offsets = [0] + [-k for k in range(1, done + 1)] + list(range(1, done + 1))
    blocks = [on_chip(w_out)] + flat(moved[:done]) + flat(swapped[:done])
    sums = pl.pallas_call(
        functools.partial(early_kernel, offsets=offsets, spans=spans, depth=depth),
        in_specs=[fixed] * (1 + len(blocks)),
        out_specs=fixed,
        out_shape=pltpu.VMEM((BLOCK, out_width), F32),
        compiler_params=limit(16),
        name="early",
    )(arrived, *blocks)
    while len(moved) < reach:
        sums = advance(sums, STREAMS)
    offsets = [-k for k in range(done + 1, reach + 1)] + list(range(done + 1, reach))
    blocks = flat(moved[done:]) + flat(swapped[done:])
    return pl.pallas_call(
        functools.partial(late_kernel, offsets=offsets, spans=spans, depth=depth, channels=heads * head),
        in_specs=[fixed] * (2 + len(blocks)),
        out_specs=fixed,
        out_shape=jax.ShapeDtypeStruct((BLOCK, out_width), BF16),
        compiler_params=limit(16),
        name="late",
    )(arrived, on_chip(sums), *blocks)


def solution(mesh):
    return jax.shard_map(
        body,
        mesh=mesh,
        in_specs=(
            P(("grp", "sp"), None), P(), P(None, "tp"), P(None, "tp"), P(None, "tp"),
            P("tp", None, None), P("tp", None, None), P("tp"), P("tp", ("grp", "sp")), P("tp"), P("sp", None),
        ),
        out_specs=P(("grp", "sp", "tp"), None),
        check_vma=False,
    )
```

time: 144 us -> 122 us (0.85)
  starting transfers between devices: 47.6 us -> 72.3 us
  blocking collectives: 16.8 us -> 0 us
  Pallas kernels: 44.1 us -> 28.9 us
  waiting for transfers between devices: 30.3 us -> 15.5 us
    ppermute x15 -> x29, starting transfers between devices: 41.5 us -> 66.7 us  [the longest x12 44.7 us: onward(): moved.append([lax.ppermute(part, ('sp', 'tp'), around) for part in parts])]
    all_to_all x1 -> x0, blocking collectives: 16.8 us -> none  [body(): lax.all_to_all(ends, 'sp', split_axis=0, concat_axis=0, tiled=True)]
    all_to_all x1, waiting for transfers between devices: 11.2 us -> 0.91 us  [body(): lax.all_to_all(ends, 'sp', split_axis=0, concat_axis=0, tiled=True)]
    pallas_call x5, Pallas kernels: 33.3 us -> 24 us  [the longest x2 9.57 us: recur(): pl.pallas_call(functools.partial(recur_kernel, first=first), in_specs=[fi...]
    ppermute x15 -> x29, waiting for transfers between devices: 19.1 us -> 12.7 us  [the longest x7 6.49 us: body(): moves.append(lax.ppermute(part, 'tp', [(t, to(t)) for t in range(heads)]))]
    pallas_call x1, Pallas kernels: 6.13 us -> 2.86 us  [body(): pl.pallas_call(functools.partial(early_kernel, offsets=offsets, spans=spa...]
    pallas_call x1, Pallas kernels: 4.67 us -> 2.03 us  [body(): pl.pallas_call(functools.partial(late_kernel, offsets=offsets, spans=span...]
    ppermute x1, waiting for transfers between devices: 0.01 us -> 1.89 us  [body(): lax.ppermute(tokens[rows - 16:], 'sp', [(i, i + 1) for i in range(spans -...]
  transfers between devices with their start and end apart: 17 -> 31, of which waited for: 7 -> 8; matrix products, arithmetic and copies ran while one was open for 1% -> 1% of each run, Pallas kernels for 28% -> 22%
where the time goes in v2:
time: 122 us; the launch traced here: 120 us
  starting transfers between devices  72.3 us (59%)
  Pallas kernels  28.9 us (24%)
  waiting for transfers between devices  15.5 us (13%)
  local copies, waits for them, and re-layouts  3.24 us (3%)
    ppermute x12, starting transfers between devices, onward(): moved.append([lax.ppermute(part, ('sp', 'tp'), around) for part in parts])  44.7 us
    ppermute x7, starting transfers between devices, body(): moves.append(lax.ppermute(part, 'tp', [(t, to(t)) for t in range(heads)]))  11.8 us
    ppermute x10, starting transfers between devices, across(): swapped.append([lax.ppermute(part, ('sp', 'tp'), swap) for part in parts])  10.2 us
    pallas_call x2, Pallas kernels, recur(): pl.pallas_call(functools.partial(recur_kernel, first=first), in_specs=[fi...  9.57 us
    ppermute x7, waiting for transfers between devices, body(): moves.append(lax.ppermute(part, 'tp', [(t, to(t)) for t in range(heads)]))  6.49 us
    ppermute x12, waiting for transfers between devices, onward(): moved.append([lax.ppermute(part, ('sp', 'tp'), around) for part in parts])  6.15 us
    pallas_call x1, Pallas kernels, body(): pl.pallas_call(gate_kernel, in_specs=[hbm, fixed, fixed], out_specs=hbm,...  6.07 us
    pallas_call x1, Pallas kernels, body(): pl.pallas_call(input_kernel, in_specs=[hbm, fixed, fixed], out_specs=[fix...  4.87 us
  transfers between devices with their start and end apart: 31, of which 8 were waited for; matrix products, arithmetic and copies ran while one was open for 1% of the time, Pallas kernels for 22%

profile of v2, /device:TPU:33, one launch (start us, length us, event | category | flops | bytes accessed | tf_op | source)
XLA Modules:
  0.0 120.3 jit_solution(12845996124731205290)
XLA Ops:
  0.0 22.9 %collective-permute-start = (bf16[128,2048]{1,0:T(8,128)(2,1)}, bf16[128,2048]{1,0:T(8,128)(2,1)S(1)}, u32[]{:S(2)}, u32[]{:S(2)}) collective-permute-start(bf16[128,2048]{1,0:T(8,128)(2,1)} %refs_0_.1), channel_id=1, source_target_pairs={{0,8},{1,121},{2,10},{3,123},{4,12},{5,125},{6,14},{7,127},{8,16},... | collective-permute-start | bytes 1572872 | tf_op jit(solution)/shard_map/ppermute | solution.py:329
  24.9 4.9 %input.1 = (bf16[2048,256]{1,0:T(8,128)(2,1)S(1)}, bf16[2048,256]{1,0:T(8,128)(2,1)S(1)}) custom-call(bf16[2048,2048]{1,0:T(8,128)(2,1)} %tokens.2, f32[1,2048]{1,0:T(1,128)S(1)} %bitcast.6, bf16[2048,256]{1,0:T(8,128)(2,1)S(1)} %copy-done.1), custom_call_target="tpu_custom_call" | custom-call | tf_op jit(solution)/shard_map/input/pallas_call | solution.py:356
  31.2 1.7 %collective-permute-start.3 = (bf16[128,2048]{1,0:T(8,128)(2,1)S(1)}, bf16[128,2048]{1,0:T(8,128)(2,1)S(1)}, u32[]{:S(2)}, u32[]{:S(2)}) collective-permute-start(bf16[128,2048]{1,0:T(8,128)(2,1)S(1)} %collective-permute-done.refs_1_), channel_id=1, source_target_pairs={{0,8},{1,121},{2,10},{3,123},{4,12},{5,125},{6,14},{7,127},{8,16},... | collective-permute-start | bytes 1572872 | tf_op jit(solution)/shard_map/ppermute | solution.py:329
  35.4 1.9 %collective-permute-done.1.refs_0_ = bf16[16,2048]{1,0:T(8,128)(2,1)S(1)} collective-permute-done((bf16[16,2048]{1,0:T(8,128)(2,1)S(1)}, bf16[16,2048]{1,0:T(8,128)(2,1)S(1)}, u32[]{:S(2)}, u32[]{:S(2)}) %collective-permute-start.1) | collective-permute-done | bytes 65568 | tf_op jit(solution)/shard_map/ppermute | solution.py:352
  37.3 4.6 %recur.2 = (f32[2,1024,128]{2,1,0:T(8,128)}, f32[2,1024,128]{2,1,0:T(8,128)}, f32[1,8,256]{2,1,0:T(8,128)S(1)}) custom-call(bf16[2048,256]{1,0:T(8,128)(2,1)S(1)} %get-tuple-element.35.projected, f32[4,256]{1,0:T(4,128)S(1)} %copy-done.8, bf16[1,256,256]{2,1,0:T(8,128)(2,1)S(1)} %copy-done.3, bf16[1,256,256]{2,1,0:T(8,128)(2,1)S(1)} %copy-done.4, ...), custom_call_target="tpu_custom_call" | custom-call | tf_op jit(solution)/shard_map/recur/pallas_call | solution.py:371
  41.9 5.0 %recur.3 = (f32[2,1024,128]{2,1,0:T(8,128)}, f32[2,1024,128]{2,1,0:T(8,128)}, f32[16,8,256]{2,1,0:T(8,128)}) custom-call(bf16[2048,256]{1,0:T(8,128)(2,1)S(1)} %get-tuple-element.35.projected, f32[4,256]{1,0:T(4,128)S(1)} %copy-done.8, bf16[1,256,256]{2,1,0:T(8,128)(2,1)S(1)} %copy-done.3, bf16[1,256,256]{2,1,0:T(8,128)(2,1)S(1)} %copy-done.4, ...), custom_call_target="tpu_custom_call" | custom-call | tf_op jit(solution)/shard_map/recur/pallas_call | solution.py:371
  47.0 2.1 %collective-permute-start.4 = (bf16[128,2048]{1,0:T(8,128)(2,1)S(1)}, bf16[128,2048]{1,0:T(8,128)(2,1)S(1)}, u32[]{:S(2)}, u32[]{:S(2)}) collective-permute-start(bf16[128,2048]{1,0:T(8,128)(2,1)S(1)} %collective-permute-done.3.refs_2_), channel_id=1, source_target_pairs={{0,1},{1,0},{2,3},{3,2},{4,5},{5,4},{6,7},{7,6},{8,9},{9,8},{10,11... | collective-permute-start | bytes 1572872 | tf_op jit(solution)/shard_map/ppermute | solution.py:332
  49.1 4.2 %collective-permute-start.5 = (bf16[128,2048]{1,0:T(8,128)(2,1)S(1)}, bf16[128,2048]{1,0:T(8,128)(2,1)}, u32[]{:S(2)}, u32[]{:S(2)}) collective-permute-start(bf16[128,2048]{1,0:T(8,128)(2,1)S(1)} %collective-permute-done.3.refs_2_), channel_id=1, source_target_pairs={{0,8},{1,121},{2,10},{3,123},{4,12},{5,125},{6,14},{7,127},{8,16},... | collective-permute-start | bytes 1572872 | tf_op jit(solution)/shard_map/ppermute | solution.py:329
  53.3 4.0 %all-to-all-start = ((f32[16,8,256]{2,1,0:T(8,128)}), f32[16,8,256]{2,1,0:T(8,128)S(1)}, u32[]{:S(2)}, u32[]{:S(2)}) async-start(f32[16,8,256]{2,1,0:T(8,128)} %get-tuple-element.44), calls=%async_computation | async-start | bytes 262144 | tf_op jit(solution)/shard_map/all_to_all | solution.py:393
  57.3 6.1 %gate.1 = f32[2048,256]{1,0:T(8,128)} custom-call(bf16[2048,2048]{1,0:T(8,128)(2,1)} %tokens.2, f32[1,2048]{1,0:T(1,128)S(1)} %bitcast.7, bf16[2048,256]{1,0:T(8,128)(2,1)S(1)} %copy-done), custom_call_target="tpu_custom_call" | custom-call | tf_op jit(solution)/shard_map/gate/pallas_call | solution.py:395
  63.4 2.0 %collective-permute-start.13 = (bf16[128,2048]{1,0:T(8,128)(2,1)}, bf16[128,2048]{1,0:T(8,128)(2,1)S(1)}, u32[]{:S(2)}, u32[]{:S(2)}) collective-permute-start(bf16[128,2048]{1,0:T(8,128)(2,1)} %collective-permute-done.5.refs_3_), channel_id=1, source_target_pairs={{0,1},{1,0},{2,3},{3,2},{4,5},{5,4},{6,7},{7,6},{8,9},{9,8},{10,11... | collective-permute-start | bytes 1572872 | tf_op jit(solution)/shard_map/ppermute | solution.py:332
  65.4 2.7 %collective-permute-start.14 = (bf16[128,2048]{1,0:T(8,128)(2,1)}, bf16[128,2048]{1,0:T(8,128)(2,1)S(1)}, u32[]{:S(2)}, u32[]{:S(2)}) collective-permute-start(bf16[128,2048]{1,0:T(8,128)(2,1)} %collective-permute-done.5.refs_3_), channel_id=1, source_target_pairs={{0,8},{1,121},{2,10},{3,123},{4,12},{5,125},{6,14},{7,127},{8,16},... | collective-permute-start | bytes 1572872 | tf_op jit(solution)/shard_map/ppermute | solution.py:329
  69.0 3.5 %gated.1 = bf16[8,2,272,128]{3,2,1,0:T(8,128)(2,1)S(1)} custom-call(f32[2,1024,128]{2,1,0:T(8,128)} %get-tuple-element.37.state_1, f32[2,1024,128]{2,1,0:T(8,128)} %get-tuple-element.39.state_2, f32[2,1024,128]{2,1,0:T(8,128)} %get-tuple-element.40.prod_1, f32[2,1024,128]{2,1,0:T(8,128)} %get-tuple-element.41.prod_2, f32[2048,256]{1,0:T(8,128)} %gate.1, ...), custom_call_target="tpu_custom_call" | custom-call | tf_op jit(solution)/shard_map/gated/pallas_call | solution.py:409
  72.8 3.3 %collective-permute-start.6 = (bf16[1,2,272,128]{3,2,1,0:T(8,128)(2,1)S(1)}, bf16[1,2,272,128]{3,2,1,0:T(8,128)(2,1)S(1)}, u32[]{:S(2)}, u32[]{:S(2)}) collective-permute-start(bf16[1,2,272,128]{3,2,1,0:T(8,128)(2,1)S(1)} %get-tuple-element.69), channel_id=1, source_target_pairs={{0,4},{1,5},{2,6},{3,7},{4,0},{5,1},{6,2},{7,3},{8,12},{9,13},{10,... | collective-permute-start | bytes 417800 | tf_op jit(solution)/shard_map/ppermute | solution.py:431
  76.1 4.3 %collective-permute-start.7 = (bf16[1,2,272,128]{3,2,1,0:T(8,128)(2,1)S(1)}, bf16[1,2,272,128]{3,2,1,0:T(8,128)(2,1)S(1)}, u32[]{:S(2)}, u32[]{:S(2)}) collective-permute-start(bf16[1,2,272,128]{3,2,1,0:T(8,128)(2,1)S(1)} %get-tuple-element.68), channel_id=1, source_target_pairs={{0,5},{1,4},{2,7},{3,6},{4,1},{5,0},{6,3},{7,2},{8,13},{9,12},{10,... | collective-permute-start | bytes 417800 | tf_op jit(solution)/shard_map/ppermute | solution.py:431
  86.7 2.6 %collective-permute-done.8 = bf16[1,2,272,128]{3,2,1,0:T(8,128)(2,1)S(1)} collective-permute-done((bf16[1,2,272,128]{3,2,1,0:T(8,128)(2,1)S(1)}, bf16[1,2,272,128]{3,2,1,0:T(8,128)(2,1)S(1)}, u32[]{:S(2)}, u32[]{:S(2)}) %collective-permute-start.8) | collective-permute-done | bytes 139296 | tf_op jit(solution)/shard_map/ppermute | solution.py:431
  96.1 2.3 %collective-permute-done.11 = bf16[1,2,272,128]{3,2,1,0:T(8,128)(2,1)S(1)} collective-permute-done((bf16[1,2,272,128]{3,2,1,0:T(8,128)(2,1)S(1)}, bf16[1,2,272,128]{3,2,1,0:T(8,128)(2,1)S(1)}, u32[]{:S(2)}, u32[]{:S(2)}) %collective-permute-start.11) | collective-permute-done | bytes 139296 | tf_op jit(solution)/shard_map/ppermute | solution.py:431
  101.3 2.6 %collective-permute-done.20.refs_0_ = bf16[64,2048]{1,0:T(8,128)(2,1)S(1)} collective-permute-done((bf16[64,2048]{1,0:T(8,128)(2,1)S(1)}, bf16[64,2048]{1,0:T(8,128)(2,1)S(1)}, u32[]{:S(2)}, u32[]{:S(2)}) %collective-permute-start.20) | collective-permute-done | bytes 262176 | tf_op jit(solution)/shard_map/ppermute | solution.py:329
  103.9 2.3 %collective-permute-start.21 = (bf16[64,2048]{1,0:T(8,128)(2,1)S(1)}, bf16[64,2048]{1,0:T(8,128)(2,1)S(1)}, u32[]{:S(2)}, u32[]{:S(2)}) collective-permute-start(bf16[64,2048]{1,0:T(8,128)(2,1)S(1)} %collective-permute-done.20.refs_0_), channel_id=1, source_target_pairs={{0,1},{1,0},{2,3},{3,2},{4,5},{5,4},{6,7},{7,6},{8,9},{9,8},{10,11... | collective-permute-start | bytes 786440 | tf_op jit(solution)/shard_map/ppermute | solution.py:332
  106.7 2.5 %collective-permute-start.27 = (bf16[64,2048]{1,0:T(8,128)(2,1)S(1)}, bf16[64,2048]{1,0:T(8,128)(2,1)S(1)}, u32[]{:S(2)}, u32[]{:S(2)}) collective-permute-start(bf16[64,2048]{1,0:T(8,128)(2,1)S(1)} %collective-permute-done.25.refs_3_), channel_id=1, source_target_pairs={{0,8},{1,121},{2,10},{3,123},{4,12},{5,125},{6,14},{7,127},{8,16},... | collective-permute-start | bytes 786440 | tf_op jit(solution)/shard_map/ppermute | solution.py:329
  109.2 2.9 %early.1.sums = f32[256,2048]{1,0:T(8,128)S(1)} custom-call(bf16[16,272,128]{2,1,0:T(8,128)(2,1)S(1)} %bitcast.4, bf16[128,2048]{1,0:T(8,128)(2,1)S(1)} %copy-done.2, bf16[128,2048]{1,0:T(8,128)(2,1)S(1)} %collective-permute-done.refs_1_, bf16[128,2048]{1,0:T(8,128)(2,1)S(1)} %collective-permute-done.3.refs_2_, ...), custom_call_target="tpu_custom_call" | custom-call | tf_op jit(solution)/shard_map/early/pallas_call | solution.py:444
  112.1 2.8 %collective-permute-start.26 = (bf16[64,2048]{1,0:T(8,128)(2,1)S(1)}, bf16[64,2048]{1,0:T(8,128)(2,1)S(1)}, u32[]{:S(2)}, u32[]{:S(2)}) collective-permute-start(bf16[64,2048]{1,0:T(8,128)(2,1)S(1)} %collective-permute-done.24.refs_2_), channel_id=1, source_target_pairs={{0,8},{1,121},{2,10},{3,123},{4,12},{5,125},{6,14},{7,127},{8,16},... | collective-permute-start | bytes 786440 | tf_op jit(solution)/shard_map/ppermute | solution.py:329
  114.9 3.3 %collective-permute-done.26.refs_4_ = bf16[64,2048]{1,0:T(8,128)(2,1)S(1)} collective-permute-done((bf16[64,2048]{1,0:T(8,128)(2,1)S(1)}, bf16[64,2048]{1,0:T(8,128)(2,1)S(1)}, u32[]{:S(2)}, u32[]{:S(2)}) %collective-permute-start.26) | collective-permute-done | bytes 262176 | tf_op jit(solution)/shard_map/ppermute | solution.py:329
  118.2 2.0 %late.1 = bf16[256,2048]{1,0:T(8,128)(2,1)} custom-call(bf16[16,272,128]{2,1,0:T(8,128)(2,1)S(1)} %bitcast.5, f32[256,2048]{1,0:T(8,128)S(1)} %early.1.sums, bf16[64,2048]{1,0:T(8,128)(2,1)S(1)} %collective-permute-done.20.refs_0_, bf16[64,2048]{1,0:T(8,128)(2,1)S(1)} %collective-permute-done.22.refs_1_, ...), custom_call_target="tpu_custom_call" | custom-call | tf_op jit(solution)/shard_map/late/pallas_call | solution.py:456
  (78 shorter events, 23.6 us)
Async XLA Ops:
  0.0 29.7 %collective-permute-start = (bf16[128,2048]{1,0:T(8,128)(2,1)}, bf16[128,2048]{1,0:T(8,128)(2,1)S(1)}, u32[]{:S(2)}, u32[]{:S(2)}) collective-permute-start(bf16[128,2048]{1,0:T(8,128)(2,1)} %refs_0_.1), channel_id=1, source_target_pairs={{0,8},{1,121},{2,10},{3,123},{4,12},{5,125},{6,14},{7,127},{8,16},... | collective-permute-start | bytes 1572872 | tf_op jit(solution)/shard_map/ppermute | solution.py:329
  29.7 17.2 %collective-permute-start.2 = (bf16[128,2048]{1,0:T(8,128)(2,1)S(1)}, bf16[128,2048]{1,0:T(8,128)(2,1)S(1)}, u32[]{:S(2)}, u32[]{:S(2)}) collective-permute-start(bf16[128,2048]{1,0:T(8,128)(2,1)S(1)} %collective-permute-done.refs_1_), channel_id=1, source_target_pairs={{0,1},{1,0},{2,3},{3,2},{4,5},{5,4},{6,7},{7,6},{8,9},{9,8},{10,11... | collective-permute-start | bytes 1572872 | tf_op jit(solution)/shard_map/ppermute | solution.py:332
  31.2 15.8 %collective-permute-start.3 = (bf16[128,2048]{1,0:T(8,128)(2,1)S(1)}, bf16[128,2048]{1,0:T(8,128)(2,1)S(1)}, u32[]{:S(2)}, u32[]{:S(2)}) collective-permute-start(bf16[128,2048]{1,0:T(8,128)(2,1)S(1)} %collective-permute-done.refs_1_), channel_id=1, source_target_pairs={{0,8},{1,121},{2,10},{3,123},{4,12},{5,125},{6,14},{7,127},{8,16},... | collective-permute-start | bytes 1572872 | tf_op jit(solution)/shard_map/ppermute | solution.py:329
  47.0 16.4 %collective-permute-start.4 = (bf16[128,2048]{1,0:T(8,128)(2,1)S(1)}, bf16[128,2048]{1,0:T(8,128)(2,1)S(1)}, u32[]{:S(2)}, u32[]{:S(2)}) collective-permute-start(bf16[128,2048]{1,0:T(8,128)(2,1)S(1)} %collective-permute-done.3.refs_2_), channel_id=1, source_target_pairs={{0,1},{1,0},{2,3},{3,2},{4,5},{5,4},{6,7},{7,6},{8,9},{9,8},{10,11... | collective-permute-start | bytes 1572872 | tf_op jit(solution)/shard_map/ppermute | solution.py:332
  49.1 14.3 %collective-permute-start.5 = (bf16[128,2048]{1,0:T(8,128)(2,1)S(1)}, bf16[128,2048]{1,0:T(8,128)(2,1)}, u32[]{:S(2)}, u32[]{:S(2)}) collective-permute-start(bf16[128,2048]{1,0:T(8,128)(2,1)S(1)} %collective-permute-done.3.refs_2_), channel_id=1, source_target_pairs={{0,8},{1,121},{2,10},{3,123},{4,12},{5,125},{6,14},{7,127},{8,16},... | collective-permute-start | bytes 1572872 | tf_op jit(solution)/shard_map/ppermute | solution.py:329
  53.3 15.7 %all-to-all-start = ((f32[16,8,256]{2,1,0:T(8,128)}), f32[16,8,256]{2,1,0:T(8,128)S(1)}, u32[]{:S(2)}, u32[]{:S(2)}) async-start(f32[16,8,256]{2,1,0:T(8,128)} %get-tuple-element.44), calls=%async_computation | async-start | bytes 262144 | tf_op jit(solution)/shard_map/all_to_all | solution.py:393
  63.4 18.3 %collective-permute-start.13 = (bf16[128,2048]{1,0:T(8,128)(2,1)}, bf16[128,2048]{1,0:T(8,128)(2,1)S(1)}, u32[]{:S(2)}, u32[]{:S(2)}) collective-permute-start(bf16[128,2048]{1,0:T(8,128)(2,1)} %collective-permute-done.5.refs_3_), channel_id=1, source_target_pairs={{0,1},{1,0},{2,3},{3,2},{4,5},{5,4},{6,7},{7,6},{8,9},{9,8},{10,11... | collective-permute-start | bytes 1572872 | tf_op jit(solution)/shard_map/ppermute | solution.py:332
  65.4 16.3 %collective-permute-start.14 = (bf16[128,2048]{1,0:T(8,128)(2,1)}, bf16[128,2048]{1,0:T(8,128)(2,1)S(1)}, u32[]{:S(2)}, u32[]{:S(2)}) collective-permute-start(bf16[128,2048]{1,0:T(8,128)(2,1)} %collective-permute-done.5.refs_3_), channel_id=1, source_target_pairs={{0,8},{1,121},{2,10},{3,123},{4,12},{5,125},{6,14},{7,127},{8,16},... | collective-permute-start | bytes 1572872 | tf_op jit(solution)/shard_map/ppermute | solution.py:329
  72.8 10.8 %collective-permute-start.6 = (bf16[1,2,272,128]{3,2,1,0:T(8,128)(2,1)S(1)}, bf16[1,2,272,128]{3,2,1,0:T(8,128)(2,1)S(1)}, u32[]{:S(2)}, u32[]{:S(2)}) collective-permute-start(bf16[1,2,272,128]{3,2,1,0:T(8,128)(2,1)S(1)} %get-tuple-element.69), channel_id=1, source_target_pairs={{0,4},{1,5},{2,6},{3,7},{4,0},{5,1},{6,2},{7,3},{8,12},{9,13},{10,... | collective-permute-start | bytes 417800 | tf_op jit(solution)/shard_map/ppermute | solution.py:431
  76.1 9.2 %collective-permute-start.7 = (bf16[1,2,272,128]{3,2,1,0:T(8,128)(2,1)S(1)}, bf16[1,2,272,128]{3,2,1,0:T(8,128)(2,1)S(1)}, u32[]{:S(2)}, u32[]{:S(2)}) collective-permute-start(bf16[1,2,272,128]{3,2,1,0:T(8,128)(2,1)S(1)} %get-tuple-element.68), channel_id=1, source_target_pairs={{0,5},{1,4},{2,7},{3,6},{4,1},{5,0},{6,3},{7,2},{8,13},{9,12},{10,... | collective-permute-start | bytes 417800 | tf_op jit(solution)/shard_map/ppermute | solution.py:431
  80.4 9.0 %collective-permute-start.8 = (bf16[1,2,272,128]{3,2,1,0:T(8,128)(2,1)S(1)}, bf16[1,2,272,128]{3,2,1,0:T(8,128)(2,1)S(1)}, u32[]{:S(2)}, u32[]{:S(2)}) collective-permute-start(bf16[1,2,272,128]{3,2,1,0:T(8,128)(2,1)S(1)} %get-tuple-element.67), channel_id=1, source_target_pairs={{0,2},{1,3},{2,4},{3,5},{4,6},{5,7},{6,0},{7,1},{8,10},{9,11},{10,... | collective-permute-start | bytes 417800 | tf_op jit(solution)/shard_map/ppermute | solution.py:431
  81.7 10.6 %collective-permute-start.9 = (bf16[1,2,272,128]{3,2,1,0:T(8,128)(2,1)S(1)}, bf16[1,2,272,128]{3,2,1,0:T(8,128)(2,1)S(1)}, u32[]{:S(2)}, u32[]{:S(2)}) collective-permute-start(bf16[1,2,272,128]{3,2,1,0:T(8,128)(2,1)S(1)} %get-tuple-element.66), channel_id=1, source_target_pairs={{0,3},{1,2},{2,5},{3,4},{4,7},{5,6},{6,1},{7,0},{8,11},{9,10},{10,... | collective-permute-start | bytes 417800 | tf_op jit(solution)/shard_map/ppermute | solution.py:431
  81.7 13.9 %collective-permute-start.15 = (bf16[128,2048]{1,0:T(8,128)(2,1)S(1)}, bf16[128,2048]{1,0:T(8,128)(2,1)S(1)}, u32[]{:S(2)}, u32[]{:S(2)}) collective-permute-start(bf16[128,2048]{1,0:T(8,128)(2,1)S(1)} %collective-permute-done.14.refs_4_), channel_id=1, source_target_pairs={{0,1},{1,0},{2,3},{3,2},{4,5},{5,4},{6,7},{7,6},{8,9},{9,8},{10,11... | collective-permute-start | bytes 1572872 | tf_op jit(solution)/shard_map/ppermute | solution.py:332
  83.5 9.4 %collective-permute-start.18 = (bf16[64,2048]{1,0:T(8,128)(2,1)S(1)}, bf16[64,2048]{1,0:T(8,128)(2,1)S(1)}, u32[]{:S(2)}, u32[]{:S(2)}) collective-permute-start(bf16[64,2048]{1,0:T(8,128)(2,1)S(1)} %get-tuple-element.71), channel_id=1, source_target_pairs={{0,8},{1,121},{2,10},{3,123},{4,12},{5,125},{6,14},{7,127},{8,16},... | collective-permute-start | bytes 786440 | tf_op jit(solution)/shard_map/ppermute | solution.py:329
  85.2 9.4 %collective-permute-start.16 = (bf16[64,2048]{1,0:T(8,128)(2,1)S(1)}, bf16[64,2048]{1,0:T(8,128)(2,1)S(1)}, u32[]{:S(2)}, u32[]{:S(2)}) collective-permute-start(bf16[64,2048]{1,0:T(8,128)(2,1)S(1)} %get-tuple-element.72), channel_id=1, source_target_pairs={{0,8},{1,121},{2,10},{3,123},{4,12},{5,125},{6,14},{7,127},{8,16},... | collective-permute-start | bytes 786440 | tf_op jit(solution)/shard_map/ppermute | solution.py:329
  89.3 6.3 %collective-permute-start.10 = (bf16[1,2,272,128]{3,2,1,0:T(8,128)(2,1)S(1)}, bf16[1,2,272,128]{3,2,1,0:T(8,128)(2,1)S(1)}, u32[]{:S(2)}, u32[]{:S(2)}) collective-permute-start(bf16[1,2,272,128]{3,2,1,0:T(8,128)(2,1)S(1)} %get-tuple-element.65), channel_id=1, source_target_pairs={{0,6},{1,7},{2,0},{3,1},{4,2},{5,3},{6,4},{7,5},{8,14},{9,15},{10,... | collective-permute-start | bytes 417800 | tf_op jit(solution)/shard_map/ppermute | solution.py:431
  92.3 6.1 %collective-permute-start.11 = (bf16[1,2,272,128]{3,2,1,0:T(8,128)(2,1)S(1)}, bf16[1,2,272,128]{3,2,1,0:T(8,128)(2,1)S(1)}, u32[]{:S(2)}, u32[]{:S(2)}) collective-permute-start(bf16[1,2,272,128]{3,2,1,0:T(8,128)(2,1)S(1)} %get-tuple-element.64), channel_id=1, source_target_pairs={{0,7},{1,6},{2,1},{3,0},{4,3},{5,2},{6,5},{7,4},{8,15},{9,14},{10,... | collective-permute-start | bytes 417800 | tf_op jit(solution)/shard_map/ppermute | solution.py:431
  92.9 7.1 %collective-permute-start.22 = (bf16[64,2048]{1,0:T(8,128)(2,1)S(1)}, bf16[64,2048]{1,0:T(8,128)(2,1)S(1)}, u32[]{:S(2)}, u32[]{:S(2)}) collective-permute-start(bf16[64,2048]{1,0:T(8,128)(2,1)S(1)} %collective-permute-done.18.refs_6_), channel_id=1, source_target_pairs={{0,8},{1,121},{2,10},{3,123},{4,12},{5,125},{6,14},{7,127},{8,16},... | collective-permute-start | bytes 786440 | tf_op jit(solution)/shard_map/ppermute | solution.py:329
  94.7 6.4 %collective-permute-start.12 = (bf16[1,2,272,128]{3,2,1,0:T(8,128)(2,1)S(1)}, bf16[1,2,272,128]{3,2,1,0:T(8,128)(2,1)S(1)}, u32[]{:S(2)}, u32[]{:S(2)}) collective-permute-start(bf16[1,2,272,128]{3,2,1,0:T(8,128)(2,1)S(1)} %get-tuple-element.63), channel_id=1, source_target_pairs={{0,1},{1,0},{2,3},{3,2},{4,5},{5,4},{6,7},{7,6},{8,9},{9,8},{10,11... | collective-permute-start | bytes 417800 | tf_op jit(solution)/shard_map/ppermute | solution.py:431
  100.0 6.7 %collective-permute-start.25 = (bf16[64,2048]{1,0:T(8,128)(2,1)S(1)}, bf16[64,2048]{1,0:T(8,128)(2,1)S(1)}, u32[]{:S(2)}, u32[]{:S(2)}) collective-permute-start(bf16[64,2048]{1,0:T(8,128)(2,1)S(1)} %collective-permute-done.22.refs_1_), channel_id=1, source_target_pairs={{0,8},{1,121},{2,10},{3,123},{4,12},{5,125},{6,14},{7,127},{8,16},... | collective-permute-start | bytes 786440 | tf_op jit(solution)/shard_map/ppermute | solution.py:329
  101.1 11.0 %collective-permute-start.23 = (bf16[64,2048]{1,0:T(8,128)(2,1)S(1)}, bf16[64,2048]{1,0:T(8,128)(2,1)S(1)}, u32[]{:S(2)}, u32[]{:S(2)}) collective-permute-start(bf16[64,2048]{1,0:T(8,128)(2,1)S(1)} %collective-permute-done.22.refs_1_), channel_id=1, source_target_pairs={{0,1},{1,0},{2,3},{3,2},{4,5},{5,4},{6,7},{7,6},{8,9},{9,8},{10,11... | collective-permute-start | bytes 786440 | tf_op jit(solution)/shard_map/ppermute | solution.py:332
  103.9 8.2 %collective-permute-start.21 = (bf16[64,2048]{1,0:T(8,128)(2,1)S(1)}, bf16[64,2048]{1,0:T(8,128)(2,1)S(1)}, u32[]{:S(2)}, u32[]{:S(2)}) collective-permute-start(bf16[64,2048]{1,0:T(8,128)(2,1)S(1)} %collective-permute-done.20.refs_0_), channel_id=1, source_target_pairs={{0,1},{1,0},{2,3},{3,2},{4,5},{5,4},{6,7},{7,6},{8,9},{9,8},{10,11... | collective-permute-start | bytes 786440 | tf_op jit(solution)/shard_map/ppermute | solution.py:332
  106.7 8.2 %collective-permute-start.27 = (bf16[64,2048]{1,0:T(8,128)(2,1)S(1)}, bf16[64,2048]{1,0:T(8,128)(2,1)S(1)}, u32[]{:S(2)}, u32[]{:S(2)}) collective-permute-start(bf16[64,2048]{1,0:T(8,128)(2,1)S(1)} %collective-permute-done.25.refs_3_), channel_id=1, source_target_pairs={{0,8},{1,121},{2,10},{3,123},{4,12},{5,125},{6,14},{7,127},{8,16},... | collective-permute-start | bytes 786440 | tf_op jit(solution)/shard_map/ppermute | solution.py:329
  112.1 6.1 %collective-permute-start.26 = (bf16[64,2048]{1,0:T(8,128)(2,1)S(1)}, bf16[64,2048]{1,0:T(8,128)(2,1)S(1)}, u32[]{:S(2)}, u32[]{:S(2)}) collective-permute-start(bf16[64,2048]{1,0:T(8,128)(2,1)S(1)} %collective-permute-done.24.refs_2_), channel_id=1, source_target_pairs={{0,8},{1,121},{2,10},{3,123},{4,12},{5,125},{6,14},{7,127},{8,16},... | collective-permute-start | bytes 786440 | tf_op jit(solution)/shard_map/ppermute | solution.py:329
  (18 other events, 167.8 us)

commit v3 on v2

--- a/solution.py
+++ b/solution.py
@@ -92,11 +92,19 @@
     return at, pltpu.make_async_copy(source.at[at, :], target.at[at, :], sems.at[k])
 
 
-def input_kernel(tokens, gain, w_input, projected, scaled, kept, sems):
+def input_kernel(tokens, gain, w_input, projected, scaled, kept, gain_here, w_here, sems, small_sems):
     count = sems.shape[0]
+    small = [
+        pltpu.make_async_copy(gain, gain_here, small_sems.at[0]),
+        pltpu.make_async_copy(w_input, w_here, small_sems.at[1]),
+    ]
+    for copy in small:
+        copy.start()
     for k in range(count):
         chunk_copy(tokens, kept, sems, k)[1].start()
-    scaled[...] = scaled_weights(w_input, gain)
+    for copy in small:
+        copy.wait()
+    scaled[...] = scaled_weights(w_here, gain_here)
 
     def part(k, _):
         at, copy = chunk_copy(tokens, kept, sems, k)
@@ -248,10 +256,12 @@
             sent[d, half, BLOCK : BLOCK + EXTRA, :] = lines[:, half * 128 : half * 128 + 128]
 
 
-def product(arrived, places, blocks, low, step):
-    mixed = jnp.concatenate([arrived[place, 0:BLOCK, :] for place in places], 1)
-    weights = jnp.concatenate([block[:, low : low + step] for block in blocks], 0)
-    return jnp.dot(mixed, weights, preferred_element_type=F32)
+def neighbour(seat, dx, dc, chips):
+    return lax_rem(seat // 2 + dx, chips) * 2 + lax_rem(seat % 2 + dc, 2)
+
+
+def lax_rem(a, b):
+    return a % b if isinstance(a, int) else lax.rem(a, b)
 
 
 def places_of(offsets, spans):
@@ -270,13 +280,18 @@
 
 
 def product(arrived, places, groups, low, step):
-    mixed = jnp.concatenate([arrived[place, 0:BLOCK, :] for place in places], 1)
+    mixed = jnp.concatenate([arrived[lax.div(place, 2), lax.rem(place, 2), 0:BLOCK, :] for place in places], 1)
     weights = jnp.concatenate([part[:, low : low + step] for parts in groups for part in parts], 0)
     return jnp.dot(mixed, weights, preferred_element_type=F32)
 
 
-def early_kernel(arrived, *refs, offsets, spans, depth):
-    groups, out = joined(refs[:-1], depth), refs[-1]
+def early_kernel(*refs, order, offsets, spans, depth):
+    count = len(order)
+    out, arrived = refs[-2:]
+    seat = lax.axis_index("tp")
+    for (dx, dc), part in zip(order, refs[:count]):
+        arrived[neighbour(seat, count // 2 - dx, dc, count // 2)] = part[0]
+    groups = joined(refs[count:-2], depth)
     places = places_of(offsets, spans)
     step = 512
     for low in range(0, out.shape[1], step):
@@ -286,10 +301,10 @@
 def late_kernel(arrived, sums, *refs, offsets, spans, depth, channels):
     groups, out = joined(refs[:-1], depth), refs[-1]
     places = places_of(offsets, spans)
-    ones = jnp.ones((arrived.shape[0] // 2 * EXTRA, 128), BF16)
+    ones = jnp.ones((arrived.shape[0] * EXTRA, 128), BF16)
     square = []
     for half in range(2):
-        lines = [arrived[k, BLOCK : BLOCK + EXTRA, :] for k in range(half, arrived.shape[0], 2)]
+        lines = [arrived[k, half, BLOCK : BLOCK + EXTRA, :] for k in range(arrived.shape[0])]
         square.append(
             lax.dot_general(
                 jnp.concatenate(lines, 0), ones, (((0,), (0,)), ((), ())), preferred_element_type=F32
@@ -326,16 +341,22 @@
     moved, swapped = [], []
 
     def onward(parts):
-        moved.append([lax.ppermute(part, ("sp", "tp"), around) for part in parts])
+        made = []
+        for part in parts:
+            made.append(lax.ppermute(part, ("sp", "tp"), around))
+        moved.append(made)
 
     def across(parts):
-        swapped.append([lax.ppermute(part, ("sp", "tp"), swap) for part in parts])
+        made = []
+        for part in parts:
+            made.append(lax.ppermute(part, ("sp", "tp"), swap))
+        swapped.append(made)
 
     def advance(value, pieces=1):
-        before = swapped[-1] if swapped else []
+        before = swapped[-2] if len(swapped) > 1 else []
         value, *rest = tie(value, *before, *moved[-1][:1])
-        if swapped:
-            swapped[-1] = rest[:-1]
+        if before:
+            swapped[-2] = rest[:-1]
         moved[-1] = rest[-1:] + moved[-1][1:]
         if len(moved) < reach:
             parts = moved[-1]
@@ -355,13 +376,16 @@
     in_hbm = lambda x: pltpu.with_memory_space_constraint(x, pltpu.HBM)
     projected, scaled = pl.pallas_call(
         input_kernel,
-        in_specs=[hbm, fixed, fixed],
+        in_specs=[hbm] * 3,
         out_specs=[fixed] * 2,
         out_shape=[pltpu.VMEM((rows, head), BF16), pltpu.VMEM((width, head), BF16)],
-        scratch_shapes=[pltpu.VMEM((rows, width), BF16), pltpu.SemaphoreType.DMA((4,))],
+        scratch_shapes=[
+            pltpu.VMEM((rows, width), BF16), pltpu.VMEM((1, width), F32), pltpu.VMEM((width, head), BF16),
+            pltpu.SemaphoreType.DMA((4,)), pltpu.SemaphoreType.DMA((2,)),
+        ],
         compiler_params=limit(16),
         name="input",
-    )(in_hbm(tokens), gain_row, w_input)
+    )(in_hbm(tokens), in_hbm(gain_row), in_hbm(w_input))
 
     half_rows = rows // 2
 
@@ -420,35 +444,30 @@
         name="gated",
     )(*map(in_hbm, (state_1, state_2, prod_1, prod_2, gate)), all_ends, out_gain.reshape(1, head))
     seat = lax.axis_index("tp")
-    chips = heads // 2
-    arrived = lax.dynamic_slice_in_dim(sent, seat, 1, 0)
-    arrived = lax.dynamic_update_slice_in_dim(jnp.zeros_like(sent), arrived, seat, 0)
     order = [(dx, dc) for dx in EXCHANGE for dc in range(2) if (dx, dc) != (0, 0)]
     moves = []
     for dx, dc in order:
-        to = lambda t: (t // 2 + dx) % chips * 2 + (t % 2 + dc) % 2
+        to = lambda t: neighbour(t, dx, dc, heads // 2)
+        if (dx, dc) == (1, 0):
+            sent = advance(sent, STREAMS)
         part = lax.dynamic_slice_in_dim(sent, to(seat), 1, 0)
         moves.append(lax.ppermute(part, "tp", [(t, to(t)) for t in range(heads)]))
-    for (dx, dc), part in zip(order, moves):
-        source = (seat // 2 - dx + chips) % chips * 2 + (seat % 2 + dc) % 2
-        arrived = lax.dynamic_update_slice_in_dim(arrived, part, source, 0)
     holding = sent
-    while len(moved) < reach - 2:
+    while len(moved) < reach - 1:
         holding = advance(holding, STREAMS)
-    arrived = arrived.reshape(2 * heads, BLOCK + EXTRA, head // 2)
-    arrived = advance(arrived, STREAMS)
+    own = lax.dynamic_slice_in_dim(holding, seat, 1, 0)
     flat = lambda groups: [on_chip(part) for parts in groups for part in parts]
     done = len(swapped) - 1
     offsets = [0] + [-k for k in range(1, done + 1)] + list(range(1, done + 1))
     blocks = [on_chip(w_out)] + flat(moved[:done]) + flat(swapped[:done])
-    sums = pl.pallas_call(
-        functools.partial(early_kernel, offsets=offsets, spans=spans, depth=depth),
-        in_specs=[fixed] * (1 + len(blocks)),
-        out_specs=fixed,
-        out_shape=pltpu.VMEM((BLOCK, out_width), F32),
-        compiler_params=limit(16),
+    sums, arrived = pl.pallas_call(
+        functools.partial(early_kernel, order=[(0, 0)] + order, offsets=offsets, spans=spans, depth=depth),
+        in_specs=[fixed] * (1 + len(moves) + len(blocks)),
+        out_specs=[fixed] * 2,
+        out_shape=[pltpu.VMEM((BLOCK, out_width), F32), pltpu.VMEM(sent.shape, BF16)],
+        compiler_params=limit(12),
         name="early",
-    )(arrived, *blocks)
+    )(on_chip(own), *map(on_chip, moves), *blocks)
     while len(moved) < reach:
         sums = advance(sums, STREAMS)
     offsets = [-k for k in range(done + 1, reach + 1)] + list(range(done + 1, reach))
@@ -458,9 +477,9 @@
         in_specs=[fixed] * (2 + len(blocks)),
         out_specs=fixed,
         out_shape=jax.ShapeDtypeStruct((BLOCK, out_width), BF16),
-        compiler_params=limit(16),
+        compiler_params=limit(12),
         name="late",
-    )(arrived, on_chip(sums), *blocks)
+    )(on_chip(arrived), on_chip(sums), *blocks)
 
 
 def solution(mesh):

time: 122 us -> 131 us (1.074)
  local copies, waits for them, and re-layouts: 3.24 us -> 14 us
  waiting for transfers between devices: 15.5 us -> 9.88 us
  Pallas kernels: 28.9 us -> 32.8 us
    unnamed x22 -> x46, local copies, waits for them, and re-layouts: 1.96 us -> 11.5 us
    ppermute x7, waiting for transfers between devices: 6.49 us -> 3.41 us  [body(): moves.append(lax.ppermute(part, 'tp', [(t, to(t)) for t in range(heads)]))]
    ppermute x7, starting transfers between devices: 11.8 us -> 14.5 us  [body(): moves.append(lax.ppermute(part, 'tp', [(t, to(t)) for t in range(heads)]))]
    pallas_call x2, Pallas kernels: 7.73 us -> 10.3 us  [the longest x1 6.78 us: body(): pl.pallas_call(input_kernel, in_specs=[hbm] * 3, out_specs=[fixed] * 2, o...]
    ppermute x22, starting transfers between devices: 54.9 us -> 53.2 us  [the longest x12 41 us: onward(): made.append(lax.ppermute(part, ('sp', 'tp'), around))]
    ppermute x22, waiting for transfers between devices: 6.18 us -> 4.72 us  [the longest x12 4.7 us: onward(): made.append(lax.ppermute(part, ('sp', 'tp'), around))]
  transfers between devices with their start and end apart: 31 -> 31, of which waited for: 8 -> 6; matrix products, arithmetic and copies ran while one was open for 1% -> 2% of each run, Pallas kernels for 22% -> 23%
where the time goes in v3:
time: 131 us; the launch traced here: 130 us
  starting transfers between devices  73 us (56%)
  Pallas kernels  32.8 us (25%)
  local copies, waits for them, and re-layouts  14 us (11%)
  waiting for transfers between devices  9.88 us (8%)
    ppermute x12, starting transfers between devices, onward(): made.append(lax.ppermute(part, ('sp', 'tp'), around))  41 us
    ppermute x7, starting transfers between devices, body(): moves.append(lax.ppermute(part, 'tp', [(t, to(t)) for t in range(heads)]))  14.5 us
    ppermute x10, starting transfers between devices, across(): made.append(lax.ppermute(part, ('sp', 'tp'), swap))  12.2 us
    unnamed x46, local copies, waits for them, and re-layouts  11.5 us
    pallas_call x2, Pallas kernels, recur(): pl.pallas_call(functools.partial(recur_kernel, first=first), in_specs=[fi...  9.61 us
    pallas_call x1, Pallas kernels, body(): pl.pallas_call(input_kernel, in_specs=[hbm] * 3, out_specs=[fixed] * 2, o...  6.78 us
    pallas_call x1, Pallas kernels, body(): pl.pallas_call(gate_kernel, in_specs=[hbm, fixed, fixed], out_specs=hbm,...  6.07 us
    ppermute x12, waiting for transfers between devices, onward(): made.append(lax.ppermute(part, ('sp', 'tp'), around))  4.7 us
  transfers between devices with their start and end apart: 31, of which 6 were waited for; matrix products, arithmetic and copies ran while one was open for 2% of the time, Pallas kernels for 23%

profile of v3, /device:TPU:33, one launch (start us, length us, event | category | flops | bytes accessed | tf_op | source)
XLA Modules:
  0.0 129.9 jit_solution(15582613270550078492)
XLA Ops:
  0.0 22.9 %collective-permute-start = (bf16[128,2048]{1,0:T(8,128)(2,1)}, bf16[128,2048]{1,0:T(8,128)(2,1)S(1)}, u32[]{:S(2)}, u32[]{:S(2)}) collective-permute-start(bf16[128,2048]{1,0:T(8,128)(2,1)} %refs_8_.1), channel_id=1, source_target_pairs={{0,8},{1,121},{2,10},{3,123},{4,12},{5,125},{6,14},{7,127},{8,16},... | collective-permute-start | bytes 1572872 | tf_op jit(solution)/shard_map/ppermute | solution.py:346
  22.9 6.8 %input.1 = (bf16[2048,256]{1,0:T(8,128)(2,1)S(1)}, bf16[2048,256]{1,0:T(8,128)(2,1)S(1)}) custom-call(bf16[2048,2048]{1,0:T(8,128)(2,1)} %tokens.2, f32[1,2048]{1,0:T(1,128)} %bitcast.3, bf16[2048,256]{1,0:T(8,128)(2,1)} %w_input.1), custom_call_target="tpu_custom_call" | custom-call | tf_op jit(solution)/shard_map/input/pallas_call | solution.py:377
  29.7 2.6 %collective-permute-start.2 = (bf16[128,2048]{1,0:T(8,128)(2,1)S(1)}, bf16[128,2048]{1,0:T(8,128)(2,1)S(1)}, u32[]{:S(2)}, u32[]{:S(2)}) collective-permute-start(bf16[128,2048]{1,0:T(8,128)(2,1)S(1)} %collective-permute-done.refs_9_), channel_id=1, source_target_pairs={{0,8},{1,121},{2,10},{3,123},{4,12},{5,125},{6,14},{7,127},{8,16},... | collective-permute-start | bytes 1572872 | tf_op jit(solution)/shard_map/ppermute | solution.py:346
  36.4 4.6 %recur.2 = (f32[2,1024,128]{2,1,0:T(8,128)}, f32[2,1024,128]{2,1,0:T(8,128)}, f32[1,8,256]{2,1,0:T(8,128)S(1)}) custom-call(bf16[2048,256]{1,0:T(8,128)(2,1)S(1)} %get-tuple-element.35.projected, f32[4,256]{1,0:T(4,128)S(1)} %copy-done.20, bf16[1,256,256]{2,1,0:T(8,128)(2,1)S(1)} %copy-done.1, bf16[1,256,256]{2,1,0:T(8,128)(2,1)S(1)} %copy-done.2, ...), custom_call_target="tpu_custom_call" | custom-call | tf_op jit(solution)/shard_map/recur/pallas_call | solution.py:395
  41.0 5.0 %recur.3 = (f32[2,1024,128]{2,1,0:T(8,128)}, f32[2,1024,128]{2,1,0:T(8,128)}, f32[16,8,256]{2,1,0:T(8,128)}) custom-call(bf16[2048,256]{1,0:T(8,128)(2,1)S(1)} %get-tuple-element.35.projected, f32[4,256]{1,0:T(4,128)S(1)} %copy-done.20, bf16[1,256,256]{2,1,0:T(8,128)(2,1)S(1)} %copy-done.1, bf16[1,256,256]{2,1,0:T(8,128)(2,1)S(1)} %copy-done.2, ...), custom_call_target="tpu_custom_call" | custom-call | tf_op jit(solution)/shard_map/recur/pallas_call | solution.py:395
  46.1 3.0 %collective-permute-start.4 = (bf16[128,2048]{1,0:T(8,128)(2,1)S(1)}, bf16[128,2048]{1,0:T(8,128)(2,1)}, u32[]{:S(2)}, u32[]{:S(2)}) collective-permute-start(bf16[128,2048]{1,0:T(8,128)(2,1)S(1)} %collective-permute-done.2.refs_10_), channel_id=1, source_target_pairs={{0,8},{1,121},{2,10},{3,123},{4,12},{5,125},{6,14},{7,127},{8,16},... | collective-permute-start | bytes 1572872 | tf_op jit(solution)/shard_map/ppermute | solution.py:346
  49.0 4.0 %all-to-all-start = ((f32[16,8,256]{2,1,0:T(8,128)}), f32[16,8,256]{2,1,0:T(8,128)S(1)}, u32[]{:S(2)}, u32[]{:S(2)}) async-start(f32[16,8,256]{2,1,0:T(8,128)} %get-tuple-element.44), calls=%async_computation | async-start | bytes 262144 | tf_op jit(solution)/shard_map/all_to_all | solution.py:417
  53.0 6.2 %collective-permute-start.5 = (bf16[128,2048]{1,0:T(8,128)(2,1)S(1)}, bf16[128,2048]{1,0:T(8,128)(2,1)}, u32[]{:S(2)}, u32[]{:S(2)}) collective-permute-start(bf16[128,2048]{1,0:T(8,128)(2,1)S(1)} %collective-permute-done.2.refs_10_), channel_id=1, source_target_pairs={{0,1},{1,0},{2,3},{3,2},{4,5},{5,4},{6,7},{7,6},{8,9},{9,8},{10,11... | collective-permute-start | bytes 1572872 | tf_op jit(solution)/shard_map/ppermute | solution.py:352
  59.2 6.1 %gate.1 = f32[2048,256]{1,0:T(8,128)} custom-call(bf16[2048,2048]{1,0:T(8,128)(2,1)} %tokens.2, f32[1,2048]{1,0:T(1,128)S(1)} %bitcast.4, bf16[2048,256]{1,0:T(8,128)(2,1)S(1)} %copy-done), custom_call_target="tpu_custom_call" | custom-call | tf_op jit(solution)/shard_map/gate/pallas_call | solution.py:419
  66.1 2.7 %collective-permute-start.6 = (bf16[128,2048]{1,0:T(8,128)(2,1)}, bf16[128,2048]{1,0:T(8,128)(2,1)S(1)}, u32[]{:S(2)}, u32[]{:S(2)}) collective-permute-start(bf16[128,2048]{1,0:T(8,128)(2,1)} %collective-permute-done.4.refs_11_), channel_id=1, source_target_pairs={{0,8},{1,121},{2,10},{3,123},{4,12},{5,125},{6,14},{7,127},{8,16},... | collective-permute-start | bytes 1572872 | tf_op jit(solution)/shard_map/ppermute | solution.py:346
  68.7 3.5 %gated.1 = bf16[8,2,272,128]{3,2,1,0:T(8,128)(2,1)S(1)} custom-call(f32[2,1024,128]{2,1,0:T(8,128)} %get-tuple-element.37.state_1, f32[2,1024,128]{2,1,0:T(8,128)} %get-tuple-element.39.state_2, f32[2,1024,128]{2,1,0:T(8,128)} %get-tuple-element.40.prod_1, f32[2,1024,128]{2,1,0:T(8,128)} %get-tuple-element.41.prod_2, f32[2048,256]{1,0:T(8,128)} %gate.1, ...), custom_call_target="tpu_custom_call" | custom-call | tf_op jit(solution)/shard_map/gated/pallas_call | solution.py:433
  73.0 3.0 %collective-permute-start.11 = (bf16[1,2,272,128]{3,2,1,0:T(8,128)(2,1)}, bf16[1,2,272,128]{3,2,1,0:T(8,128)(2,1)}, u32[]{:S(2)}, u32[]{:S(2)}) collective-permute-start(bf16[1,2,272,128]{3,2,1,0:T(8,128)(2,1)} %get-tuple-element.69), channel_id=1, source_target_pairs={{0,4},{1,5},{2,6},{3,7},{4,0},{5,1},{6,2},{7,3},{8,12},{9,13},{10,... | collective-permute-start | bytes 417800 | tf_op jit(solution)/shard_map/ppermute | solution.py:454
  76.0 3.5 %collective-permute-start.12 = (bf16[1,2,272,128]{3,2,1,0:T(8,128)(2,1)}, bf16[1,2,272,128]{3,2,1,0:T(8,128)(2,1)}, u32[]{:S(2)}, u32[]{:S(2)}) collective-permute-start(bf16[1,2,272,128]{3,2,1,0:T(8,128)(2,1)} %get-tuple-element.68), channel_id=1, source_target_pairs={{0,5},{1,4},{2,7},{3,6},{4,1},{5,0},{6,3},{7,2},{8,13},{9,12},{10,... | collective-permute-start | bytes 417800 | tf_op jit(solution)/shard_map/ppermute | solution.py:454
  81.8 1.8 %collective-permute-start.18 = (bf16[64,2048]{1,0:T(8,128)(2,1)}, bf16[64,2048]{1,0:T(8,128)(2,1)}, u32[]{:S(2)}, u32[]{:S(2)}) collective-permute-start(bf16[64,2048]{1,0:T(8,128)(2,1)} %get-tuple-element.70), channel_id=1, source_target_pairs={{0,8},{1,121},{2,10},{3,123},{4,12},{5,125},{6,14},{7,127},{8,16},... | collective-permute-start | bytes 786440 | tf_op jit(solution)/shard_map/ppermute | solution.py:346
  84.6 2.2 %collective-permute-start.13 = (bf16[1,2,272,128]{3,2,1,0:T(8,128)(2,1)S(1)}, bf16[1,2,272,128]{3,2,1,0:T(8,128)(2,1)S(1)}, u32[]{:S(2)}, u32[]{:S(2)}) collective-permute-start(bf16[1,2,272,128]{3,2,1,0:T(8,128)(2,1)S(1)} %get-tuple-element.67), channel_id=1, source_target_pairs={{0,2},{1,3},{2,4},{3,5},{4,6},{5,7},{6,0},{7,1},{8,10},{9,11},{10,... | collective-permute-start | bytes 417800 | tf_op jit(solution)/shard_map/ppermute | solution.py:454
  88.6 1.8 %collective-permute-start.15 = (bf16[1,2,272,128]{3,2,1,0:T(8,128)(2,1)S(1)}, bf16[1,2,272,128]{3,2,1,0:T(8,128)(2,1)S(1)}, u32[]{:S(2)}, u32[]{:S(2)}) collective-permute-start(bf16[1,2,272,128]{3,2,1,0:T(8,128)(2,1)S(1)} %get-tuple-element.65), channel_id=1, source_target_pairs={{0,6},{1,7},{2,0},{3,1},{4,2},{5,3},{6,4},{7,5},{8,14},{9,15},{10,... | collective-permute-start | bytes 417800 | tf_op jit(solution)/shard_map/ppermute | solution.py:454
  96.0 1.9 %collective-permute-start.16 = (bf16[1,2,272,128]{3,2,1,0:T(8,128)(2,1)S(1)}, bf16[1,2,272,128]{3,2,1,0:T(8,128)(2,1)S(1)}, u32[]{:S(2)}, u32[]{:S(2)}) collective-permute-start(bf16[1,2,272,128]{3,2,1,0:T(8,128)(2,1)S(1)} %get-tuple-element.64), channel_id=1, source_target_pairs={{0,7},{1,6},{2,1},{3,0},{4,3},{5,2},{6,5},{7,4},{8,15},{9,14},{10,... | collective-permute-start | bytes 417800 | tf_op jit(solution)/shard_map/ppermute | solution.py:454
  98.9 3.5 %collective-permute-start.19 = (bf16[64,2048]{1,0:T(8,128)(2,1)S(1)}, bf16[64,2048]{1,0:T(8,128)(2,1)}, u32[]{:S(2)}, u32[]{:S(2)}) collective-permute-start(bf16[64,2048]{1,0:T(8,128)(2,1)S(1)} %collective-permute-done.8.refs_13_), channel_id=1, source_target_pairs={{0,1},{1,0},{2,3},{3,2},{4,5},{5,4},{6,7},{7,6},{8,9},{9,8},{10,11... | collective-permute-start | bytes 786440 | tf_op jit(solution)/shard_map/ppermute | solution.py:352
  105.2 2.0 %collective-permute-start.27 = (bf16[64,2048]{1,0:T(8,128)(2,1)}, bf16[64,2048]{1,0:T(8,128)(2,1)}, u32[]{:S(2)}, u32[]{:S(2)}) collective-permute-start(bf16[64,2048]{1,0:T(8,128)(2,1)} %collective-permute-done.22.refs_1_), channel_id=1, source_target_pairs={{0,1},{1,0},{2,3},{3,2},{4,5},{5,4},{6,7},{7,6},{8,9},{9,8},{10,11... | collective-permute-start | bytes 786440 | tf_op jit(solution)/shard_map/ppermute | solution.py:352
  114.3 3.5 %early.1 = (f32[256,2048]{1,0:T(8,128)S(1)}, bf16[8,2,272,128]{3,2,1,0:T(8,128)(2,1)S(1)}) custom-call(bf16[1,2,272,128]{3,2,1,0:T(8,128)(2,1)S(1)} %constant_dynamic-slice_fusion.7.refs_0_, bf16[1,2,272,128]{3,2,1,0:T(8,128)(2,1)} %collective-permute-done.11.refs_1_, bf16[1,2,272,128]{3,2,1,0:T(8,128)(2,1)} %collective-permute-done.12.refs_2_, ...), custom_call_target="tpu_custom_call" | custom-call | tf_op jit(solution)/shard_map/early/pallas_call | solution.py:463
  117.8 2.3 %collective-permute-start.25 = (bf16[64,2048]{1,0:T(8,128)(2,1)}, bf16[64,2048]{1,0:T(8,128)(2,1)S(1)}, u32[]{:S(2)}, u32[]{:S(2)}) collective-permute-start(bf16[64,2048]{1,0:T(8,128)(2,1)} %collective-permute-done.23.refs_3_), channel_id=1, source_target_pairs={{0,8},{1,121},{2,10},{3,123},{4,12},{5,125},{6,14},{7,127},{8,16},... | collective-permute-start | bytes 786440 | tf_op jit(solution)/shard_map/ppermute | solution.py:346
  122.0 1.9 %collective-permute-done.25.refs_5_ = bf16[64,2048]{1,0:T(8,128)(2,1)S(1)} collective-permute-done((bf16[64,2048]{1,0:T(8,128)(2,1)}, bf16[64,2048]{1,0:T(8,128)(2,1)S(1)}, u32[]{:S(2)}, u32[]{:S(2)}) %collective-permute-start.25) | collective-permute-done | bytes 262176 | tf_op jit(solution)/shard_map/ppermute | solution.py:346
  123.8 2.8 %collective-permute-done.24.refs_4_ = bf16[64,2048]{1,0:T(8,128)(2,1)S(1)} collective-permute-done((bf16[64,2048]{1,0:T(8,128)(2,1)}, bf16[64,2048]{1,0:T(8,128)(2,1)S(1)}, u32[]{:S(2)}, u32[]{:S(2)}) %collective-permute-start.24) | collective-permute-done | bytes 262176 | tf_op jit(solution)/shard_map/ppermute | solution.py:346
  126.6 3.3 %late.1 = bf16[256,2048]{1,0:T(8,128)(2,1)} custom-call(bf16[8,2,272,128]{3,2,1,0:T(8,128)(2,1)S(1)} %get-tuple-element.58.arrived, f32[256,2048]{1,0:T(8,128)S(1)} %get-tuple-element.61.sums, bf16[64,2048]{1,0:T(8,128)(2,1)} %collective-permute-done.10.refs_0_, bf16[64,2048]{1,0:T(8,128)(2,1)} %collective-permute-done.22.refs_1_, ...), custom_call_target="tpu_custom_call" | custom-call | tf_op jit(solution)/shard_map/late/pallas_call | solution.py:475
  (96 shorter events, 28.8 us)
Async XLA Ops:
  0.0 29.7 %collective-permute-start = (bf16[128,2048]{1,0:T(8,128)(2,1)}, bf16[128,2048]{1,0:T(8,128)(2,1)S(1)}, u32[]{:S(2)}, u32[]{:S(2)}) collective-permute-start(bf16[128,2048]{1,0:T(8,128)(2,1)} %refs_8_.1), channel_id=1, source_target_pairs={{0,8},{1,121},{2,10},{3,123},{4,12},{5,125},{6,14},{7,127},{8,16},... | collective-permute-start | bytes 1572872 | tf_op jit(solution)/shard_map/ppermute | solution.py:346
  29.7 16.4 %collective-permute-start.2 = (bf16[128,2048]{1,0:T(8,128)(2,1)S(1)}, bf16[128,2048]{1,0:T(8,128)(2,1)S(1)}, u32[]{:S(2)}, u32[]{:S(2)}) collective-permute-start(bf16[128,2048]{1,0:T(8,128)(2,1)S(1)} %collective-permute-done.refs_9_), channel_id=1, source_target_pairs={{0,8},{1,121},{2,10},{3,123},{4,12},{5,125},{6,14},{7,127},{8,16},... | collective-permute-start | bytes 1572872 | tf_op jit(solution)/shard_map/ppermute | solution.py:346
  34.5 30.7 %collective-permute-start.3 = (bf16[128,2048]{1,0:T(8,128)(2,1)S(1)}, bf16[128,2048]{1,0:T(8,128)(2,1)S(1)}, u32[]{:S(2)}, u32[]{:S(2)}) collective-permute-start(bf16[128,2048]{1,0:T(8,128)(2,1)S(1)} %collective-permute-done.refs_9_), channel_id=1, source_target_pairs={{0,1},{1,0},{2,3},{3,2},{4,5},{5,4},{6,7},{7,6},{8,9},{9,8},{10,11... | collective-permute-start | bytes 1572872 | tf_op jit(solution)/shard_map/ppermute | solution.py:352
  46.1 20.0 %collective-permute-start.4 = (bf16[128,2048]{1,0:T(8,128)(2,1)S(1)}, bf16[128,2048]{1,0:T(8,128)(2,1)}, u32[]{:S(2)}, u32[]{:S(2)}) collective-permute-start(bf16[128,2048]{1,0:T(8,128)(2,1)S(1)} %collective-permute-done.2.refs_10_), channel_id=1, source_target_pairs={{0,8},{1,121},{2,10},{3,123},{4,12},{5,125},{6,14},{7,127},{8,16},... | collective-permute-start | bytes 1572872 | tf_op jit(solution)/shard_map/ppermute | solution.py:346
  49.0 19.7 %all-to-all-start = ((f32[16,8,256]{2,1,0:T(8,128)}), f32[16,8,256]{2,1,0:T(8,128)S(1)}, u32[]{:S(2)}, u32[]{:S(2)}) async-start(f32[16,8,256]{2,1,0:T(8,128)} %get-tuple-element.44), calls=%async_computation | async-start | bytes 262144 | tf_op jit(solution)/shard_map/all_to_all | solution.py:417
  53.0 26.5 %collective-permute-start.5 = (bf16[128,2048]{1,0:T(8,128)(2,1)S(1)}, bf16[128,2048]{1,0:T(8,128)(2,1)}, u32[]{:S(2)}, u32[]{:S(2)}) collective-permute-start(bf16[128,2048]{1,0:T(8,128)(2,1)S(1)} %collective-permute-done.2.refs_10_), channel_id=1, source_target_pairs={{0,1},{1,0},{2,3},{3,2},{4,5},{5,4},{6,7},{7,6},{8,9},{9,8},{10,11... | collective-permute-start | bytes 1572872 | tf_op jit(solution)/shard_map/ppermute | solution.py:352
  66.1 13.5 %collective-permute-start.6 = (bf16[128,2048]{1,0:T(8,128)(2,1)}, bf16[128,2048]{1,0:T(8,128)(2,1)S(1)}, u32[]{:S(2)}, u32[]{:S(2)}) collective-permute-start(bf16[128,2048]{1,0:T(8,128)(2,1)} %collective-permute-done.4.refs_11_), channel_id=1, source_target_pairs={{0,8},{1,121},{2,10},{3,123},{4,12},{5,125},{6,14},{7,127},{8,16},... | collective-permute-start | bytes 1572872 | tf_op jit(solution)/shard_map/ppermute | solution.py:346
  68.7 18.1 %collective-permute-start.7 = (bf16[128,2048]{1,0:T(8,128)(2,1)}, bf16[128,2048]{1,0:T(8,128)(2,1)}, u32[]{:S(2)}, u32[]{:S(2)}) collective-permute-start(bf16[128,2048]{1,0:T(8,128)(2,1)} %collective-permute-done.4.refs_11_), channel_id=1, source_target_pairs={{0,1},{1,0},{2,3},{3,2},{4,5},{5,4},{6,7},{7,6},{8,9},{9,8},{10,11... | collective-permute-start | bytes 1572872 | tf_op jit(solution)/shard_map/ppermute | solution.py:352
  73.0 8.8 %collective-permute-start.11 = (bf16[1,2,272,128]{3,2,1,0:T(8,128)(2,1)}, bf16[1,2,272,128]{3,2,1,0:T(8,128)(2,1)}, u32[]{:S(2)}, u32[]{:S(2)}) collective-permute-start(bf16[1,2,272,128]{3,2,1,0:T(8,128)(2,1)} %get-tuple-element.69), channel_id=1, source_target_pairs={{0,4},{1,5},{2,6},{3,7},{4,0},{5,1},{6,2},{7,3},{8,12},{9,13},{10,... | collective-permute-start | bytes 417800 | tf_op jit(solution)/shard_map/ppermute | solution.py:454
  76.0 8.6 %collective-permute-start.12 = (bf16[1,2,272,128]{3,2,1,0:T(8,128)(2,1)}, bf16[1,2,272,128]{3,2,1,0:T(8,128)(2,1)}, u32[]{:S(2)}, u32[]{:S(2)}) collective-permute-start(bf16[1,2,272,128]{3,2,1,0:T(8,128)(2,1)} %get-tuple-element.68), channel_id=1, source_target_pairs={{0,5},{1,4},{2,7},{3,6},{4,1},{5,0},{6,3},{7,2},{8,13},{9,12},{10,... | collective-permute-start | bytes 417800 | tf_op jit(solution)/shard_map/ppermute | solution.py:454
  80.4 8.2 %collective-permute-start.8 = (bf16[64,2048]{1,0:T(8,128)(2,1)}, bf16[64,2048]{1,0:T(8,128)(2,1)S(1)}, u32[]{:S(2)}, u32[]{:S(2)}) collective-permute-start(bf16[64,2048]{1,0:T(8,128)(2,1)} %get-tuple-element.71), channel_id=1, source_target_pairs={{0,8},{1,121},{2,10},{3,123},{4,12},{5,125},{6,14},{7,127},{8,16},... | collective-permute-start | bytes 786440 | tf_op jit(solution)/shard_map/ppermute | solution.py:346
  81.7 20.6 %collective-permute-start.9 = (bf16[128,2048]{1,0:T(8,128)(2,1)S(1)}, bf16[128,2048]{1,0:T(8,128)(2,1)S(1)}, u32[]{:S(2)}, u32[]{:S(2)}) collective-permute-start(bf16[128,2048]{1,0:T(8,128)(2,1)S(1)} %collective-permute-done.6.refs_12_), channel_id=1, source_target_pairs={{0,1},{1,0},{2,3},{3,2},{4,5},{5,4},{6,7},{7,6},{8,9},{9,8},{10,11... | collective-permute-start | bytes 1572872 | tf_op jit(solution)/shard_map/ppermute | solution.py:352
  81.8 12.0 %collective-permute-start.18 = (bf16[64,2048]{1,0:T(8,128)(2,1)}, bf16[64,2048]{1,0:T(8,128)(2,1)}, u32[]{:S(2)}, u32[]{:S(2)}) collective-permute-start(bf16[64,2048]{1,0:T(8,128)(2,1)} %get-tuple-element.70), channel_id=1, source_target_pairs={{0,8},{1,121},{2,10},{3,123},{4,12},{5,125},{6,14},{7,127},{8,16},... | collective-permute-start | bytes 786440 | tf_op jit(solution)/shard_map/ppermute | solution.py:346
  84.6 7.1 %collective-permute-start.13 = (bf16[1,2,272,128]{3,2,1,0:T(8,128)(2,1)S(1)}, bf16[1,2,272,128]{3,2,1,0:T(8,128)(2,1)S(1)}, u32[]{:S(2)}, u32[]{:S(2)}) collective-permute-start(bf16[1,2,272,128]{3,2,1,0:T(8,128)(2,1)S(1)} %get-tuple-element.67), channel_id=1, source_target_pairs={{0,2},{1,3},{2,4},{3,5},{4,6},{5,7},{6,0},{7,1},{8,10},{9,11},{10,... | collective-permute-start | bytes 417800 | tf_op jit(solution)/shard_map/ppermute | solution.py:454
  86.9 8.5 %collective-permute-start.14 = (bf16[1,2,272,128]{3,2,1,0:T(8,128)(2,1)S(1)}, bf16[1,2,272,128]{3,2,1,0:T(8,128)(2,1)S(1)}, u32[]{:S(2)}, u32[]{:S(2)}) collective-permute-start(bf16[1,2,272,128]{3,2,1,0:T(8,128)(2,1)S(1)} %get-tuple-element.66), channel_id=1, source_target_pairs={{0,3},{1,2},{2,5},{3,4},{4,7},{5,6},{6,1},{7,0},{8,11},{9,10},{10,... | collective-permute-start | bytes 417800 | tf_op jit(solution)/shard_map/ppermute | solution.py:454
  88.6 9.3 %collective-permute-start.15 = (bf16[1,2,272,128]{3,2,1,0:T(8,128)(2,1)S(1)}, bf16[1,2,272,128]{3,2,1,0:T(8,128)(2,1)S(1)}, u32[]{:S(2)}, u32[]{:S(2)}) collective-permute-start(bf16[1,2,272,128]{3,2,1,0:T(8,128)(2,1)S(1)} %get-tuple-element.65), channel_id=1, source_target_pairs={{0,6},{1,7},{2,0},{3,1},{4,2},{5,3},{6,4},{7,5},{8,14},{9,15},{10,... | collective-permute-start | bytes 417800 | tf_op jit(solution)/shard_map/ppermute | solution.py:454
  93.8 9.4 %collective-permute-start.22 = (bf16[64,2048]{1,0:T(8,128)(2,1)}, bf16[64,2048]{1,0:T(8,128)(2,1)}, u32[]{:S(2)}, u32[]{:S(2)}) collective-permute-start(bf16[64,2048]{1,0:T(8,128)(2,1)} %collective-permute-done.18.refs_14_), channel_id=1, source_target_pairs={{0,8},{1,121},{2,10},{3,123},{4,12},{5,125},{6,14},{7,127},{8,16},... | collective-permute-start | bytes 786440 | tf_op jit(solution)/shard_map/ppermute | solution.py:346
  96.0 7.3 %collective-permute-start.16 = (bf16[1,2,272,128]{3,2,1,0:T(8,128)(2,1)S(1)}, bf16[1,2,272,128]{3,2,1,0:T(8,128)(2,1)S(1)}, u32[]{:S(2)}, u32[]{:S(2)}) collective-permute-start(bf16[1,2,272,128]{3,2,1,0:T(8,128)(2,1)S(1)} %get-tuple-element.64), channel_id=1, source_target_pairs={{0,7},{1,6},{2,1},{3,0},{4,3},{5,2},{6,5},{7,4},{8,15},{9,14},{10,... | collective-permute-start | bytes 417800 | tf_op jit(solution)/shard_map/ppermute | solution.py:454
  98.9 8.4 %collective-permute-start.19 = (bf16[64,2048]{1,0:T(8,128)(2,1)S(1)}, bf16[64,2048]{1,0:T(8,128)(2,1)}, u32[]{:S(2)}, u32[]{:S(2)}) collective-permute-start(bf16[64,2048]{1,0:T(8,128)(2,1)S(1)} %collective-permute-done.8.refs_13_), channel_id=1, source_target_pairs={{0,1},{1,0},{2,3},{3,2},{4,5},{5,4},{6,7},{7,6},{8,9},{9,8},{10,11... | collective-permute-start | bytes 786440 | tf_op jit(solution)/shard_map/ppermute | solution.py:352
  103.2 14.7 %collective-permute-start.23 = (bf16[64,2048]{1,0:T(8,128)(2,1)}, bf16[64,2048]{1,0:T(8,128)(2,1)}, u32[]{:S(2)}, u32[]{:S(2)}) collective-permute-start(bf16[64,2048]{1,0:T(8,128)(2,1)} %collective-permute-done.22.refs_1_), channel_id=1, source_target_pairs={{0,8},{1,121},{2,10},{3,123},{4,12},{5,125},{6,14},{7,127},{8,16},... | collective-permute-start | bytes 786440 | tf_op jit(solution)/shard_map/ppermute | solution.py:346
  104.0 16.2 %collective-permute-start.21 = (bf16[64,2048]{1,0:T(8,128)(2,1)}, bf16[64,2048]{1,0:T(8,128)(2,1)}, u32[]{:S(2)}, u32[]{:S(2)}) collective-permute-start(bf16[64,2048]{1,0:T(8,128)(2,1)} %collective-permute-done.10.refs_0_), channel_id=1, source_target_pairs={{0,8},{1,121},{2,10},{3,123},{4,12},{5,125},{6,14},{7,127},{8,16},... | collective-permute-start | bytes 786440 | tf_op jit(solution)/shard_map/ppermute | solution.py:346
  105.2 16.7 %collective-permute-start.27 = (bf16[64,2048]{1,0:T(8,128)(2,1)}, bf16[64,2048]{1,0:T(8,128)(2,1)}, u32[]{:S(2)}, u32[]{:S(2)}) collective-permute-start(bf16[64,2048]{1,0:T(8,128)(2,1)} %collective-permute-done.22.refs_1_), channel_id=1, source_target_pairs={{0,1},{1,0},{2,3},{3,2},{4,5},{5,4},{6,7},{7,6},{8,9},{9,8},{10,11... | collective-permute-start | bytes 786440 | tf_op jit(solution)/shard_map/ppermute | solution.py:352
  107.3 14.7 %collective-permute-start.26 = (bf16[64,2048]{1,0:T(8,128)(2,1)}, bf16[64,2048]{1,0:T(8,128)(2,1)S(1)}, u32[]{:S(2)}, u32[]{:S(2)}) collective-permute-start(bf16[64,2048]{1,0:T(8,128)(2,1)} %collective-permute-done.10.refs_0_), channel_id=1, source_target_pairs={{0,1},{1,0},{2,3},{3,2},{4,5},{5,4},{6,7},{7,6},{8,9},{9,8},{10,11... | collective-permute-start | bytes 786440 | tf_op jit(solution)/shard_map/ppermute | solution.py:352
  120.2 6.4 %collective-permute-start.24 = (bf16[64,2048]{1,0:T(8,128)(2,1)}, bf16[64,2048]{1,0:T(8,128)(2,1)S(1)}, u32[]{:S(2)}, u32[]{:S(2)}) collective-permute-start(bf16[64,2048]{1,0:T(8,128)(2,1)} %collective-permute-done.21.refs_2_), channel_id=1, source_target_pairs={{0,8},{1,121},{2,10},{3,123},{4,12},{5,125},{6,14},{7,127},{8,16},... | collective-permute-start | bytes 786440 | tf_op jit(solution)/shard_map/ppermute | solution.py:346
  (30 other events, 192.7 us)

commit v4 on v3

--- a/solution.py
+++ b/solution.py
@@ -137,7 +137,7 @@
     if first:
         halo, scaled, refs = *refs[:2], refs[2:]
     else:
-        begun, refs = refs[0], refs[1:]
+        begun, refs = refs[0], refs[3:]
     state_out, prod_out, ends, conv_buf, decay_buf, drive_buf, carry, state, prod, sems = refs
     if first:
         conv_buf[0:8, :] = branch_product(halo[...], scaled[...]).astype(F32)[8:16]
@@ -153,8 +153,10 @@
 
     def leaving(k):
         at = (slice(None), pl.ds(pl.multiple_of(k * BLOCK, BLOCK), BLOCK), slice(None))
+        block = k + (0 if first else blocks)
+        to = (slice(None), pl.ds(pl.multiple_of(block * BLOCK, BLOCK), BLOCK), slice(None))
         return [
-            pltpu.make_async_copy(ref.at[at], out.at[at], sems.at[n, k])
+            pltpu.make_async_copy(ref.at[at], out.at[to], sems.at[n, k])
             for n, (ref, out) in enumerate(((state, state_out), (prod, prod_out)))
         ]
 
@@ -210,18 +212,20 @@
     ends[...] = jnp.broadcast_to(carry[...][None], ends.shape)
 
 
-def gated_kernel(state_1, state_2, prod_1, prod_2, gate, ends, gain, sent, incoming, states, prods, gates, sems):
-    count = sent.shape[0]
+def gated_kernel(state, prod, gate, ends, gain, *refs, order):
+    count = len(order)
+    parts, (incoming, states, prods, gates, sems) = refs[:count], refs[count:]
+    seat = lax.axis_index("tp")
     copies = []
-    for d in range(count):
-        state, prod = (state_1, prod_1) if d < count // 2 else (state_2, prod_2)
-        near = pl.ds(d % (count // 2) * BLOCK, BLOCK)
-        at = pl.ds(d * BLOCK, BLOCK)
+    for k, (dx, dc) in enumerate(order):
+        to = neighbour(seat, dx, dc, count // 2)
+        far = pl.ds(pl.multiple_of(to * BLOCK, BLOCK), BLOCK)
+        at = pl.ds(k * BLOCK, BLOCK)
         copies.append(
             [
-                pltpu.make_async_copy(state.at[:, near, :], states.at[:, at, :], sems.at[0, d]),
-                pltpu.make_async_copy(prod.at[:, near, :], prods.at[:, at, :], sems.at[1, d]),
-                pltpu.make_async_copy(gate.at[at, :], gates.at[at, :], sems.at[2, d]),
+                pltpu.make_async_copy(state.at[:, far, :], states.at[:, at, :], sems.at[0, k]),
+                pltpu.make_async_copy(prod.at[:, far, :], prods.at[:, at, :], sems.at[1, k]),
+                pltpu.make_async_copy(gate.at[far, :], gates.at[at, :], sems.at[2, k]),
             ]
         )
         for copy in copies[-1]:
@@ -234,15 +238,15 @@
 
     ones = jnp.ones((8, 128), BF16)
     over = (((1,), (1,)), ((), ()))
-    for d in range(count):
-        for copy in copies[d]:
+    for k, part in enumerate(parts):
+        for copy in copies[k]:
             copy.wait()
-        rows = slice(d * BLOCK, d * BLOCK + BLOCK)
+        rows = slice(k * BLOCK, k * BLOCK + BLOCK)
         total = jnp.zeros((8, BLOCK), F32)
         for half in range(2):
             lanes = slice(half * 128, half * 128 + 128)
             gated = (states[half, rows, :] + prods[half, rows, :] * incoming[0:1, lanes]) * gates[rows, lanes]
-            sent[d, half, 0:BLOCK, :] = (gated * gain[:, lanes]).astype(BF16)
+            part[half, 0:BLOCK, :] = (gated * gain[:, lanes]).astype(BF16)
             square = gated * gated
             high = square.astype(BF16)
             low = (square - high.astype(F32)).astype(BF16)
@@ -253,7 +257,7 @@
         lines = jnp.where(row == 0, top, jnp.where(row == 1, total - top, 0.0))
         lines = jnp.concatenate([lines, jnp.zeros_like(lines)], 0).astype(BF16)
         for half in range(2):
-            sent[d, half, BLOCK : BLOCK + EXTRA, :] = lines[:, half * 128 : half * 128 + 128]
+            part[half, BLOCK : BLOCK + EXTRA, :] = lines[:, half * 128 : half * 128 + 128]
 
 
 def neighbour(seat, dx, dc, chips):
@@ -269,38 +273,57 @@
     return [lax.rem(span + spans + jnp.where(core == 0, k, -k), spans) for k in offsets]
 
 
-def joined(blocks, depth):
-    whole, parts = [], []
-    for block in blocks:
-        parts.append(block)
-        if sum(part.shape[0] for part in parts) == depth:
-            whole.append(parts)
-            parts = []
-    return whole
+def grouped(refs, sizes):
+    refs = list(refs)
+    return [[refs.pop(0) for _ in range(size)] for size in sizes]
 
 
 def product(arrived, places, groups, low, step):
     mixed = jnp.concatenate([arrived[lax.div(place, 2), lax.rem(place, 2), 0:BLOCK, :] for place in places], 1)
-    weights = jnp.concatenate([part[:, low : low + step] for parts in groups for part in parts], 0)
-    return jnp.dot(mixed, weights, preferred_element_type=F32)
-
-
-def early_kernel(*refs, order, offsets, spans, depth):
+    weights = []
+    for parts in groups:
+        span = parts[0].shape[1]
+        weights.append(parts[low // span][:, low % span : low % span + step])
+    return jnp.dot(mixed, jnp.concatenate(weights, 0), preferred_element_type=F32)
+
+
+def early_kernel(*refs, order, here, away, sizes, spans):
     count = len(order)
-    out, arrived = refs[-2:]
+    out, arrived, held, sems = refs[-4:]
+    outside = refs[-4 - len(away) : -4]
+    depth = outside[0].shape[0]
+    copies = [
+        pltpu.make_async_copy(block, held.at[pl.ds(k * depth, depth), :], sems.at[k])
+        for k, block in enumerate(outside)
+    ]
+    for copy in copies:
+        copy.start()
     seat = lax.axis_index("tp")
     for (dx, dc), part in zip(order, refs[:count]):
-        arrived[neighbour(seat, count // 2 - dx, dc, count // 2)] = part[0]
-    groups = joined(refs[count:-2], depth)
+        arrived[neighbour(seat, count // 2 - dx, dc, count // 2)] = part[...]
+    groups = grouped(refs[count:], sizes)
+    places = places_of(here, spans)
+    step = 512
+    for low in range(0, out.shape[1], step):
+        out[:, low : low + step] = product(arrived, places, groups, low, step)
+    for copy in copies:
+        copy.wait()
+    places = places_of(away, spans)
+    for low in range(0, out.shape[1], step):
+        out[:, low : low + step] = out[:, low : low + step] + product(arrived, places, [[held]], low, step)
+
+
+def middle_kernel(arrived, sums, *refs, offsets, sizes, spans):
+    groups, out = grouped(refs, sizes), refs[-1]
     places = places_of(offsets, spans)
     step = 512
     for low in range(0, out.shape[1], step):
-        out[:, low : low + step] = product(arrived, places, groups, low, step)
-
-
-def late_kernel(arrived, sums, *refs, offsets, spans, depth, channels):
-    groups, out = joined(refs[:-1], depth), refs[-1]
-    places = places_of(offsets, spans)
+        out[:, low : low + step] = sums[:, low : low + step] + product(arrived, places, groups, low, step)
+
+
+def late_kernel(arrived, sums, near, far, out, *, offset, spans, channels):
+    places = places_of([offset], spans)
+    core = lax.axis_index("tp") % 2
     ones = jnp.ones((arrived.shape[0] * EXTRA, 128), BF16)
     square = []
     for half in range(2):
@@ -312,8 +335,12 @@
         )
     scale = lax.rsqrt(jnp.concatenate(square, 0)[:, 0:1] / channels + EPS)
     step = 512
+    span = near.shape[1]
+    mixed = arrived[lax.div(places[0], 2), lax.rem(places[0], 2), 0:BLOCK, :]
     for low in range(0, out.shape[1], step):
-        acc = sums[:, low : low + step] + product(arrived, places, groups, low, step)
+        at = slice(low % span, low % span + step)
+        weights = jnp.where(core == low // span, near[:, at].astype(F32), far[:, at].astype(F32)).astype(BF16)
+        acc = sums[:, low : low + step] + jnp.dot(mixed, weights, preferred_element_type=F32)
         out[:, low : low + step] = (acc * scale).astype(BF16)
 
 
@@ -353,18 +380,15 @@
         swapped.append(made)
 
     def advance(value, pieces=1):
-        before = swapped[-2] if len(swapped) > 1 else []
-        value, *rest = tie(value, *before, *moved[-1][:1])
-        if before:
-            swapped[-2] = rest[:-1]
-        moved[-1] = rest[-1:] + moved[-1][1:]
-        if len(moved) < reach:
-            parts = moved[-1]
-            if len(parts) < pieces:
-                cut = depth // pieces
-                parts = [parts[0][k * cut : k * cut + cut] for k in range(pieces)]
-            onward(parts)
-            across(moved[-2])
+        *value, moved[-1][0] = tie(*value, moved[-1][0])
+        parts = moved[-1]
+        across(parts)
+        if len(parts) < pieces:
+            cut = out_width // pieces
+            parts = [parts[0][:, k * cut : k * cut + cut] for k in range(pieces)]
+        if len(moved) == reach - 1:
+            parts = [jnp.where(lax.axis_index("tp") % 2 == 0, *parts)]
+        onward(parts)
         return value
 
     fixed = pl.BlockSpec(memory_space=pltpu.VMEM)
@@ -394,10 +418,10 @@
         half_shape = (2, half_rows, head // 2)
         return pl.pallas_call(
             functools.partial(recur_kernel, first=first),
-            in_specs=[fixed] * (6 + len(extra)),
+            in_specs=[fixed] * (8 if first else 7) + [hbm] * (0 if first else 2),
             out_specs=[hbm, hbm, fixed],
             out_shape=[
-                pltpu.HBM(half_shape, F32), pltpu.HBM(half_shape, F32),
+                pltpu.HBM((2, rows, head // 2), F32), pltpu.HBM((2, rows, head // 2), F32),
                 jax.ShapeDtypeStruct((many, 8, head), F32),
             ],
             scratch_shapes=[
@@ -406,16 +430,18 @@
                 pltpu.VMEM(half_shape, F32), pltpu.VMEM(half_shape, F32),
                 pltpu.SemaphoreType.DMA((2, half_rows // BLOCK)),
             ],
+            input_output_aliases={} if first else {7: 0, 8: 1},
             compiler_params=limit(12),
             name="recur",
         )(on_chip(projected), conv_taps, w_rate, w_inlet, decay_param.reshape(1, head), decay_bias, *extra)
 
-    projected = advance(projected)
-    state_1, prod_1, begun = recur(True, halo, on_chip(scaled))
-    state_2, prod_2, ends = recur(False, begun)
-    ends = advance(ends)
+    (projected,) = advance([projected])
+    state, prod, begun = recur(True, halo, on_chip(scaled))
+    state, prod, ends = recur(False, begun, in_hbm(state), in_hbm(prod))
+    (ends,) = advance([ends])
     all_ends = lax.all_to_all(ends, "sp", split_axis=0, concat_axis=0, tiled=True)
     late_tokens, _ = tie(tokens, ends)
+    (late_tokens,) = advance([late_tokens])
     gate = pl.pallas_call(
         gate_kernel,
         in_specs=[hbm, fixed, fixed],
@@ -428,13 +454,13 @@
         compiler_params=limit(20),
         name="gate",
     )(in_hbm(late_tokens), gain_row, w_gate)
-    gate = advance(gate)
-
-    sent = pl.pallas_call(
-        gated_kernel,
-        in_specs=[hbm] * 5 + [fixed] * 2,
-        out_specs=fixed,
-        out_shape=pltpu.VMEM((heads, 2, BLOCK + EXTRA, head // 2), BF16),
+    order = [(dx, dc) for dx in EXCHANGE for dc in range(2)]
+    part_shape = (2, BLOCK + EXTRA, head // 2)
+    parts = pl.pallas_call(
+        functools.partial(gated_kernel, order=order),
+        in_specs=[hbm] * 3 + [fixed] * 2,
+        out_specs=[fixed] * heads,
+        out_shape=[pltpu.VMEM(part_shape, BF16)] * heads,
         scratch_shapes=[
             pltpu.VMEM((8, head), F32), pltpu.VMEM((2, rows, head // 2), F32),
             pltpu.VMEM((2, rows, head // 2), F32), pltpu.VMEM((rows, head), F32),
@@ -442,44 +468,58 @@
         ],
         compiler_params=limit(12),
         name="gated",
-    )(*map(in_hbm, (state_1, state_2, prod_1, prod_2, gate)), all_ends, out_gain.reshape(1, head))
-    seat = lax.axis_index("tp")
-    order = [(dx, dc) for dx in EXCHANGE for dc in range(2) if (dx, dc) != (0, 0)]
+    )(*map(in_hbm, (state, prod, gate)), all_ends, out_gain.reshape(1, head))
+
+    parts = advance(parts, STREAMS)
     moves = []
-    for dx, dc in order:
+    for k, (dx, dc) in enumerate(order):
+        if (dx, dc) == (1, 0):
+            parts = parts[:k] + advance(parts[k:])
+        if (dx, dc) == (0, 0):
+            parts = parts[:k] + advance(parts[k:])
+            moves.append(parts[k])
+            continue
         to = lambda t: neighbour(t, dx, dc, heads // 2)
-        if (dx, dc) == (1, 0):
-            sent = advance(sent, STREAMS)
-        part = lax.dynamic_slice_in_dim(sent, to(seat), 1, 0)
-        moves.append(lax.ppermute(part, "tp", [(t, to(t)) for t in range(heads)]))
-    holding = sent
-    while len(moved) < reach - 1:
-        holding = advance(holding, STREAMS)
-    own = lax.dynamic_slice_in_dim(holding, seat, 1, 0)
+        moves.append(lax.ppermute(parts[k], "tp", [(t, to(t)) for t in range(heads)]))
+    (moves[-2],) = advance([moves[-2]])
+    across(moved[-1])
+
     flat = lambda groups: [on_chip(part) for parts in groups for part in parts]
-    done = len(swapped) - 1
-    offsets = [0] + [-k for k in range(1, done + 1)] + list(range(1, done + 1))
-    blocks = [on_chip(w_out)] + flat(moved[:done]) + flat(swapped[:done])
+    sizes_of = lambda groups: [len(parts) for parts in groups]
+    groups = moved[3:6] + swapped[3:5]
+    here = [-4, -5, -6, 4, 5]
+    outside = [w_out] + [parts[0] for parts in moved[:3] + swapped[:3]]
+    away = [0, -1, -2, -3, 1, 2, 3]
     sums, arrived = pl.pallas_call(
-        functools.partial(early_kernel, order=[(0, 0)] + order, offsets=offsets, spans=spans, depth=depth),
-        in_specs=[fixed] * (1 + len(moves) + len(blocks)),
+        functools.partial(
+            early_kernel, order=order, here=here, away=away, sizes=sizes_of(groups), spans=spans
+        ),
+        in_specs=[fixed] * (len(moves) + len(flat(groups))) + [hbm] * len(outside),
         out_specs=[fixed] * 2,
-        out_shape=[pltpu.VMEM((BLOCK, out_width), F32), pltpu.VMEM(sent.shape, BF16)],
+        out_shape=[pltpu.VMEM((BLOCK, out_width), F32), pltpu.VMEM((heads, *part_shape), BF16)],
+        scratch_shapes=[
+            pltpu.VMEM((len(away) * depth, out_width), BF16), pltpu.SemaphoreType.DMA((len(away),)),
+        ],
+        compiler_params=limit(20),
+        name="early",
+    )(*map(on_chip, moves), *flat(groups), *map(in_hbm, outside))
+    groups = moved[6:7] + swapped[5:7]
+    sums = pl.pallas_call(
+        functools.partial(middle_kernel, offsets=[-7, 6, 7], sizes=sizes_of(groups), spans=spans),
+        in_specs=[fixed] * (2 + len(flat(groups))),
+        out_specs=fixed,
+        out_shape=pltpu.VMEM((BLOCK, out_width), F32),
         compiler_params=limit(12),
-        name="early",
-    )(on_chip(own), *map(on_chip, moves), *blocks)
-    while len(moved) < reach:
-        sums = advance(sums, STREAMS)
-    offsets = [-k for k in range(done + 1, reach + 1)] + list(range(done + 1, reach))
-    blocks = flat(moved[done:]) + flat(swapped[done:])
+        name="middle",
+    )(on_chip(arrived), on_chip(sums), *flat(groups))
     return pl.pallas_call(
-        functools.partial(late_kernel, offsets=offsets, spans=spans, depth=depth, channels=heads * head),
-        in_specs=[fixed] * (2 + len(blocks)),
+        functools.partial(late_kernel, offset=reach, spans=spans, channels=heads * head),
+        in_specs=[fixed] * 4,
         out_specs=fixed,
         out_shape=jax.ShapeDtypeStruct((BLOCK, out_width), BF16),
         compiler_params=limit(12),
         name="late",
-    )(on_chip(arrived), on_chip(sums), *blocks)
+    )(on_chip(arrived), on_chip(sums), *flat(moved[7:] + swapped[7:]))
 
 
 def solution(mesh):

time: 131 us -> 136 us (1.038)
  waiting for transfers between devices: 9.88 us -> 26.3 us
  local copies, waits for them, and re-layouts: 14 us -> 0.95 us
  starting transfers between devices: 73 us -> 75.3 us
    unnamed x46 -> x30, local copies, waits for them, and re-layouts: 11.5 us -> 0.07 us
    ppermute x7, waiting for transfers between devices: 3.41 us -> 9.84 us  [body(): lax.ppermute(parts[k], 'tp', [(t, to(t)) for t in range(heads)])]
    all_to_all x1, waiting for transfers between devices: 0.01 us -> 5.36 us  [body(): lax.all_to_all(ends, 'sp', split_axis=0, concat_axis=0, tiled=True)]
    ppermute x12 -> x11, waiting for transfers between devices: 4.7 us -> 9.14 us  [onward(): made.append(lax.ppermute(part, ('sp', 'tp'), around))]
    ppermute x12 -> x11, starting transfers between devices: 41 us -> 44.5 us  [onward(): made.append(lax.ppermute(part, ('sp', 'tp'), around))]
    ppermute x7, starting transfers between devices: 14.5 us -> 11.7 us  [body(): lax.ppermute(parts[k], 'tp', [(t, to(t)) for t in range(heads)])]
    ppermute x10 -> x11, starting transfers between devices: 12.2 us -> 13.8 us  [across(): made.append(lax.ppermute(part, ('sp', 'tp'), swap))]
    pallas_call x3 -> x4, Pallas kernels: 10.3 us -> 10.4 us  [the longest x1 4.12 us: body(): pl.pallas_call(functools.partial(early_kernel, order=order, here=here, aw...]
  transfers between devices with their start and end apart: 31 -> 31, of which waited for: 6 -> 12; matrix products, arithmetic and copies ran while one was open for 2% -> 1% of each run, Pallas kernels for 23% -> 23%
where the time goes in v4:
time: 136 us
  starting transfers between devices  75.3 us (55%)
  Pallas kernels  32.9 us (24%)
  waiting for transfers between devices  26.3 us (19%)
    ppermute x11, starting transfers between devices, onward(): made.append(lax.ppermute(part, ('sp', 'tp'), around))  44.5 us
    ppermute x11, starting transfers between devices, across(): made.append(lax.ppermute(part, ('sp', 'tp'), swap))  13.8 us
    ppermute x7, starting transfers between devices, body(): lax.ppermute(parts[k], 'tp', [(t, to(t)) for t in range(heads)])  11.7 us
    ppermute x7, waiting for transfers between devices, body(): lax.ppermute(parts[k], 'tp', [(t, to(t)) for t in range(heads)])  9.84 us
    pallas_call x2, Pallas kernels, recur(): pl.pallas_call(functools.partial(recur_kernel, first=first), in_specs=[fi...  9.64 us
    ppermute x11, waiting for transfers between devices, onward(): made.append(lax.ppermute(part, ('sp', 'tp'), around))  9.14 us
    pallas_call x1, Pallas kernels, body(): pl.pallas_call(input_kernel, in_specs=[hbm] * 3, out_specs=[fixed] * 2, o...  6.78 us
    pallas_call x1, Pallas kernels, body(): pl.pallas_call(gate_kernel, in_specs=[hbm, fixed, fixed], out_specs=hbm,...  6.06 us
  transfers between devices with their start and end apart: 31, of which 12 were waited for; matrix products, arithmetic and copies ran while one was open for 1% of the time, Pallas kernels for 23%

profile of v4, /device:TPU:33, one launch (start us, length us, event | category | flops | bytes accessed | tf_op | source)
XLA Modules:
  0.0 135.7 jit_solution(9782669660236298416)
XLA Ops:
  0.0 22.9 %collective-permute-start = (bf16[128,2048]{1,0:T(8,128)(2,1)}, bf16[128,2048]{1,0:T(8,128)(2,1)S(1)}, u32[]{:S(2)}, u32[]{:S(2)}) collective-permute-start(bf16[128,2048]{1,0:T(8,128)(2,1)} %refs_16_.1), channel_id=1, source_target_pairs={{0,8},{1,121},{2,10},{3,123},{4,12},{5,125},{6,14},{7,127},{8,16},... | collective-permute-start | bytes 1572872 | tf_op jit(solution)/shard_map/ppermute | solution.py:373
  22.9 6.8 %input.1 = (bf16[2048,256]{1,0:T(8,128)(2,1)S(1)}, bf16[2048,256]{1,0:T(8,128)(2,1)S(1)}) custom-call(bf16[2048,2048]{1,0:T(8,128)(2,1)} %tokens.2, f32[1,2048]{1,0:T(1,128)} %bitcast.3, bf16[2048,256]{1,0:T(8,128)(2,1)} %w_input.1), custom_call_target="tpu_custom_call" | custom-call | tf_op jit(solution)/shard_map/input/pallas_call | solution.py:401
  29.7 2.6 %collective-permute-start.2 = (bf16[128,2048]{1,0:T(8,128)(2,1)S(1)}, bf16[128,2048]{1,0:T(8,128)(2,1)S(1)}, u32[]{:S(2)}, u32[]{:S(2)}) collective-permute-start(bf16[128,2048]{1,0:T(8,128)(2,1)S(1)} %collective-permute-done.refs_17_), channel_id=1, source_target_pairs={{0,8},{1,121},{2,10},{3,123},{4,12},{5,125},{6,14},{7,127},{8,16},... | collective-permute-start | bytes 1572872 | tf_op jit(solution)/shard_map/ppermute | solution.py:373
  36.4 4.6 %recur.2 = (f32[2,2048,128]{2,1,0:T(8,128)}, f32[2,2048,128]{2,1,0:T(8,128)}, f32[1,8,256]{2,1,0:T(8,128)S(1)}) custom-call(bf16[2048,256]{1,0:T(8,128)(2,1)S(1)} %get-tuple-element.52.projected, f32[4,256]{1,0:T(4,128)S(1)} %copy-done.5, bf16[1,256,256]{2,1,0:T(8,128)(2,1)S(1)} %copy-done.1, bf16[1,256,256]{2,1,0:T(8,128)(2,1)S(1)} %copy-done.2, ...), custom_call_target="tpu_custom_call" | custom-call | tf_op jit(solution)/shard_map/recur/pallas_call | solution.py:419
  41.1 5.0 %recur.3 = (f32[2,2048,128]{2,1,0:T(8,128)}, f32[2,2048,128]{2,1,0:T(8,128)}, f32[16,8,256]{2,1,0:T(8,128)}) custom-call(bf16[2048,256]{1,0:T(8,128)(2,1)S(1)} %get-tuple-element.52.projected, f32[4,256]{1,0:T(4,128)S(1)} %copy-done.5, bf16[1,256,256]{2,1,0:T(8,128)(2,1)S(1)} %copy-done.1, ...), custom_call_target="tpu_custom_call", output_to_operand_aliasing={{0}: (7, {}), {1}: (8, {})} | custom-call | tf_op jit(solution)/shard_map/recur/pallas_call | solution.py:419
  46.1 3.0 %collective-permute-start.3 = (bf16[128,2048]{1,0:T(8,128)(2,1)S(1)}, bf16[128,2048]{1,0:T(8,128)(2,1)}, u32[]{:S(2)}, u32[]{:S(2)}) collective-permute-start(bf16[128,2048]{1,0:T(8,128)(2,1)S(1)} %collective-permute-done.2.refs_18_), channel_id=1, source_target_pairs={{0,8},{1,121},{2,10},{3,123},{4,12},{5,125},{6,14},{7,127},{8,16},... | collective-permute-start | bytes 1572872 | tf_op jit(solution)/shard_map/ppermute | solution.py:373
  49.1 6.3 %collective-permute-done.3.refs_19_ = bf16[128,2048]{1,0:T(8,128)(2,1)} collective-permute-done((bf16[128,2048]{1,0:T(8,128)(2,1)S(1)}, bf16[128,2048]{1,0:T(8,128)(2,1)}, u32[]{:S(2)}, u32[]{:S(2)}) %collective-permute-start.3) | collective-permute-done | bytes 524320 | tf_op jit(solution)/shard_map/ppermute | solution.py:373
  55.4 3.0 %collective-permute-start.4 = (bf16[128,2048]{1,0:T(8,128)(2,1)}, bf16[128,2048]{1,0:T(8,128)(2,1)S(1)}, u32[]{:S(2)}, u32[]{:S(2)}) collective-permute-start(bf16[128,2048]{1,0:T(8,128)(2,1)} %collective-permute-done.3.refs_19_), channel_id=1, source_target_pairs={{0,8},{1,121},{2,10},{3,123},{4,12},{5,125},{6,14},{7,127},{8,16},... | collective-permute-start | bytes 1572872 | tf_op jit(solution)/shard_map/ppermute | solution.py:373
  58.5 4.0 %all-to-all-start = ((f32[16,8,256]{2,1,0:T(8,128)}), f32[16,8,256]{2,1,0:T(8,128)S(1)}, u32[]{:S(2)}, u32[]{:S(2)}) async-start(f32[16,8,256]{2,1,0:T(8,128)} %get-tuple-element.61), calls=%async_computation | async-start | bytes 262144 | tf_op jit(solution)/shard_map/all_to_all | solution.py:442
  62.5 6.1 %gate.1 = f32[2048,256]{1,0:T(8,128)} custom-call(bf16[2048,2048]{1,0:T(8,128)(2,1)} %tokens.2, f32[1,2048]{1,0:T(1,128)S(1)} %bitcast.4, bf16[2048,256]{1,0:T(8,128)(2,1)S(1)} %copy-done), custom_call_target="tpu_custom_call" | custom-call | tf_op jit(solution)/shard_map/gate/pallas_call | solution.py:445
  68.5 5.4 %all-to-all-done.ends = f32[16,8,256]{2,1,0:T(8,128)S(1)} async-done(((f32[16,8,256]{2,1,0:T(8,128)}), f32[16,8,256]{2,1,0:T(8,128)S(1)}, u32[]{:S(2)}, u32[]{:S(2)}) %all-to-all-start) | async-done | bytes 131104 | tf_op jit(solution)/shard_map/all_to_all | solution.py:442
  73.9 4.0 %gated.1 = (bf16[2,272,128]{2,1,0:T(8,128)(2,1)S(1)}, bf16[2,272,128]{2,1,0:T(8,128)(2,1)}, bf16[2,272,128]{2,1,0:T(8,128)(2,1)}, bf16[2,272,128]{2,1,0:T(8,128)...) custom-call(f32[2,2048,128]{2,1,0:T(8,128)} %get-tuple-element.57.st, ...), custom_call_target="tpu_custom_call" | custom-call | tf_op jit(solution)/shard_map/gated/pallas_call | solution.py:459
  79.6 8.4 %collective-permute-start.20 = (bf16[128,2048]{1,0:T(8,128)(2,1)S(1)}, bf16[128,2048]{1,0:T(8,128)(2,1)S(1)}, u32[]{:S(2)}, u32[]{:S(2)}) collective-permute-start(bf16[128,2048]{1,0:T(8,128)(2,1)S(1)} %collective-permute-done.refs_17_), channel_id=1, source_target_pairs={{0,1},{1,0},{2,3},{3,2},{4,5},{5,4},{6,7},{7,6},{8,9},{9,8},{10,11... | collective-permute-start | bytes 1572872 | tf_op jit(solution)/shard_map/ppermute | solution.py:379
  91.3 2.3 %collective-permute-done.15.refs_10_ = bf16[128,1024]{1,0:T(8,128)(2,1)S(1)} collective-permute-done((bf16[128,1024]{1,0:T(8,128)(2,1)S(1)}, bf16[128,1024]{1,0:T(8,128)(2,1)S(1)}, u32[]{:S(2)}, u32[]{:S(2)}) %collective-permute-start.15) | collective-permute-done | bytes 262176 | tf_op jit(solution)/shard_map/ppermute | solution.py:373
  93.5 2.6 %collective-permute-start.16 = (bf16[128,1024]{1,0:T(8,128)(2,1)S(1)}, bf16[128,1024]{1,0:T(8,128)(2,1)S(1)}, u32[]{:S(2)}, u32[]{:S(2)}) collective-permute-start(bf16[128,1024]{1,0:T(8,128)(2,1)S(1)} %collective-permute-done.15.refs_10_), channel_id=1, source_target_pairs={{0,8},{1,121},{2,10},{3,123},{4,12},{5,125},{6,14},{7,127},{8,16},... | collective-permute-start | bytes 786440 | tf_op jit(solution)/shard_map/ppermute | solution.py:373
  96.3 2.6 %collective-permute-start.13 = (bf16[128,1024]{1,0:T(8,128)(2,1)S(1)}, bf16[128,1024]{1,0:T(8,128)(2,1)S(1)}, u32[]{:S(2)}, u32[]{:S(2)}) collective-permute-start(bf16[128,1024]{1,0:T(8,128)(2,1)S(1)} %collective-permute-done.12.refs_11_), channel_id=1, source_target_pairs={{0,8},{1,121},{2,10},{3,123},{4,12},{5,125},{6,14},{7,127},{8,16},... | collective-permute-start | bytes 786440 | tf_op jit(solution)/shard_map/ppermute | solution.py:373
  99.0 3.0 %collective-permute-start.5 = (bf16[2,272,128]{2,1,0:T(8,128)(2,1)S(1)}, bf16[2,272,128]{2,1,0:T(8,128)(2,1)S(1)}, u32[]{:S(2)}, u32[]{:S(2)}) collective-permute-start(bf16[2,272,128]{2,1,0:T(8,128)(2,1)S(1)} %get-tuple-element.74), channel_id=1, source_target_pairs={{0,4},{1,5},{2,6},{3,7},{4,0},{5,1},{6,2},{7,3},{8,12},{9,13},{10,... | collective-permute-start | bytes 417800 | tf_op jit(solution)/shard_map/ppermute | solution.py:483
  102.6 5.2 %collective-permute-start.6 = (bf16[2,272,128]{2,1,0:T(8,128)(2,1)}, bf16[2,272,128]{2,1,0:T(8,128)(2,1)S(1)}, u32[]{:S(2)}, u32[]{:S(2)}) collective-permute-start(bf16[2,272,128]{2,1,0:T(8,128)(2,1)} %get-tuple-element.75), channel_id=1, source_target_pairs={{0,5},{1,4},{2,7},{3,6},{4,1},{5,0},{6,3},{7,2},{8,13},{9,12},{10,... | collective-permute-start | bytes 417800 | tf_op jit(solution)/shard_map/ppermute | solution.py:483
  109.9 2.3 %collective-permute-done.6.refs_1_ = bf16[2,272,128]{2,1,0:T(8,128)(2,1)S(1)} collective-permute-done((bf16[2,272,128]{2,1,0:T(8,128)(2,1)}, bf16[2,272,128]{2,1,0:T(8,128)(2,1)S(1)}, u32[]{:S(2)}, u32[]{:S(2)}) %collective-permute-start.6) | collective-permute-done | bytes 139296 | tf_op jit(solution)/shard_map/ppermute | solution.py:483
  113.2 2.2 %collective-permute-done.8.refs_2_ = bf16[2,272,128]{2,1,0:T(8,128)(2,1)S(1)} collective-permute-done((bf16[2,272,128]{2,1,0:T(8,128)(2,1)}, bf16[2,272,128]{2,1,0:T(8,128)(2,1)S(1)}, u32[]{:S(2)}, u32[]{:S(2)}) %collective-permute-start.8) | collective-permute-done | bytes 139296 | tf_op jit(solution)/shard_map/ppermute | solution.py:483
  115.8 2.6 %collective-permute-done.9.refs_3_ = bf16[2,272,128]{2,1,0:T(8,128)(2,1)S(1)} collective-permute-done((bf16[2,272,128]{2,1,0:T(8,128)(2,1)}, bf16[2,272,128]{2,1,0:T(8,128)(2,1)S(1)}, u32[]{:S(2)}, u32[]{:S(2)}) %collective-permute-start.9) | collective-permute-done | bytes 139296 | tf_op jit(solution)/shard_map/ppermute | solution.py:483
  120.4 2.8 %collective-permute-start.28 = (bf16[128,1024]{1,0:T(8,128)(2,1)S(1)}, bf16[128,1024]{1,0:T(8,128)(2,1)S(1)}, u32[]{:S(2)}, u32[]{:S(2)}) collective-permute-start(bf16[128,1024]{1,0:T(8,128)(2,1)S(1)} %broadcast_select_fusion), channel_id=1, source_target_pairs={{0,8},{1,121},{2,10},{3,123},{4,12},{5,125},{6,14},{7,127},{8,16},... | collective-permute-start | bytes 786440 | tf_op jit(solution)/shard_map/ppermute | solution.py:373
  126.6 2.7 %collective-permute-start.29 = (bf16[128,1024]{1,0:T(8,128)(2,1)S(1)}, bf16[128,1024]{1,0:T(8,128)(2,1)S(1)}, u32[]{:S(2)}, u32[]{:S(2)}) collective-permute-start(bf16[128,1024]{1,0:T(8,128)(2,1)S(1)} %collective-permute-done.28.near), channel_id=1, source_target_pairs={{0,1},{1,0},{2,3},{3,2},{4,5},{5,4},{6,7},{7,6},{8,9},{9,8},{10,11... | collective-permute-start | bytes 786440 | tf_op jit(solution)/shard_map/ppermute | solution.py:379
  129.3 4.1 %early.1 = (f32[256,2048]{1,0:T(8,128)S(1)}, bf16[8,2,272,128]{3,2,1,0:T(8,128)(2,1)S(1)}) custom-call(bf16[2,272,128]{2,1,0:T(8,128)(2,1)S(1)} %collective-permute-done.5.refs_0_, bf16[2,272,128]{2,1,0:T(8,128)(2,1)S(1)} %collective-permute-done.6.refs_1_, bf16[2,272,128]{2,1,0:T(8,128)(2,1)S(1)} %collective-permute-done.8.refs_2_, ...), custom_call_target="tpu_custom_call" | custom-call | tf_op jit(solution)/shard_map/early/pallas_call | solution.py:493
  (79 shorter events, 20.8 us)
Async XLA Ops:
  0.0 29.7 %collective-permute-start = (bf16[128,2048]{1,0:T(8,128)(2,1)}, bf16[128,2048]{1,0:T(8,128)(2,1)S(1)}, u32[]{:S(2)}, u32[]{:S(2)}) collective-permute-start(bf16[128,2048]{1,0:T(8,128)(2,1)} %refs_16_.1), channel_id=1, source_target_pairs={{0,8},{1,121},{2,10},{3,123},{4,12},{5,125},{6,14},{7,127},{8,16},... | collective-permute-start | bytes 1572872 | tf_op jit(solution)/shard_map/ppermute | solution.py:373
  29.7 16.4 %collective-permute-start.2 = (bf16[128,2048]{1,0:T(8,128)(2,1)S(1)}, bf16[128,2048]{1,0:T(8,128)(2,1)S(1)}, u32[]{:S(2)}, u32[]{:S(2)}) collective-permute-start(bf16[128,2048]{1,0:T(8,128)(2,1)S(1)} %collective-permute-done.refs_17_), channel_id=1, source_target_pairs={{0,8},{1,121},{2,10},{3,123},{4,12},{5,125},{6,14},{7,127},{8,16},... | collective-permute-start | bytes 1572872 | tf_op jit(solution)/shard_map/ppermute | solution.py:373
  46.1 9.3 %collective-permute-start.3 = (bf16[128,2048]{1,0:T(8,128)(2,1)S(1)}, bf16[128,2048]{1,0:T(8,128)(2,1)}, u32[]{:S(2)}, u32[]{:S(2)}) collective-permute-start(bf16[128,2048]{1,0:T(8,128)(2,1)S(1)} %collective-permute-done.2.refs_18_), channel_id=1, source_target_pairs={{0,8},{1,121},{2,10},{3,123},{4,12},{5,125},{6,14},{7,127},{8,16},... | collective-permute-start | bytes 1572872 | tf_op jit(solution)/shard_map/ppermute | solution.py:373
  55.4 22.5 %collective-permute-start.4 = (bf16[128,2048]{1,0:T(8,128)(2,1)}, bf16[128,2048]{1,0:T(8,128)(2,1)S(1)}, u32[]{:S(2)}, u32[]{:S(2)}) collective-permute-start(bf16[128,2048]{1,0:T(8,128)(2,1)} %collective-permute-done.3.refs_19_), channel_id=1, source_target_pairs={{0,8},{1,121},{2,10},{3,123},{4,12},{5,125},{6,14},{7,127},{8,16},... | collective-permute-start | bytes 1572872 | tf_op jit(solution)/shard_map/ppermute | solution.py:373
  58.5 15.4 %all-to-all-start = ((f32[16,8,256]{2,1,0:T(8,128)}), f32[16,8,256]{2,1,0:T(8,128)S(1)}, u32[]{:S(2)}, u32[]{:S(2)}) async-start(f32[16,8,256]{2,1,0:T(8,128)} %get-tuple-element.61), calls=%async_computation | async-start | bytes 262144 | tf_op jit(solution)/shard_map/all_to_all | solution.py:442
  78.0 12.2 %collective-permute-start.7 = (bf16[128,1024]{1,0:T(8,128)(2,1)S(1)}, bf16[128,1024]{1,0:T(8,128)(2,1)S(1)}, u32[]{:S(2)}, u32[]{:S(2)}) collective-permute-start(bf16[128,1024]{1,0:T(8,128)(2,1)S(1)} %get-tuple-element.98), channel_id=1, source_target_pairs={{0,8},{1,121},{2,10},{3,123},{4,12},{5,125},{6,14},{7,127},{8,16},... | collective-permute-start | bytes 786440 | tf_op jit(solution)/shard_map/ppermute | solution.py:373
  79.6 19.4 %collective-permute-start.20 = (bf16[128,2048]{1,0:T(8,128)(2,1)S(1)}, bf16[128,2048]{1,0:T(8,128)(2,1)S(1)}, u32[]{:S(2)}, u32[]{:S(2)}) collective-permute-start(bf16[128,2048]{1,0:T(8,128)(2,1)S(1)} %collective-permute-done.refs_17_), channel_id=1, source_target_pairs={{0,1},{1,0},{2,3},{3,2},{4,5},{5,4},{6,7},{7,6},{8,9},{9,8},{10,11... | collective-permute-start | bytes 1572872 | tf_op jit(solution)/shard_map/ppermute | solution.py:379
  89.7 12.9 %collective-permute-start.21 = (bf16[128,2048]{1,0:T(8,128)(2,1)S(1)}, bf16[128,2048]{1,0:T(8,128)(2,1)S(1)}, u32[]{:S(2)}, u32[]{:S(2)}) collective-permute-start(bf16[128,2048]{1,0:T(8,128)(2,1)S(1)} %collective-permute-done.2.refs_18_), channel_id=1, source_target_pairs={{0,1},{1,0},{2,3},{3,2},{4,5},{5,4},{6,7},{7,6},{8,9},{9,8},{10,11... | collective-permute-start | bytes 1572872 | tf_op jit(solution)/shard_map/ppermute | solution.py:379
  89.7 18.0 %collective-permute-start.22 = (bf16[128,2048]{1,0:T(8,128)(2,1)}, bf16[128,2048]{1,0:T(8,128)(2,1)S(1)}, u32[]{:S(2)}, u32[]{:S(2)}) collective-permute-start(bf16[128,2048]{1,0:T(8,128)(2,1)} %collective-permute-done.3.refs_19_), channel_id=1, source_target_pairs={{0,1},{1,0},{2,3},{3,2},{4,5},{5,4},{6,7},{7,6},{8,9},{9,8},{10,11... | collective-permute-start | bytes 1572872 | tf_op jit(solution)/shard_map/ppermute | solution.py:379
  93.5 8.4 %collective-permute-start.16 = (bf16[128,1024]{1,0:T(8,128)(2,1)S(1)}, bf16[128,1024]{1,0:T(8,128)(2,1)S(1)}, u32[]{:S(2)}, u32[]{:S(2)}) collective-permute-start(bf16[128,1024]{1,0:T(8,128)(2,1)S(1)} %collective-permute-done.15.refs_10_), channel_id=1, source_target_pairs={{0,8},{1,121},{2,10},{3,123},{4,12},{5,125},{6,14},{7,127},{8,16},... | collective-permute-start | bytes 786440 | tf_op jit(solution)/shard_map/ppermute | solution.py:373
  96.3 13.5 %collective-permute-start.13 = (bf16[128,1024]{1,0:T(8,128)(2,1)S(1)}, bf16[128,1024]{1,0:T(8,128)(2,1)S(1)}, u32[]{:S(2)}, u32[]{:S(2)}) collective-permute-start(bf16[128,1024]{1,0:T(8,128)(2,1)S(1)} %collective-permute-done.12.refs_11_), channel_id=1, source_target_pairs={{0,8},{1,121},{2,10},{3,123},{4,12},{5,125},{6,14},{7,127},{8,16},... | collective-permute-start | bytes 786440 | tf_op jit(solution)/shard_map/ppermute | solution.py:373
  99.0 9.3 %collective-permute-start.5 = (bf16[2,272,128]{2,1,0:T(8,128)(2,1)S(1)}, bf16[2,272,128]{2,1,0:T(8,128)(2,1)S(1)}, u32[]{:S(2)}, u32[]{:S(2)}) collective-permute-start(bf16[2,272,128]{2,1,0:T(8,128)(2,1)S(1)} %get-tuple-element.74), channel_id=1, source_target_pairs={{0,4},{1,5},{2,6},{3,7},{4,0},{5,1},{6,2},{7,3},{8,12},{9,13},{10,... | collective-permute-start | bytes 417800 | tf_op jit(solution)/shard_map/ppermute | solution.py:483
  102.0 17.1 %collective-permute-start.23 = (bf16[128,1024]{1,0:T(8,128)(2,1)S(1)}, bf16[128,1024]{1,0:T(8,128)(2,1)S(1)}, u32[]{:S(2)}, u32[]{:S(2)}) collective-permute-start(bf16[128,1024]{1,0:T(8,128)(2,1)S(1)} %collective-permute-done.16.refs_12_), channel_id=1, source_target_pairs={{0,8},{1,121},{2,10},{3,123},{4,12},{5,125},{6,14},{7,127},{8,16},... | collective-permute-start | bytes 786440 | tf_op jit(solution)/shard_map/ppermute | solution.py:373
  102.6 9.7 %collective-permute-start.6 = (bf16[2,272,128]{2,1,0:T(8,128)(2,1)}, bf16[2,272,128]{2,1,0:T(8,128)(2,1)S(1)}, u32[]{:S(2)}, u32[]{:S(2)}) collective-permute-start(bf16[2,272,128]{2,1,0:T(8,128)(2,1)} %get-tuple-element.75), channel_id=1, source_target_pairs={{0,5},{1,4},{2,7},{3,6},{4,1},{5,0},{6,3},{7,2},{8,13},{9,12},{10,... | collective-permute-start | bytes 417800 | tf_op jit(solution)/shard_map/ppermute | solution.py:483
  107.8 7.6 %collective-permute-start.8 = (bf16[2,272,128]{2,1,0:T(8,128)(2,1)}, bf16[2,272,128]{2,1,0:T(8,128)(2,1)S(1)}, u32[]{:S(2)}, u32[]{:S(2)}) collective-permute-start(bf16[2,272,128]{2,1,0:T(8,128)(2,1)} %get-tuple-element.83), channel_id=1, source_target_pairs={{0,2},{1,3},{2,4},{3,5},{4,6},{5,7},{6,0},{7,1},{8,10},{9,11},{10,... | collective-permute-start | bytes 417800 | tf_op jit(solution)/shard_map/ppermute | solution.py:483
  108.2 10.2 %collective-permute-start.9 = (bf16[2,272,128]{2,1,0:T(8,128)(2,1)}, bf16[2,272,128]{2,1,0:T(8,128)(2,1)S(1)}, u32[]{:S(2)}, u32[]{:S(2)}) collective-permute-start(bf16[2,272,128]{2,1,0:T(8,128)(2,1)} %get-tuple-element.84), channel_id=1, source_target_pairs={{0,3},{1,2},{2,5},{3,4},{4,7},{5,6},{6,1},{7,0},{8,11},{9,10},{10,... | collective-permute-start | bytes 417800 | tf_op jit(solution)/shard_map/ppermute | solution.py:483
  109.8 15.5 %collective-permute-start.17 = (bf16[128,2048]{1,0:T(8,128)(2,1)S(1)}, bf16[128,2048]{1,0:T(8,128)(2,1)S(1)}, u32[]{:S(2)}, u32[]{:S(2)}) collective-permute-start(bf16[128,2048]{1,0:T(8,128)(2,1)S(1)} %collective-permute-done.4.refs_8_), channel_id=1, source_target_pairs={{0,1},{1,0},{2,3},{3,2},{4,5},{5,4},{6,7},{7,6},{8,9},{9,8},{10,11... | collective-permute-start | bytes 1572872 | tf_op jit(solution)/shard_map/ppermute | solution.py:379
  112.2 12.6 %collective-permute-start.18 = (bf16[128,1024]{1,0:T(8,128)(2,1)S(1)}, bf16[128,1024]{1,0:T(8,128)(2,1)S(1)}, u32[]{:S(2)}, u32[]{:S(2)}) collective-permute-start(bf16[128,1024]{1,0:T(8,128)(2,1)S(1)} %collective-permute-done.7.refs_9_), channel_id=1, source_target_pairs={{0,1},{1,0},{2,3},{3,2},{4,5},{5,4},{6,7},{7,6},{8,9},{9,8},{10,11... | collective-permute-start | bytes 786440 | tf_op jit(solution)/shard_map/ppermute | solution.py:379
  120.4 6.1 %collective-permute-start.28 = (bf16[128,1024]{1,0:T(8,128)(2,1)S(1)}, bf16[128,1024]{1,0:T(8,128)(2,1)S(1)}, u32[]{:S(2)}, u32[]{:S(2)}) collective-permute-start(bf16[128,1024]{1,0:T(8,128)(2,1)S(1)} %broadcast_select_fusion), channel_id=1, source_target_pairs={{0,8},{1,121},{2,10},{3,123},{4,12},{5,125},{6,14},{7,127},{8,16},... | collective-permute-start | bytes 786440 | tf_op jit(solution)/shard_map/ppermute | solution.py:373
  124.9 8.5 %collective-permute-start.24 = (bf16[128,1024]{1,0:T(8,128)(2,1)S(1)}, bf16[128,1024]{1,0:T(8,128)(2,1)S(1)}, u32[]{:S(2)}, u32[]{:S(2)}) collective-permute-start(bf16[128,1024]{1,0:T(8,128)(2,1)S(1)} %collective-permute-done.12.refs_11_), channel_id=1, source_target_pairs={{0,1},{1,0},{2,3},{3,2},{4,5},{5,4},{6,7},{7,6},{8,9},{9,8},{10,11... | collective-permute-start | bytes 786440 | tf_op jit(solution)/shard_map/ppermute | solution.py:379
  125.0 8.4 %collective-permute-start.25 = (bf16[128,1024]{1,0:T(8,128)(2,1)S(1)}, bf16[128,1024]{1,0:T(8,128)(2,1)S(1)}, u32[]{:S(2)}, u32[]{:S(2)}) collective-permute-start(bf16[128,1024]{1,0:T(8,128)(2,1)S(1)} %collective-permute-done.16.refs_12_), channel_id=1, source_target_pairs={{0,1},{1,0},{2,3},{3,2},{4,5},{5,4},{6,7},{7,6},{8,9},{9,8},{10,11... | collective-permute-start | bytes 786440 | tf_op jit(solution)/shard_map/ppermute | solution.py:379
  125.4 8.0 %collective-permute-start.26 = (bf16[128,1024]{1,0:T(8,128)(2,1)S(1)}, bf16[128,1024]{1,0:T(8,128)(2,1)S(1)}, u32[]{:S(2)}, u32[]{:S(2)}) collective-permute-start(bf16[128,1024]{1,0:T(8,128)(2,1)S(1)} %collective-permute-done.13.refs_0_), channel_id=1, source_target_pairs={{0,1},{1,0},{2,3},{3,2},{4,5},{5,4},{6,7},{7,6},{8,9},{9,8},{10,11... | collective-permute-start | bytes 786440 | tf_op jit(solution)/shard_map/ppermute | solution.py:379
  125.8 7.6 %collective-permute-start.27 = (bf16[128,1024]{1,0:T(8,128)(2,1)S(1)}, bf16[128,1024]{1,0:T(8,128)(2,1)S(1)}, u32[]{:S(2)}, u32[]{:S(2)}) collective-permute-start(bf16[128,1024]{1,0:T(8,128)(2,1)S(1)} %collective-permute-done.23.refs_1_), channel_id=1, source_target_pairs={{0,1},{1,0},{2,3},{3,2},{4,5},{5,4},{6,7},{7,6},{8,9},{9,8},{10,11... | collective-permute-start | bytes 786440 | tf_op jit(solution)/shard_map/ppermute | solution.py:379
  126.6 7.6 %collective-permute-start.29 = (bf16[128,1024]{1,0:T(8,128)(2,1)S(1)}, bf16[128,1024]{1,0:T(8,128)(2,1)S(1)}, u32[]{:S(2)}, u32[]{:S(2)}) collective-permute-start(bf16[128,1024]{1,0:T(8,128)(2,1)S(1)} %collective-permute-done.28.near), channel_id=1, source_target_pairs={{0,1},{1,0},{2,3},{3,2},{4,5},{5,4},{6,7},{7,6},{8,9},{9,8},{10,11... | collective-permute-start | bytes 786440 | tf_op jit(solution)/shard_map/ppermute | solution.py:379
  (22 other events, 332.5 us)

commit v5 on v4

--- a/solution.py
+++ b/solution.py
@@ -14,7 +14,7 @@
 EXTRA = 16
 EPS = 1e-06
 STREAMS = 2
-EXCHANGE = (2, 1, 3, 0)
+EXCHANGE = (2, 1, 3)
 
 
 def on_chip(x):
@@ -209,12 +209,12 @@
     for k in range(blocks):
         for copy in leaving(k):
             copy.wait()
-    ends[...] = jnp.broadcast_to(carry[...][None], ends.shape)
+    ends[...] = jnp.broadcast_to(carry[0 : ends.shape[1], :][None], ends.shape)
 
 
 def gated_kernel(state, prod, gate, ends, gain, *refs, order):
     count = len(order)
-    parts, (incoming, states, prods, gates, sems) = refs[:count], refs[count:]
+    kept, given, incoming, states, prods, gates, sems = refs
     seat = lax.axis_index("tp")
     copies = []
     for k, (dx, dc) in enumerate(order):
@@ -238,7 +238,8 @@
 
     ones = jnp.ones((8, 128), BF16)
     over = (((1,), (1,)), ((), ()))
-    for k, part in enumerate(parts):
+    for k, (dx, dc) in enumerate(order):
+        part = (kept, given)[dc].at[dx]
         for copy in copies[k]:
             copy.wait()
         rows = slice(k * BLOCK, k * BLOCK + BLOCK)
@@ -287,21 +288,26 @@
     return jnp.dot(mixed, jnp.concatenate(weights, 0), preferred_element_type=F32)
 
 
-def early_kernel(*refs, order, here, away, sizes, spans):
-    count = len(order)
+def early_kernel(kept, given, *refs, dist, here, away, sizes, away_sizes, spans):
     out, arrived, held, sems = refs[-4:]
-    outside = refs[-4 - len(away) : -4]
-    depth = outside[0].shape[0]
-    copies = [
-        pltpu.make_async_copy(block, held.at[pl.ds(k * depth, depth), :], sems.at[k])
-        for k, block in enumerate(outside)
-    ]
+    outside = grouped(refs[-4 - sum(away_sizes) : -4], away_sizes)
+    depth = outside[0][0].shape[0]
+    copies = []
+    for k, parts in enumerate(outside):
+        for side, part in enumerate(parts):
+            width = part.shape[1]
+            into = held.at[pl.ds(k * depth, depth), pl.ds(side * width, width)]
+            copies.append(pltpu.make_async_copy(part, into, sems.at[len(copies)]))
     for copy in copies:
         copy.start()
     seat = lax.axis_index("tp")
-    for (dx, dc), part in zip(order, refs[:count]):
-        arrived[neighbour(seat, count // 2 - dx, dc, count // 2)] = part[...]
-    groups = grouped(refs[count:], sizes)
+    chips = arrived.shape[0] // 2
+    arrived[seat] = kept[0]
+    arrived[neighbour(seat, 0, 1, chips)] = given[0]
+    for dx, part in zip(dist, refs):
+        for side in range(2):
+            arrived[neighbour(seat, chips - dx, side, chips)] = part[side]
+    groups = grouped(refs[len(dist) :], sizes)
     places = places_of(here, spans)
     step = 512
     for low in range(0, out.shape[1], step):
@@ -414,7 +420,7 @@
     half_rows = rows // 2
 
     def recur(first, *extra):
-        many = 1 if first else spans
+        many = (1, 8, head) if first else (spans, 2, head)
         half_shape = (2, half_rows, head // 2)
         return pl.pallas_call(
             functools.partial(recur_kernel, first=first),
@@ -422,7 +428,7 @@
             out_specs=[hbm, hbm, fixed],
             out_shape=[
                 pltpu.HBM((2, rows, head // 2), F32), pltpu.HBM((2, rows, head // 2), F32),
-                jax.ShapeDtypeStruct((many, 8, head), F32),
+                jax.ShapeDtypeStruct(many, F32),
             ],
             scratch_shapes=[
                 pltpu.VMEM((BLOCK + 8, head), F32), pltpu.VMEM((2, BLOCK, head // 2), F32),
@@ -454,13 +460,15 @@
         compiler_params=limit(20),
         name="gate",
     )(in_hbm(late_tokens), gain_row, w_gate)
-    order = [(dx, dc) for dx in EXCHANGE for dc in range(2)]
+    (gate,) = advance([gate], STREAMS)
+    chips = heads // 2
+    order = [(dx, dc) for dc in (1, 0) for dx in range(chips)]
     part_shape = (2, BLOCK + EXTRA, head // 2)
-    parts = pl.pallas_call(
+    kept, given = pl.pallas_call(
         functools.partial(gated_kernel, order=order),
         in_specs=[hbm] * 3 + [fixed] * 2,
-        out_specs=[fixed] * heads,
-        out_shape=[pltpu.VMEM(part_shape, BF16)] * heads,
+        out_specs=[fixed] * 2,
+        out_shape=[pltpu.VMEM((chips, *part_shape), BF16)] * 2,
         scratch_shapes=[
             pltpu.VMEM((8, head), F32), pltpu.VMEM((2, rows, head // 2), F32),
             pltpu.VMEM((2, rows, head // 2), F32), pltpu.VMEM((rows, head), F32),
@@ -470,39 +478,35 @@
         name="gated",
     )(*map(in_hbm, (state, prod, gate)), all_ends, out_gain.reshape(1, head))
 
-    parts = advance(parts, STREAMS)
+    given = lax.ppermute(given, "tp", [(t, neighbour(t, 0, 1, chips)) for t in range(heads)])
+    (kept,) = advance([kept])
     moves = []
-    for k, (dx, dc) in enumerate(order):
-        if (dx, dc) == (1, 0):
-            parts = parts[:k] + advance(parts[k:])
-        if (dx, dc) == (0, 0):
-            parts = parts[:k] + advance(parts[k:])
-            moves.append(parts[k])
-            continue
-        to = lambda t: neighbour(t, dx, dc, heads // 2)
-        moves.append(lax.ppermute(parts[k], "tp", [(t, to(t)) for t in range(heads)]))
-    (moves[-2],) = advance([moves[-2]])
+    for dx in EXCHANGE:
+        both = jnp.stack([kept[dx], given[dx]])
+        moves.append(lax.ppermute(both, "tp", [(t, neighbour(t, dx, 0, chips)) for t in range(heads)]))
+    while len(moved) < reach:
+        (kept,) = advance([kept])
     across(moved[-1])
 
     flat = lambda groups: [on_chip(part) for parts in groups for part in parts]
     sizes_of = lambda groups: [len(parts) for parts in groups]
-    groups = moved[3:6] + swapped[3:5]
-    here = [-4, -5, -6, 4, 5]
-    outside = [w_out] + [parts[0] for parts in moved[:3] + swapped[:3]]
-    away = [0, -1, -2, -3, 1, 2, 3]
+    groups = moved[5:6] + swapped[3:5]
+    here = [-6, 4, 5]
+    outside = [[w_out]] + moved[:5] + swapped[:3]
+    away = [0, -1, -2, -3, -4, -5, 1, 2, 3]
+    away_sizes = sizes_of(outside)
     sums, arrived = pl.pallas_call(
         functools.partial(
-            early_kernel, order=order, here=here, away=away, sizes=sizes_of(groups), spans=spans
+            early_kernel, dist=EXCHANGE, here=here, away=away, sizes=sizes_of(groups),
+            away_sizes=away_sizes, spans=spans,
         ),
-        in_specs=[fixed] * (len(moves) + len(flat(groups))) + [hbm] * len(outside),
+        in_specs=[fixed] * (2 + len(moves) + len(flat(groups))) + [hbm] * sum(away_sizes),
         out_specs=[fixed] * 2,
         out_shape=[pltpu.VMEM((BLOCK, out_width), F32), pltpu.VMEM((heads, *part_shape), BF16)],
-        scratch_shapes=[
-            pltpu.VMEM((len(away) * depth, out_width), BF16), pltpu.SemaphoreType.DMA((len(away),)),
-        ],
+        scratch_shapes=[pltpu.VMEM((len(away) * depth, out_width), BF16), pltpu.SemaphoreType.DMA((sum(away_sizes),))],
         compiler_params=limit(20),
         name="early",
-    )(*map(on_chip, moves), *flat(groups), *map(in_hbm, outside))
+    )(*map(on_chip, (kept, given, *moves)), *flat(groups), *[in_hbm(part) for parts in outside for part in parts])
     groups = moved[6:7] + swapped[5:7]
     sums = pl.pallas_call(
         functools.partial(middle_kernel, offsets=[-7, 6, 7], sizes=sizes_of(groups), spans=spans),

time: 136 us -> 134 us (0.985)
  starting transfers between devices: 75.3 us -> 70.2 us
  waiting for transfers between devices: 26.3 us -> 28.4 us
    ppermute x11, starting transfers between devices: 44.5 us -> 39.4 us  [onward(): made.append(lax.ppermute(part, ('sp', 'tp'), around))]
    ppermute x11, waiting for transfers between devices: 9.14 us -> 13.6 us  [onward(): made.append(lax.ppermute(part, ('sp', 'tp'), around))]
    ppermute x7 -> x4, starting transfers between devices: 11.7 us -> 14.6 us  [the longest x1 8.77 us: body(): lax.ppermute(given, 'tp', [(t, neighbour(t, 0, 1, chips)) for t in range(...]
    ppermute x11, starting transfers between devices: 13.8 us -> 11 us  [across(): made.append(lax.ppermute(part, ('sp', 'tp'), swap))]
    ppermute x7 -> x4, waiting for transfers between devices: 9.84 us -> 8.1 us  [the longest x3 8.09 us: body(): lax.ppermute(both, 'tp', [(t, neighbour(t, dx, 0, chips)) for t in range(...]
  transfers between devices with their start and end apart: 31 -> 28, of which waited for: 12 -> 9; matrix products, arithmetic and copies ran while one was open for 1% -> 1% of each run, Pallas kernels for 23% -> 21%
where the time goes in v5:
time: 134 us; the launch traced here: 133 us
  starting transfers between devices  70.2 us (52%)
  Pallas kernels  32.6 us (24%)
  waiting for transfers between devices  28.4 us (21%)
  local copies, waits for them, and re-layouts  1.71 us (1%)
    ppermute x11, starting transfers between devices, onward(): made.append(lax.ppermute(part, ('sp', 'tp'), around))  39.4 us
    ppermute x11, waiting for transfers between devices, onward(): made.append(lax.ppermute(part, ('sp', 'tp'), around))  13.6 us
    ppermute x11, starting transfers between devices, across(): made.append(lax.ppermute(part, ('sp', 'tp'), swap))  11 us
    pallas_call x2, Pallas kernels, recur(): pl.pallas_call(functools.partial(recur_kernel, first=first), in_specs=[fi...  9.57 us
    ppermute x1, starting transfers between devices, body(): lax.ppermute(given, 'tp', [(t, neighbour(t, 0, 1, chips)) for t in range(...  8.77 us
    ppermute x3, waiting for transfers between devices, body(): lax.ppermute(both, 'tp', [(t, neighbour(t, dx, 0, chips)) for t in range(...  8.09 us
    pallas_call x1, Pallas kernels, body(): pl.pallas_call(input_kernel, in_specs=[hbm] * 3, out_specs=[fixed] * 2, o...  6.78 us
    pallas_call x1, Pallas kernels, body(): pl.pallas_call(gate_kernel, in_specs=[hbm, fixed, fixed], out_specs=hbm,...  6.06 us
  transfers between devices with their start and end apart: 28, of which 9 were waited for; matrix products, arithmetic and copies ran while one was open for 1% of the time, Pallas kernels for 21%

profile of v5, /device:TPU:33, one launch (start us, length us, event | category | flops | bytes accessed | tf_op | source)
XLA Modules:
  0.0 133.4 jit_solution(14585404844351998779)
XLA Ops:
  0.0 22.9 %collective-permute-start = (bf16[128,2048]{1,0:T(8,128)(2,1)}, bf16[128,2048]{1,0:T(8,128)(2,1)S(1)}, u32[]{:S(2)}, u32[]{:S(2)}) collective-permute-start(bf16[128,2048]{1,0:T(8,128)(2,1)} %refs_8_.1), channel_id=1, source_target_pairs={{0,8},{1,121},{2,10},{3,123},{4,12},{5,125},{6,14},{7,127},{8,16},... | collective-permute-start | bytes 1572872 | tf_op jit(solution)/shard_map/ppermute | solution.py:379
  22.9 6.8 %input.1 = (bf16[2048,256]{1,0:T(8,128)(2,1)S(1)}, bf16[2048,256]{1,0:T(8,128)(2,1)S(1)}) custom-call(bf16[2048,2048]{1,0:T(8,128)(2,1)} %tokens.2, f32[1,2048]{1,0:T(1,128)} %bitcast.3, bf16[2048,256]{1,0:T(8,128)(2,1)} %w_input.1), custom_call_target="tpu_custom_call" | custom-call | tf_op jit(solution)/shard_map/input/pallas_call | solution.py:407
  29.7 2.6 %collective-permute-start.2 = (bf16[128,2048]{1,0:T(8,128)(2,1)S(1)}, bf16[128,2048]{1,0:T(8,128)(2,1)S(1)}, u32[]{:S(2)}, u32[]{:S(2)}) collective-permute-start(bf16[128,2048]{1,0:T(8,128)(2,1)S(1)} %collective-permute-done.refs_9_), channel_id=1, source_target_pairs={{0,8},{1,121},{2,10},{3,123},{4,12},{5,125},{6,14},{7,127},{8,16},... | collective-permute-start | bytes 1572872 | tf_op jit(solution)/shard_map/ppermute | solution.py:379
  36.4 4.6 %recur.2 = (f32[2,2048,128]{2,1,0:T(8,128)}, f32[2,2048,128]{2,1,0:T(8,128)}, f32[1,8,256]{2,1,0:T(8,128)S(1)}) custom-call(bf16[2048,256]{1,0:T(8,128)(2,1)S(1)} %get-tuple-element.33.projected, f32[4,256]{1,0:T(4,128)S(1)} %copy-done.5, bf16[1,256,256]{2,1,0:T(8,128)(2,1)S(1)} %copy-done.1, bf16[1,256,256]{2,1,0:T(8,128)(2,1)S(1)} %copy-done.2, ...), custom_call_target="tpu_custom_call" | custom-call | tf_op jit(solution)/shard_map/recur/pallas_call | solution.py:425
  41.0 5.0 %recur.3 = (f32[2,2048,128]{2,1,0:T(8,128)}, f32[2,2048,128]{2,1,0:T(8,128)}, f32[16,2,256]{2,1,0:T(2,128)}) custom-call(bf16[2048,256]{1,0:T(8,128)(2,1)S(1)} %get-tuple-element.33.projected, f32[4,256]{1,0:T(4,128)S(1)} %copy-done.5, bf16[1,256,256]{2,1,0:T(8,128)(2,1)S(1)} %copy-done.1, ...), custom_call_target="tpu_custom_call", output_to_operand_aliasing={{0}: (7, {}), {1}: (8, {})} | custom-call | tf_op jit(solution)/shard_map/recur/pallas_call | solution.py:425
  46.1 3.0 %collective-permute-start.3 = (bf16[128,2048]{1,0:T(8,128)(2,1)S(1)}, bf16[128,2048]{1,0:T(8,128)(2,1)S(1)}, u32[]{:S(2)}, u32[]{:S(2)}) collective-permute-start(bf16[128,2048]{1,0:T(8,128)(2,1)S(1)} %collective-permute-done.2.refs_10_), channel_id=1, source_target_pairs={{0,8},{1,121},{2,10},{3,123},{4,12},{5,125},{6,14},{7,127},{8,16},... | collective-permute-start | bytes 1572872 | tf_op jit(solution)/shard_map/ppermute | solution.py:379
  49.1 6.2 %collective-permute-done.3.refs_11_ = bf16[128,2048]{1,0:T(8,128)(2,1)S(1)} collective-permute-done((bf16[128,2048]{1,0:T(8,128)(2,1)S(1)}, bf16[128,2048]{1,0:T(8,128)(2,1)S(1)}, u32[]{:S(2)}, u32[]{:S(2)}) %collective-permute-start.3) | collective-permute-done | bytes 524320 | tf_op jit(solution)/shard_map/ppermute | solution.py:379
  55.3 3.0 %collective-permute-start.4 = (bf16[128,2048]{1,0:T(8,128)(2,1)S(1)}, bf16[128,2048]{1,0:T(8,128)(2,1)S(1)}, u32[]{:S(2)}, u32[]{:S(2)}) collective-permute-start(bf16[128,2048]{1,0:T(8,128)(2,1)S(1)} %collective-permute-done.3.refs_11_), channel_id=1, source_target_pairs={{0,8},{1,121},{2,10},{3,123},{4,12},{5,125},{6,14},{7,127},{8,16},... | collective-permute-start | bytes 1572872 | tf_op jit(solution)/shard_map/ppermute | solution.py:379
  58.3 3.9 %all-to-all-start = ((f32[16,2,256]{2,1,0:T(2,128)}), f32[16,2,256]{2,1,0:T(2,128)S(1)}, u32[]{:S(2)}, u32[]{:S(2)}) async-start(f32[16,2,256]{2,1,0:T(2,128)} %get-tuple-element.42), calls=%async_computation | async-start | bytes 65536 | tf_op jit(solution)/shard_map/all_to_all | solution.py:448
  62.3 6.1 %gate.1 = f32[2048,256]{1,0:T(8,128)} custom-call(bf16[2048,2048]{1,0:T(8,128)(2,1)} %tokens.2, f32[1,2048]{1,0:T(1,128)S(1)} %bitcast.4, bf16[2048,256]{1,0:T(8,128)(2,1)S(1)} %copy-done), custom_call_target="tpu_custom_call" | custom-call | tf_op jit(solution)/shard_map/gate/pallas_call | solution.py:451
  68.4 4.8 %all-to-all-done.ends = f32[16,2,256]{2,1,0:T(2,128)S(1)} async-done(((f32[16,2,256]{2,1,0:T(2,128)}), f32[16,2,256]{2,1,0:T(2,128)S(1)}, u32[]{:S(2)}, u32[]{:S(2)}) %all-to-all-start) | async-done | bytes 32800 | tf_op jit(solution)/shard_map/all_to_all | solution.py:448
  73.2 3.5 %gated.1 = (bf16[4,2,272,128]{3,2,1,0:T(8,128)(2,1)S(1)}, bf16[4,2,272,128]{3,2,1,0:T(8,128)(2,1)S(1)}) custom-call(f32[2,2048,128]{2,1,0:T(8,128)} %get-tuple-element.38.state, f32[2,2048,128]{2,1,0:T(8,128)} %get-tuple-element.39.prod, f32[2048,256]{1,0:T(8,128)} %gate.1, f32[16,2,256]{2,1,0:T(2,128)S(1)} %all-to-all-done.ends, f32[1,256]{1,0:T(1,128)S(1)} %bitcast.7), custom_call_target="tpu_custom_call" | custom-call | tf_op jit(solution)/shard_map/gated/pallas_call | solution.py:467
  76.7 8.8 %collective-permute-start.8 = (bf16[4,2,272,128]{3,2,1,0:T(8,128)(2,1)S(1)}, bf16[4,2,272,128]{3,2,1,0:T(8,128)(2,1)S(1)}, u32[]{:S(2)}, u32[]{:S(2)}) collective-permute-start(bf16[4,2,272,128]{3,2,1,0:T(8,128)(2,1)S(1)} %get-tuple-element.55), channel_id=1, source_target_pairs={{0,1},{1,0},{2,3},{3,2},{4,5},{5,4},{6,7},{7,6},{8,9},{9,8},{10,11... | collective-permute-start | bytes 1671176 | tf_op jit(solution)/shard_map/ppermute | solution.py:481
  87.7 4.2 %collective-permute-done.5.refs_13_ = bf16[128,1024]{1,0:T(8,128)(2,1)} collective-permute-done((bf16[128,1024]{1,0:T(8,128)(2,1)S(1)}, bf16[128,1024]{1,0:T(8,128)(2,1)}, u32[]{:S(2)}, u32[]{:S(2)}) %collective-permute-start.5) | collective-permute-done | bytes 262176 | tf_op jit(solution)/shard_map/ppermute | solution.py:379
  94.6 2.2 %collective-permute-start.13 = (bf16[128,1024]{1,0:T(8,128)(2,1)}, bf16[128,1024]{1,0:T(8,128)(2,1)S(1)}, u32[]{:S(2)}, u32[]{:S(2)}) collective-permute-start(bf16[128,1024]{1,0:T(8,128)(2,1)} %collective-permute-done.12.refs_14_), channel_id=1, source_target_pairs={{0,8},{1,121},{2,10},{3,123},{4,12},{5,125},{6,14},{7,127},{8,16},... | collective-permute-start | bytes 786440 | tf_op jit(solution)/shard_map/ppermute | solution.py:379
  97.3 4.5 %collective-permute-start.19 = (bf16[128,2048]{1,0:T(8,128)(2,1)}, bf16[128,2048]{1,0:T(8,128)(2,1)S(1)}, u32[]{:S(2)}, u32[]{:S(2)}) collective-permute-start(bf16[128,2048]{1,0:T(8,128)(2,1)} %copy-done.11), channel_id=1, source_target_pairs={{0,1},{1,0},{2,3},{3,2},{4,5},{5,4},{6,7},{7,6},{8,9},{9,8},{10,11... | collective-permute-start | bytes 1572872 | tf_op jit(solution)/shard_map/ppermute | solution.py:385
  101.9 2.9 %collective-permute-start.20 = (bf16[128,1024]{1,0:T(8,128)(2,1)S(1)}, bf16[128,1024]{1,0:T(8,128)(2,1)S(1)}, u32[]{:S(2)}, u32[]{:S(2)}) collective-permute-start(bf16[128,1024]{1,0:T(8,128)(2,1)S(1)} %collective-permute-done.13.refs_4_), channel_id=1, source_target_pairs={{0,8},{1,121},{2,10},{3,123},{4,12},{5,125},{6,14},{7,127},{8,16},... | collective-permute-start | bytes 786440 | tf_op jit(solution)/shard_map/ppermute | solution.py:379
  105.1 2.1 %collective-permute-done.7.refs_0_ = bf16[128,1024]{1,0:T(8,128)(2,1)S(1)} collective-permute-done((bf16[128,1024]{1,0:T(8,128)(2,1)S(1)}, bf16[128,1024]{1,0:T(8,128)(2,1)S(1)}, u32[]{:S(2)}, u32[]{:S(2)}) %collective-permute-start.7) | collective-permute-done | bytes 262176 | tf_op jit(solution)/shard_map/ppermute | solution.py:379
  107.2 2.1 %collective-permute-start.16 = (bf16[128,1024]{1,0:T(8,128)(2,1)}, bf16[128,1024]{1,0:T(8,128)(2,1)S(1)}, u32[]{:S(2)}, u32[]{:S(2)}) collective-permute-start(bf16[128,1024]{1,0:T(8,128)(2,1)} %collective-permute-done.12.refs_14_), channel_id=1, source_target_pairs={{0,1},{1,0},{2,3},{3,2},{4,5},{5,4},{6,7},{7,6},{8,9},{9,8},{10,11... | collective-permute-start | bytes 786440 | tf_op jit(solution)/shard_map/ppermute | solution.py:385
  109.4 3.1 %collective-permute-start.9 = (bf16[2,2,272,128]{3,2,1,0:T(8,128)(2,1)S(1)}, bf16[2,2,272,128]{3,2,1,0:T(8,128)(2,1)S(1)}, u32[]{:S(2)}, u32[]{:S(2)}) collective-permute-start(bf16[2,2,272,128]{3,2,1,0:T(8,128)(2,1)S(1)} %pad_maximum_fusion), channel_id=1, source_target_pairs={{0,4},{1,5},{2,6},{3,7},{4,0},{5,1},{6,2},{7,3},{8,12},{9,13},{10,... | collective-permute-start | bytes 835592 | tf_op jit(solution)/shard_map/ppermute | solution.py:486
  113.0 2.2 %collective-permute-start.11 = (bf16[2,2,272,128]{3,2,1,0:T(8,128)(2,1)S(1)}, bf16[2,2,272,128]{3,2,1,0:T(8,128)(2,1)S(1)}, u32[]{:S(2)}, u32[]{:S(2)}) collective-permute-start(bf16[2,2,272,128]{3,2,1,0:T(8,128)(2,1)S(1)} %pad_maximum_fusion.2), channel_id=1, source_target_pairs={{0,6},{1,7},{2,0},{3,1},{4,2},{5,3},{6,4},{7,5},{8,14},{9,15},{10,... | collective-permute-start | bytes 835592 | tf_op jit(solution)/shard_map/ppermute | solution.py:486
  116.4 3.0 %collective-permute-done.9.refs_0_ = bf16[2,2,272,128]{3,2,1,0:T(8,128)(2,1)S(1)} collective-permute-done((bf16[2,2,272,128]{3,2,1,0:T(8,128)(2,1)S(1)}, bf16[2,2,272,128]{3,2,1,0:T(8,128)(2,1)S(1)}, u32[]{:S(2)}, u32[]{:S(2)}) %collective-permute-start.9) | collective-permute-done | bytes 278560 | tf_op jit(solution)/shard_map/ppermute | solution.py:486
  120.6 5.1 %collective-permute-done.10.refs_1_ = bf16[2,2,272,128]{3,2,1,0:T(8,128)(2,1)S(1)} collective-permute-done((bf16[2,2,272,128]{3,2,1,0:T(8,128)(2,1)S(1)}, bf16[2,2,272,128]{3,2,1,0:T(8,128)(2,1)S(1)}, u32[]{:S(2)}, u32[]{:S(2)}) %collective-permute-start.10) | collective-permute-done | bytes 278560 | tf_op jit(solution)/shard_map/ppermute | solution.py:486
  126.6 4.5 %early.1 = (f32[256,2048]{1,0:T(8,128)S(1)}, bf16[8,2,272,128]{3,2,1,0:T(8,128)(2,1)S(1)}) custom-call(bf16[4,2,272,128]{3,2,1,0:T(8,128)(2,1)S(1)} %get-tuple-element.54.kept, bf16[4,2,272,128]{3,2,1,0:T(8,128)(2,1)S(1)} %collective-permute-done.8.given, bf16[2,2,272,128]{3,2,1,0:T(8,128)(2,1)S(1)} %collective-permute-done.9.refs_0_, ...), custom_call_target="tpu_custom_call" | custom-call | tf_op jit(solution)/shard_map/early/pallas_call | solution.py:498
  (76 shorter events, 15.9 us)
Async XLA Ops:
  0.0 29.7 %collective-permute-start = (bf16[128,2048]{1,0:T(8,128)(2,1)}, bf16[128,2048]{1,0:T(8,128)(2,1)S(1)}, u32[]{:S(2)}, u32[]{:S(2)}) collective-permute-start(bf16[128,2048]{1,0:T(8,128)(2,1)} %refs_8_.1), channel_id=1, source_target_pairs={{0,8},{1,121},{2,10},{3,123},{4,12},{5,125},{6,14},{7,127},{8,16},... | collective-permute-start | bytes 1572872 | tf_op jit(solution)/shard_map/ppermute | solution.py:379
  29.7 16.3 %collective-permute-start.2 = (bf16[128,2048]{1,0:T(8,128)(2,1)S(1)}, bf16[128,2048]{1,0:T(8,128)(2,1)S(1)}, u32[]{:S(2)}, u32[]{:S(2)}) collective-permute-start(bf16[128,2048]{1,0:T(8,128)(2,1)S(1)} %collective-permute-done.refs_9_), channel_id=1, source_target_pairs={{0,8},{1,121},{2,10},{3,123},{4,12},{5,125},{6,14},{7,127},{8,16},... | collective-permute-start | bytes 1572872 | tf_op jit(solution)/shard_map/ppermute | solution.py:379
  46.1 9.2 %collective-permute-start.3 = (bf16[128,2048]{1,0:T(8,128)(2,1)S(1)}, bf16[128,2048]{1,0:T(8,128)(2,1)S(1)}, u32[]{:S(2)}, u32[]{:S(2)}) collective-permute-start(bf16[128,2048]{1,0:T(8,128)(2,1)S(1)} %collective-permute-done.2.refs_10_), channel_id=1, source_target_pairs={{0,8},{1,121},{2,10},{3,123},{4,12},{5,125},{6,14},{7,127},{8,16},... | collective-permute-start | bytes 1572872 | tf_op jit(solution)/shard_map/ppermute | solution.py:379
  55.3 13.1 %collective-permute-start.4 = (bf16[128,2048]{1,0:T(8,128)(2,1)S(1)}, bf16[128,2048]{1,0:T(8,128)(2,1)S(1)}, u32[]{:S(2)}, u32[]{:S(2)}) collective-permute-start(bf16[128,2048]{1,0:T(8,128)(2,1)S(1)} %collective-permute-done.3.refs_11_), channel_id=1, source_target_pairs={{0,8},{1,121},{2,10},{3,123},{4,12},{5,125},{6,14},{7,127},{8,16},... | collective-permute-start | bytes 1572872 | tf_op jit(solution)/shard_map/ppermute | solution.py:379
  58.3 14.9 %all-to-all-start = ((f32[16,2,256]{2,1,0:T(2,128)}), f32[16,2,256]{2,1,0:T(2,128)S(1)}, u32[]{:S(2)}, u32[]{:S(2)}) async-start(f32[16,2,256]{2,1,0:T(2,128)} %get-tuple-element.42), calls=%async_computation | async-start | bytes 65536 | tf_op jit(solution)/shard_map/all_to_all | solution.py:448
  76.7 25.0 %collective-permute-start.8 = (bf16[4,2,272,128]{3,2,1,0:T(8,128)(2,1)S(1)}, bf16[4,2,272,128]{3,2,1,0:T(8,128)(2,1)S(1)}, u32[]{:S(2)}, u32[]{:S(2)}) collective-permute-start(bf16[4,2,272,128]{3,2,1,0:T(8,128)(2,1)S(1)} %get-tuple-element.55), channel_id=1, source_target_pairs={{0,1},{1,0},{2,3},{3,2},{4,5},{5,4},{6,7},{7,6},{8,9},{9,8},{10,11... | collective-permute-start | bytes 1671176 | tf_op jit(solution)/shard_map/ppermute | solution.py:481
  86.2 5.6 %collective-permute-start.5 = (bf16[128,1024]{1,0:T(8,128)(2,1)S(1)}, bf16[128,1024]{1,0:T(8,128)(2,1)}, u32[]{:S(2)}, u32[]{:S(2)}) collective-permute-start(bf16[128,1024]{1,0:T(8,128)(2,1)S(1)} %get-tuple-element.66), channel_id=1, source_target_pairs={{0,8},{1,121},{2,10},{3,123},{4,12},{5,125},{6,14},{7,127},{8,16},... | collective-permute-start | bytes 786440 | tf_op jit(solution)/shard_map/ppermute | solution.py:379
  86.9 7.7 %collective-permute-start.12 = (bf16[128,1024]{1,0:T(8,128)(2,1)}, bf16[128,1024]{1,0:T(8,128)(2,1)}, u32[]{:S(2)}, u32[]{:S(2)}) collective-permute-start(bf16[128,1024]{1,0:T(8,128)(2,1)} %get-tuple-element.65), channel_id=1, source_target_pairs={{0,8},{1,121},{2,10},{3,123},{4,12},{5,125},{6,14},{7,127},{8,16},... | collective-permute-start | bytes 786440 | tf_op jit(solution)/shard_map/ppermute | solution.py:379
  87.1 14.6 %collective-permute-start.17 = (bf16[128,2048]{1,0:T(8,128)(2,1)S(1)}, bf16[128,2048]{1,0:T(8,128)(2,1)}, u32[]{:S(2)}, u32[]{:S(2)}) collective-permute-start(bf16[128,2048]{1,0:T(8,128)(2,1)S(1)} %collective-permute-done.refs_9_), channel_id=1, source_target_pairs={{0,1},{1,0},{2,3},{3,2},{4,5},{5,4},{6,7},{7,6},{8,9},{9,8},{10,11... | collective-permute-start | bytes 1572872 | tf_op jit(solution)/shard_map/ppermute | solution.py:385
  93.5 11.5 %collective-permute-start.18 = (bf16[128,2048]{1,0:T(8,128)(2,1)S(1)}, bf16[128,2048]{1,0:T(8,128)(2,1)S(1)}, u32[]{:S(2)}, u32[]{:S(2)}) collective-permute-start(bf16[128,2048]{1,0:T(8,128)(2,1)S(1)} %collective-permute-done.2.refs_10_), channel_id=1, source_target_pairs={{0,1},{1,0},{2,3},{3,2},{4,5},{5,4},{6,7},{7,6},{8,9},{9,8},{10,11... | collective-permute-start | bytes 1572872 | tf_op jit(solution)/shard_map/ppermute | solution.py:385
  94.6 7.3 %collective-permute-start.13 = (bf16[128,1024]{1,0:T(8,128)(2,1)}, bf16[128,1024]{1,0:T(8,128)(2,1)S(1)}, u32[]{:S(2)}, u32[]{:S(2)}) collective-permute-start(bf16[128,1024]{1,0:T(8,128)(2,1)} %collective-permute-done.12.refs_14_), channel_id=1, source_target_pairs={{0,8},{1,121},{2,10},{3,123},{4,12},{5,125},{6,14},{7,127},{8,16},... | collective-permute-start | bytes 786440 | tf_op jit(solution)/shard_map/ppermute | solution.py:379
  97.3 12.1 %collective-permute-start.19 = (bf16[128,2048]{1,0:T(8,128)(2,1)}, bf16[128,2048]{1,0:T(8,128)(2,1)S(1)}, u32[]{:S(2)}, u32[]{:S(2)}) collective-permute-start(bf16[128,2048]{1,0:T(8,128)(2,1)} %copy-done.11), channel_id=1, source_target_pairs={{0,1},{1,0},{2,3},{3,2},{4,5},{5,4},{6,7},{7,6},{8,9},{9,8},{10,11... | collective-permute-start | bytes 1572872 | tf_op jit(solution)/shard_map/ppermute | solution.py:385
  101.7 5.5 %collective-permute-start.7 = (bf16[128,1024]{1,0:T(8,128)(2,1)S(1)}, bf16[128,1024]{1,0:T(8,128)(2,1)S(1)}, u32[]{:S(2)}, u32[]{:S(2)}) collective-permute-start(bf16[128,1024]{1,0:T(8,128)(2,1)S(1)} %collective-permute-done.6.refs_3_), channel_id=1, source_target_pairs={{0,8},{1,121},{2,10},{3,123},{4,12},{5,125},{6,14},{7,127},{8,16},... | collective-permute-start | bytes 786440 | tf_op jit(solution)/shard_map/ppermute | solution.py:379
  101.8 10.7 %collective-permute-start.15 = (bf16[128,1024]{1,0:T(8,128)(2,1)}, bf16[128,1024]{1,0:T(8,128)(2,1)S(1)}, u32[]{:S(2)}, u32[]{:S(2)}) collective-permute-start(bf16[128,1024]{1,0:T(8,128)(2,1)} %collective-permute-done.5.refs_13_), channel_id=1, source_target_pairs={{0,1},{1,0},{2,3},{3,2},{4,5},{5,4},{6,7},{7,6},{8,9},{9,8},{10,11... | collective-permute-start | bytes 786440 | tf_op jit(solution)/shard_map/ppermute | solution.py:385
  101.9 11.0 %collective-permute-start.20 = (bf16[128,1024]{1,0:T(8,128)(2,1)S(1)}, bf16[128,1024]{1,0:T(8,128)(2,1)S(1)}, u32[]{:S(2)}, u32[]{:S(2)}) collective-permute-start(bf16[128,1024]{1,0:T(8,128)(2,1)S(1)} %collective-permute-done.13.refs_4_), channel_id=1, source_target_pairs={{0,8},{1,121},{2,10},{3,123},{4,12},{5,125},{6,14},{7,127},{8,16},... | collective-permute-start | bytes 786440 | tf_op jit(solution)/shard_map/ppermute | solution.py:379
  105.0 10.4 %collective-permute-start.14 = (bf16[128,2048]{1,0:T(8,128)(2,1)S(1)}, bf16[128,2048]{1,0:T(8,128)(2,1)S(1)}, u32[]{:S(2)}, u32[]{:S(2)}) collective-permute-start(bf16[128,2048]{1,0:T(8,128)(2,1)S(1)} %collective-permute-done.4.refs_12_), channel_id=1, source_target_pairs={{0,1},{1,0},{2,3},{3,2},{4,5},{5,4},{6,7},{7,6},{8,9},{9,8},{10,11... | collective-permute-start | bytes 1572872 | tf_op jit(solution)/shard_map/ppermute | solution.py:385
  107.2 8.0 %collective-permute-start.16 = (bf16[128,1024]{1,0:T(8,128)(2,1)}, bf16[128,1024]{1,0:T(8,128)(2,1)S(1)}, u32[]{:S(2)}, u32[]{:S(2)}) collective-permute-start(bf16[128,1024]{1,0:T(8,128)(2,1)} %collective-permute-done.12.refs_14_), channel_id=1, source_target_pairs={{0,1},{1,0},{2,3},{3,2},{4,5},{5,4},{6,7},{7,6},{8,9},{9,8},{10,11... | collective-permute-start | bytes 786440 | tf_op jit(solution)/shard_map/ppermute | solution.py:385
  109.4 10.0 %collective-permute-start.9 = (bf16[2,2,272,128]{3,2,1,0:T(8,128)(2,1)S(1)}, bf16[2,2,272,128]{3,2,1,0:T(8,128)(2,1)S(1)}, u32[]{:S(2)}, u32[]{:S(2)}) collective-permute-start(bf16[2,2,272,128]{3,2,1,0:T(8,128)(2,1)S(1)} %pad_maximum_fusion), channel_id=1, source_target_pairs={{0,4},{1,5},{2,6},{3,7},{4,0},{5,1},{6,2},{7,3},{8,12},{9,13},{10,... | collective-permute-start | bytes 835592 | tf_op jit(solution)/shard_map/ppermute | solution.py:486
  112.5 13.1 %collective-permute-start.10 = (bf16[2,2,272,128]{3,2,1,0:T(8,128)(2,1)S(1)}, bf16[2,2,272,128]{3,2,1,0:T(8,128)(2,1)S(1)}, u32[]{:S(2)}, u32[]{:S(2)}) collective-permute-start(bf16[2,2,272,128]{3,2,1,0:T(8,128)(2,1)S(1)} %pad_maximum_fusion.1), channel_id=1, source_target_pairs={{0,2},{1,3},{2,4},{3,5},{4,6},{5,7},{6,0},{7,1},{8,10},{9,11},{10,... | collective-permute-start | bytes 835592 | tf_op jit(solution)/shard_map/ppermute | solution.py:486
  113.0 13.1 %collective-permute-start.11 = (bf16[2,2,272,128]{3,2,1,0:T(8,128)(2,1)S(1)}, bf16[2,2,272,128]{3,2,1,0:T(8,128)(2,1)S(1)}, u32[]{:S(2)}, u32[]{:S(2)}) collective-permute-start(bf16[2,2,272,128]{3,2,1,0:T(8,128)(2,1)S(1)} %pad_maximum_fusion.2), channel_id=1, source_target_pairs={{0,6},{1,7},{2,0},{3,1},{4,2},{5,3},{6,4},{7,5},{8,14},{9,15},{10,... | collective-permute-start | bytes 835592 | tf_op jit(solution)/shard_map/ppermute | solution.py:486
  115.2 11.3 %collective-permute-start.25 = (bf16[128,1024]{1,0:T(8,128)(2,1)S(1)}, bf16[128,1024]{1,0:T(8,128)(2,1)S(1)}, u32[]{:S(2)}, u32[]{:S(2)}) collective-permute-start(bf16[128,1024]{1,0:T(8,128)(2,1)S(1)} %broadcast_select_fusion), channel_id=1, source_target_pairs={{0,8},{1,121},{2,10},{3,123},{4,12},{5,125},{6,14},{7,127},{8,16},... | collective-permute-start | bytes 786440 | tf_op jit(solution)/shard_map/ppermute | solution.py:379
  115.4 15.7 %collective-permute-start.21 = (bf16[128,1024]{1,0:T(8,128)(2,1)S(1)}, bf16[128,1024]{1,0:T(8,128)(2,1)S(1)}, u32[]{:S(2)}, u32[]{:S(2)}) collective-permute-start(bf16[128,1024]{1,0:T(8,128)(2,1)S(1)} %collective-permute-done.6.refs_3_), channel_id=1, source_target_pairs={{0,1},{1,0},{2,3},{3,2},{4,5},{5,4},{6,7},{7,6},{8,9},{9,8},{10,11... | collective-permute-start | bytes 786440 | tf_op jit(solution)/shard_map/ppermute | solution.py:385
  119.4 11.7 %collective-permute-start.22 = (bf16[128,1024]{1,0:T(8,128)(2,1)S(1)}, bf16[128,1024]{1,0:T(8,128)(2,1)S(1)}, u32[]{:S(2)}, u32[]{:S(2)}) collective-permute-start(bf16[128,1024]{1,0:T(8,128)(2,1)S(1)} %collective-permute-done.13.refs_4_), channel_id=1, source_target_pairs={{0,1},{1,0},{2,3},{3,2},{4,5},{5,4},{6,7},{7,6},{8,9},{9,8},{10,11... | collective-permute-start | bytes 786440 | tf_op jit(solution)/shard_map/ppermute | solution.py:385
  125.6 5.5 %collective-permute-start.23 = (bf16[128,1024]{1,0:T(8,128)(2,1)S(1)}, bf16[128,1024]{1,0:T(8,128)(2,1)S(1)}, u32[]{:S(2)}, u32[]{:S(2)}) collective-permute-start(bf16[128,1024]{1,0:T(8,128)(2,1)S(1)} %collective-permute-done.7.refs_0_), channel_id=1, source_target_pairs={{0,1},{1,0},{2,3},{3,2},{4,5},{5,4},{6,7},{7,6},{8,9},{9,8},{10,11... | collective-permute-start | bytes 786440 | tf_op jit(solution)/shard_map/ppermute | solution.py:385
  (18 other events, 338.0 us)

commit v6 on v5

--- a/solution.py
+++ b/solution.py
@@ -288,6 +288,12 @@
     return jnp.dot(mixed, jnp.concatenate(weights, 0), preferred_element_type=F32)
 
 
+def pack_kernel(kept, given, *packed, dist):
+    for dx, out in zip(dist, packed):
+        out[0] = kept[dx]
+        out[1] = given[dx]
+
+
 def early_kernel(kept, given, *refs, dist, here, away, sizes, away_sizes, spans):
     out, arrived, held, sems = refs[-4:]
     outside = grouped(refs[-4 - sum(away_sizes) : -4], away_sizes)
@@ -480,9 +486,16 @@
 
     given = lax.ppermute(given, "tp", [(t, neighbour(t, 0, 1, chips)) for t in range(heads)])
     (kept,) = advance([kept])
+    packed = pl.pallas_call(
+        functools.partial(pack_kernel, dist=EXCHANGE),
+        in_specs=[fixed] * 2,
+        out_specs=[fixed] * len(EXCHANGE),
+        out_shape=[pltpu.VMEM((2, *part_shape), BF16)] * len(EXCHANGE),
+        compiler_params=limit(12),
+        name="pack",
+    )(on_chip(kept), on_chip(given))
     moves = []
-    for dx in EXCHANGE:
-        both = jnp.stack([kept[dx], given[dx]])
+    for dx, both in zip(EXCHANGE, packed):
         moves.append(lax.ppermute(both, "tp", [(t, neighbour(t, dx, 0, chips)) for t in range(heads)]))
     while len(moved) < reach:
         (kept,) = advance([kept])

time: 134 us -> 140 us (1.045)
  starting transfers between devices: 70.2 us -> 88.8 us
  waiting for transfers between devices: 28.4 us -> 15.5 us
    ppermute x11, starting transfers between devices: 11 us -> 24 us  [across(): made.append(lax.ppermute(part, ('sp', 'tp'), swap))]
    ppermute x11, waiting for transfers between devices: 13.6 us -> 6.69 us  [onward(): made.append(lax.ppermute(part, ('sp', 'tp'), around))]
    ppermute x11, starting transfers between devices: 39.4 us -> 44.4 us  [onward(): made.append(lax.ppermute(part, ('sp', 'tp'), around))]
    all_to_all x1, waiting for transfers between devices: 4.82 us -> 0.01 us  [body(): lax.all_to_all(ends, 'sp', split_axis=0, concat_axis=0, tiled=True)]
  transfers between devices with their start and end apart: 28 -> 28, of which waited for: 9 -> 5; matrix products, arithmetic and copies ran while one was open for 1% -> 1% of each run, Pallas kernels for 21% -> 22%
where the time goes in v6:
time: 140 us
  starting transfers between devices  88.8 us (63%)
  Pallas kernels  32.6 us (23%)
  waiting for transfers between devices  15.5 us (11%)
  local copies, waits for them, and re-layouts  2.6 us (2%)
    ppermute x11, starting transfers between devices, onward(): made.append(lax.ppermute(part, ('sp', 'tp'), around))  44.4 us
    ppermute x11, starting transfers between devices, across(): made.append(lax.ppermute(part, ('sp', 'tp'), swap))  24 us
    pallas_call x2, Pallas kernels, recur(): pl.pallas_call(functools.partial(recur_kernel, first=first), in_specs=[fi...  9.53 us
    ppermute x1, starting transfers between devices, body(): lax.ppermute(given, 'tp', [(t, neighbour(t, 0, 1, chips)) for t in range(...  9.33 us
    ppermute x3, waiting for transfers between devices, body(): lax.ppermute(both, 'tp', [(t, neighbour(t, dx, 0, chips)) for t in range(...  6.87 us
    pallas_call x1, Pallas kernels, body(): pl.pallas_call(input_kernel, in_specs=[hbm] * 3, out_specs=[fixed] * 2, o...  6.78 us
    ppermute x11, waiting for transfers between devices, onward(): made.append(lax.ppermute(part, ('sp', 'tp'), around))  6.69 us
    pallas_call x1, Pallas kernels, body(): pl.pallas_call(gate_kernel, in_specs=[hbm, fixed, fixed], out_specs=hbm,...  6.07 us
  transfers between devices with their start and end apart: 28, of which 5 were waited for; matrix products, arithmetic and copies ran while one was open for 1% of the time, Pallas kernels for 22%

profile of v6, /device:TPU:33, one launch (start us, length us, event | category | flops | bytes accessed | tf_op | source)
XLA Modules:
  0.0 139.8 jit_solution(10886767597659609642)
XLA Ops:
  0.0 22.9 %collective-permute-start = (bf16[128,2048]{1,0:T(8,128)(2,1)}, bf16[128,2048]{1,0:T(8,128)(2,1)S(1)}, u32[]{:S(2)}, u32[]{:S(2)}) collective-permute-start(bf16[128,2048]{1,0:T(8,128)(2,1)} %refs_8_.1), channel_id=1, source_target_pairs={{0,8},{1,121},{2,10},{3,123},{4,12},{5,125},{6,14},{7,127},{8,16},... | collective-permute-start | bytes 1572872 | tf_op jit(solution)/shard_map/ppermute | solution.py:385
  22.9 6.8 %input.1 = (bf16[2048,256]{1,0:T(8,128)(2,1)S(1)}, bf16[2048,256]{1,0:T(8,128)(2,1)S(1)}) custom-call(bf16[2048,2048]{1,0:T(8,128)(2,1)} %tokens.2, f32[1,2048]{1,0:T(1,128)} %bitcast.3, bf16[2048,256]{1,0:T(8,128)(2,1)} %w_input.1), custom_call_target="tpu_custom_call" | custom-call | tf_op jit(solution)/shard_map/input/pallas_call | solution.py:413
  29.7 2.6 %collective-permute-start.2 = (bf16[128,2048]{1,0:T(8,128)(2,1)S(1)}, bf16[128,2048]{1,0:T(8,128)(2,1)S(1)}, u32[]{:S(2)}, u32[]{:S(2)}) collective-permute-start(bf16[128,2048]{1,0:T(8,128)(2,1)S(1)} %collective-permute-done.refs_9_), channel_id=1, source_target_pairs={{0,8},{1,121},{2,10},{3,123},{4,12},{5,125},{6,14},{7,127},{8,16},... | collective-permute-start | bytes 1572872 | tf_op jit(solution)/shard_map/ppermute | solution.py:385
  36.4 4.6 %recur.2 = (f32[2,2048,128]{2,1,0:T(8,128)}, f32[2,2048,128]{2,1,0:T(8,128)}, f32[1,8,256]{2,1,0:T(8,128)S(1)}) custom-call(bf16[2048,256]{1,0:T(8,128)(2,1)S(1)} %get-tuple-element.36.projected, f32[4,256]{1,0:T(4,128)S(1)} %copy-done.5, bf16[1,256,256]{2,1,0:T(8,128)(2,1)S(1)} %copy-done.1, bf16[1,256,256]{2,1,0:T(8,128)(2,1)S(1)} %copy-done.2, ...), custom_call_target="tpu_custom_call" | custom-call | tf_op jit(solution)/shard_map/recur/pallas_call | solution.py:431
  41.1 4.9 %recur.3 = (f32[2,2048,128]{2,1,0:T(8,128)}, f32[2,2048,128]{2,1,0:T(8,128)}, f32[16,2,256]{2,1,0:T(2,128)}) custom-call(bf16[2048,256]{1,0:T(8,128)(2,1)S(1)} %get-tuple-element.36.projected, f32[4,256]{1,0:T(4,128)S(1)} %copy-done.5, bf16[1,256,256]{2,1,0:T(8,128)(2,1)S(1)} %copy-done.1, ...), custom_call_target="tpu_custom_call", output_to_operand_aliasing={{0}: (7, {}), {1}: (8, {})} | custom-call | tf_op jit(solution)/shard_map/recur/pallas_call | solution.py:431
  46.0 3.0 %collective-permute-start.3 = (bf16[128,2048]{1,0:T(8,128)(2,1)S(1)}, bf16[128,2048]{1,0:T(8,128)(2,1)}, u32[]{:S(2)}, u32[]{:S(2)}) collective-permute-start(bf16[128,2048]{1,0:T(8,128)(2,1)S(1)} %collective-permute-done.2.refs_10_), channel_id=1, source_target_pairs={{0,8},{1,121},{2,10},{3,123},{4,12},{5,125},{6,14},{7,127},{8,16},... | collective-permute-start | bytes 1572872 | tf_op jit(solution)/shard_map/ppermute | solution.py:385
  49.0 6.3 %collective-permute-done.3.refs_11_ = bf16[128,2048]{1,0:T(8,128)(2,1)} collective-permute-done((bf16[128,2048]{1,0:T(8,128)(2,1)S(1)}, bf16[128,2048]{1,0:T(8,128)(2,1)}, u32[]{:S(2)}, u32[]{:S(2)}) %collective-permute-start.3) | collective-permute-done | bytes 524320 | tf_op jit(solution)/shard_map/ppermute | solution.py:385
  55.3 3.0 %collective-permute-start.4 = (bf16[128,2048]{1,0:T(8,128)(2,1)}, bf16[128,2048]{1,0:T(8,128)(2,1)}, u32[]{:S(2)}, u32[]{:S(2)}) collective-permute-start(bf16[128,2048]{1,0:T(8,128)(2,1)} %collective-permute-done.3.refs_11_), channel_id=1, source_target_pairs={{0,8},{1,121},{2,10},{3,123},{4,12},{5,125},{6,14},{7,127},{8,16},... | collective-permute-start | bytes 1572872 | tf_op jit(solution)/shard_map/ppermute | solution.py:385
  58.4 6.1 %gate.1 = f32[2048,256]{1,0:T(8,128)} custom-call(bf16[2048,2048]{1,0:T(8,128)(2,1)} %tokens.2, f32[1,2048]{1,0:T(1,128)S(1)} %bitcast.4, bf16[2048,256]{1,0:T(8,128)(2,1)S(1)} %copy-done), custom_call_target="tpu_custom_call" | custom-call | tf_op jit(solution)/shard_map/gate/pallas_call | solution.py:457
  65.9 3.2 %collective-permute-start.5 = (bf16[128,1024]{1,0:T(8,128)(2,1)S(1)}, bf16[128,1024]{1,0:T(8,128)(2,1)S(1)}, u32[]{:S(2)}, u32[]{:S(2)}) collective-permute-start(bf16[128,1024]{1,0:T(8,128)(2,1)S(1)} %get-tuple-element.66), channel_id=1, source_target_pairs={{0,8},{1,121},{2,10},{3,123},{4,12},{5,125},{6,14},{7,127},{8,16},... | collective-permute-start | bytes 786440 | tf_op jit(solution)/shard_map/ppermute | solution.py:385
  69.1 3.9 %all-to-all-start = ((f32[16,2,256]{2,1,0:T(2,128)}), f32[16,2,256]{2,1,0:T(2,128)S(1)}, u32[]{:S(2)}, u32[]{:S(2)}) async-start(f32[16,2,256]{2,1,0:T(2,128)} %get-tuple-element.45), calls=%async_computation | async-start | bytes 65536 | tf_op jit(solution)/shard_map/all_to_all | solution.py:454
  73.1 8.4 %collective-permute-start.17 = (bf16[128,2048]{1,0:T(8,128)(2,1)S(1)}, bf16[128,2048]{1,0:T(8,128)(2,1)S(1)}, u32[]{:S(2)}, u32[]{:S(2)}) collective-permute-start(bf16[128,2048]{1,0:T(8,128)(2,1)S(1)} %collective-permute-done.refs_9_), channel_id=1, source_target_pairs={{0,1},{1,0},{2,3},{3,2},{4,5},{5,4},{6,7},{7,6},{8,9},{9,8},{10,11... | collective-permute-start | bytes 1572872 | tf_op jit(solution)/shard_map/ppermute | solution.py:391
  81.7 2.7 %collective-permute-start.12 = (bf16[128,1024]{1,0:T(8,128)(2,1)S(1)}, bf16[128,1024]{1,0:T(8,128)(2,1)}, u32[]{:S(2)}, u32[]{:S(2)}) collective-permute-start(bf16[128,1024]{1,0:T(8,128)(2,1)S(1)} %get-tuple-element.65), channel_id=1, source_target_pairs={{0,8},{1,121},{2,10},{3,123},{4,12},{5,125},{6,14},{7,127},{8,16},... | collective-permute-start | bytes 786440 | tf_op jit(solution)/shard_map/ppermute | solution.py:385
  84.3 3.5 %gated.1 = (bf16[4,2,272,128]{3,2,1,0:T(8,128)(2,1)S(1)}, bf16[4,2,272,128]{3,2,1,0:T(8,128)(2,1)S(1)}) custom-call(f32[2,2048,128]{2,1,0:T(8,128)} %get-tuple-element.41.state, f32[2,2048,128]{2,1,0:T(8,128)} %get-tuple-element.42.prod, f32[2048,256]{1,0:T(8,128)} %gate.1, f32[16,2,256]{2,1,0:T(2,128)S(1)} %all-to-all-done.ends, f32[1,256]{1,0:T(1,128)S(1)} %bitcast.7), custom_call_target="tpu_custom_call" | custom-call | tf_op jit(solution)/shard_map/gated/pallas_call | solution.py:473
  89.2 9.3 %collective-permute-start.8 = (bf16[4,2,272,128]{3,2,1,0:T(8,128)(2,1)S(1)}, bf16[4,2,272,128]{3,2,1,0:T(8,128)(2,1)S(1)}, u32[]{:S(2)}, u32[]{:S(2)}) collective-permute-start(bf16[4,2,272,128]{3,2,1,0:T(8,128)(2,1)S(1)} %get-tuple-element.58), channel_id=1, source_target_pairs={{0,1},{1,0},{2,3},{3,2},{4,5},{5,4},{6,7},{7,6},{8,9},{9,8},{10,11... | collective-permute-start | bytes 1671176 | tf_op jit(solution)/shard_map/ppermute | solution.py:487
  98.5 2.1 %collective-permute-start.13 = (bf16[128,1024]{1,0:T(8,128)(2,1)}, bf16[128,1024]{1,0:T(8,128)(2,1)S(1)}, u32[]{:S(2)}, u32[]{:S(2)}) collective-permute-start(bf16[128,1024]{1,0:T(8,128)(2,1)} %collective-permute-done.12.refs_14_), channel_id=1, source_target_pairs={{0,8},{1,121},{2,10},{3,123},{4,12},{5,125},{6,14},{7,127},{8,16},... | collective-permute-start | bytes 786440 | tf_op jit(solution)/shard_map/ppermute | solution.py:385
  101.4 4.5 %collective-permute-start.15 = (bf16[128,1024]{1,0:T(8,128)(2,1)S(1)}, bf16[128,1024]{1,0:T(8,128)(2,1)S(1)}, u32[]{:S(2)}, u32[]{:S(2)}) collective-permute-start(bf16[128,1024]{1,0:T(8,128)(2,1)S(1)} %collective-permute-done.5.refs_13_), channel_id=1, source_target_pairs={{0,1},{1,0},{2,3},{3,2},{4,5},{5,4},{6,7},{7,6},{8,9},{9,8},{10,11... | collective-permute-start | bytes 786440 | tf_op jit(solution)/shard_map/ppermute | solution.py:391
  105.9 3.0 %collective-permute-start.20 = (bf16[128,1024]{1,0:T(8,128)(2,1)S(1)}, bf16[128,1024]{1,0:T(8,128)(2,1)S(1)}, u32[]{:S(2)}, u32[]{:S(2)}) collective-permute-start(bf16[128,1024]{1,0:T(8,128)(2,1)S(1)} %collective-permute-done.13.refs_4_), channel_id=1, source_target_pairs={{0,8},{1,121},{2,10},{3,123},{4,12},{5,125},{6,14},{7,127},{8,16},... | collective-permute-start | bytes 786440 | tf_op jit(solution)/shard_map/ppermute | solution.py:385
  108.9 4.0 %collective-permute-start.14 = (bf16[128,2048]{1,0:T(8,128)(2,1)}, bf16[128,2048]{1,0:T(8,128)(2,1)S(1)}, u32[]{:S(2)}, u32[]{:S(2)}) collective-permute-start(bf16[128,2048]{1,0:T(8,128)(2,1)} %collective-permute-done.4.refs_12_), channel_id=1, source_target_pairs={{0,1},{1,0},{2,3},{3,2},{4,5},{5,4},{6,7},{7,6},{8,9},{9,8},{10,11... | collective-permute-start | bytes 1572872 | tf_op jit(solution)/shard_map/ppermute | solution.py:391
  112.9 2.8 %collective-permute-start.16 = (bf16[128,1024]{1,0:T(8,128)(2,1)}, bf16[128,1024]{1,0:T(8,128)(2,1)S(1)}, u32[]{:S(2)}, u32[]{:S(2)}) collective-permute-start(bf16[128,1024]{1,0:T(8,128)(2,1)} %collective-permute-done.12.refs_14_), channel_id=1, source_target_pairs={{0,1},{1,0},{2,3},{3,2},{4,5},{5,4},{6,7},{7,6},{8,9},{9,8},{10,11... | collective-permute-start | bytes 786440 | tf_op jit(solution)/shard_map/ppermute | solution.py:391
  115.8 3.1 %collective-permute-start.9 = (bf16[2,2,272,128]{3,2,1,0:T(8,128)(2,1)S(1)}, bf16[2,2,272,128]{3,2,1,0:T(8,128)(2,1)S(1)}, u32[]{:S(2)}, u32[]{:S(2)}) collective-permute-start(bf16[2,2,272,128]{3,2,1,0:T(8,128)(2,1)S(1)} %get-tuple-element.59), channel_id=1, source_target_pairs={{0,4},{1,5},{2,6},{3,7},{4,0},{5,1},{6,2},{7,3},{8,12},{9,13},{10,... | collective-permute-start | bytes 835592 | tf_op jit(solution)/shard_map/ppermute | solution.py:499
  119.3 2.2 %collective-permute-start.11 = (bf16[2,2,272,128]{3,2,1,0:T(8,128)(2,1)S(1)}, bf16[2,2,272,128]{3,2,1,0:T(8,128)(2,1)S(1)}, u32[]{:S(2)}, u32[]{:S(2)}) collective-permute-start(bf16[2,2,272,128]{3,2,1,0:T(8,128)(2,1)S(1)} %get-tuple-element.61), channel_id=1, source_target_pairs={{0,6},{1,7},{2,0},{3,1},{4,2},{5,3},{6,4},{7,5},{8,14},{9,15},{10,... | collective-permute-start | bytes 835592 | tf_op jit(solution)/shard_map/ppermute | solution.py:499
  127.0 5.1 %collective-permute-done.10.refs_1_ = bf16[2,2,272,128]{3,2,1,0:T(8,128)(2,1)S(1)} collective-permute-done((bf16[2,2,272,128]{3,2,1,0:T(8,128)(2,1)S(1)}, bf16[2,2,272,128]{3,2,1,0:T(8,128)(2,1)S(1)}, u32[]{:S(2)}, u32[]{:S(2)}) %collective-permute-start.10) | collective-permute-done | bytes 278560 | tf_op jit(solution)/shard_map/ppermute | solution.py:499
  133.0 4.5 %early.1 = (f32[256,2048]{1,0:T(8,128)S(1)}, bf16[8,2,272,128]{3,2,1,0:T(8,128)(2,1)S(1)}) custom-call(bf16[4,2,272,128]{3,2,1,0:T(8,128)(2,1)S(1)} %get-tuple-element.57.kept, bf16[4,2,272,128]{3,2,1,0:T(8,128)(2,1)S(1)} %collective-permute-done.8.given, bf16[2,2,272,128]{3,2,1,0:T(8,128)(2,1)S(1)} %collective-permute-done.9.refs_0_, ...), custom_call_target="tpu_custom_call" | custom-call | tf_op jit(solution)/shard_map/early/pallas_call | solution.py:511
  (68 shorter events, 16.9 us)
Async XLA Ops:
  0.0 29.7 %collective-permute-start = (bf16[128,2048]{1,0:T(8,128)(2,1)}, bf16[128,2048]{1,0:T(8,128)(2,1)S(1)}, u32[]{:S(2)}, u32[]{:S(2)}) collective-permute-start(bf16[128,2048]{1,0:T(8,128)(2,1)} %refs_8_.1), channel_id=1, source_target_pairs={{0,8},{1,121},{2,10},{3,123},{4,12},{5,125},{6,14},{7,127},{8,16},... | collective-permute-start | bytes 1572872 | tf_op jit(solution)/shard_map/ppermute | solution.py:385
  29.7 16.3 %collective-permute-start.2 = (bf16[128,2048]{1,0:T(8,128)(2,1)S(1)}, bf16[128,2048]{1,0:T(8,128)(2,1)S(1)}, u32[]{:S(2)}, u32[]{:S(2)}) collective-permute-start(bf16[128,2048]{1,0:T(8,128)(2,1)S(1)} %collective-permute-done.refs_9_), channel_id=1, source_target_pairs={{0,8},{1,121},{2,10},{3,123},{4,12},{5,125},{6,14},{7,127},{8,16},... | collective-permute-start | bytes 1572872 | tf_op jit(solution)/shard_map/ppermute | solution.py:385
  46.0 9.3 %collective-permute-start.3 = (bf16[128,2048]{1,0:T(8,128)(2,1)S(1)}, bf16[128,2048]{1,0:T(8,128)(2,1)}, u32[]{:S(2)}, u32[]{:S(2)}) collective-permute-start(bf16[128,2048]{1,0:T(8,128)(2,1)S(1)} %collective-permute-done.2.refs_10_), channel_id=1, source_target_pairs={{0,8},{1,121},{2,10},{3,123},{4,12},{5,125},{6,14},{7,127},{8,16},... | collective-permute-start | bytes 1572872 | tf_op jit(solution)/shard_map/ppermute | solution.py:385
  55.3 9.5 %collective-permute-start.4 = (bf16[128,2048]{1,0:T(8,128)(2,1)}, bf16[128,2048]{1,0:T(8,128)(2,1)}, u32[]{:S(2)}, u32[]{:S(2)}) collective-permute-start(bf16[128,2048]{1,0:T(8,128)(2,1)} %collective-permute-done.3.refs_11_), channel_id=1, source_target_pairs={{0,8},{1,121},{2,10},{3,123},{4,12},{5,125},{6,14},{7,127},{8,16},... | collective-permute-start | bytes 1572872 | tf_op jit(solution)/shard_map/ppermute | solution.py:385
  65.9 21.9 %collective-permute-start.5 = (bf16[128,1024]{1,0:T(8,128)(2,1)S(1)}, bf16[128,1024]{1,0:T(8,128)(2,1)S(1)}, u32[]{:S(2)}, u32[]{:S(2)}) collective-permute-start(bf16[128,1024]{1,0:T(8,128)(2,1)S(1)} %get-tuple-element.66), channel_id=1, source_target_pairs={{0,8},{1,121},{2,10},{3,123},{4,12},{5,125},{6,14},{7,127},{8,16},... | collective-permute-start | bytes 786440 | tf_op jit(solution)/shard_map/ppermute | solution.py:385
  69.1 15.2 %all-to-all-start = ((f32[16,2,256]{2,1,0:T(2,128)}), f32[16,2,256]{2,1,0:T(2,128)S(1)}, u32[]{:S(2)}, u32[]{:S(2)}) async-start(f32[16,2,256]{2,1,0:T(2,128)} %get-tuple-element.45), calls=%async_computation | async-start | bytes 65536 | tf_op jit(solution)/shard_map/all_to_all | solution.py:454
  73.1 27.5 %collective-permute-start.17 = (bf16[128,2048]{1,0:T(8,128)(2,1)S(1)}, bf16[128,2048]{1,0:T(8,128)(2,1)S(1)}, u32[]{:S(2)}, u32[]{:S(2)}) collective-permute-start(bf16[128,2048]{1,0:T(8,128)(2,1)S(1)} %collective-permute-done.refs_9_), channel_id=1, source_target_pairs={{0,1},{1,0},{2,3},{3,2},{4,5},{5,4},{6,7},{7,6},{8,9},{9,8},{10,11... | collective-permute-start | bytes 1572872 | tf_op jit(solution)/shard_map/ppermute | solution.py:391
  81.5 19.9 %collective-permute-start.18 = (bf16[128,2048]{1,0:T(8,128)(2,1)S(1)}, bf16[128,2048]{1,0:T(8,128)(2,1)}, u32[]{:S(2)}, u32[]{:S(2)}) collective-permute-start(bf16[128,2048]{1,0:T(8,128)(2,1)S(1)} %collective-permute-done.2.refs_10_), channel_id=1, source_target_pairs={{0,1},{1,0},{2,3},{3,2},{4,5},{5,4},{6,7},{7,6},{8,9},{9,8},{10,11... | collective-permute-start | bytes 1572872 | tf_op jit(solution)/shard_map/ppermute | solution.py:391
  81.7 16.8 %collective-permute-start.12 = (bf16[128,1024]{1,0:T(8,128)(2,1)S(1)}, bf16[128,1024]{1,0:T(8,128)(2,1)}, u32[]{:S(2)}, u32[]{:S(2)}) collective-permute-start(bf16[128,1024]{1,0:T(8,128)(2,1)S(1)} %get-tuple-element.65), channel_id=1, source_target_pairs={{0,8},{1,121},{2,10},{3,123},{4,12},{5,125},{6,14},{7,127},{8,16},... | collective-permute-start | bytes 786440 | tf_op jit(solution)/shard_map/ppermute | solution.py:385
  87.9 10.6 %collective-permute-start.6 = (bf16[128,1024]{1,0:T(8,128)(2,1)S(1)}, bf16[128,1024]{1,0:T(8,128)(2,1)S(1)}, u32[]{:S(2)}, u32[]{:S(2)}) collective-permute-start(bf16[128,1024]{1,0:T(8,128)(2,1)S(1)} %collective-permute-done.5.refs_13_), channel_id=1, source_target_pairs={{0,8},{1,121},{2,10},{3,123},{4,12},{5,125},{6,14},{7,127},{8,16},... | collective-permute-start | bytes 786440 | tf_op jit(solution)/shard_map/ppermute | solution.py:385
  89.2 19.7 %collective-permute-start.8 = (bf16[4,2,272,128]{3,2,1,0:T(8,128)(2,1)S(1)}, bf16[4,2,272,128]{3,2,1,0:T(8,128)(2,1)S(1)}, u32[]{:S(2)}, u32[]{:S(2)}) collective-permute-start(bf16[4,2,272,128]{3,2,1,0:T(8,128)(2,1)S(1)} %get-tuple-element.58), channel_id=1, source_target_pairs={{0,1},{1,0},{2,3},{3,2},{4,5},{5,4},{6,7},{7,6},{8,9},{9,8},{10,11... | collective-permute-start | bytes 1671176 | tf_op jit(solution)/shard_map/ppermute | solution.py:487
  98.5 17.3 %collective-permute-start.19 = (bf16[128,2048]{1,0:T(8,128)(2,1)}, bf16[128,2048]{1,0:T(8,128)(2,1)}, u32[]{:S(2)}, u32[]{:S(2)}) collective-permute-start(bf16[128,2048]{1,0:T(8,128)(2,1)} %collective-permute-done.3.refs_11_), channel_id=1, source_target_pairs={{0,1},{1,0},{2,3},{3,2},{4,5},{5,4},{6,7},{7,6},{8,9},{9,8},{10,11... | collective-permute-start | bytes 1572872 | tf_op jit(solution)/shard_map/ppermute | solution.py:391
  98.5 7.4 %collective-permute-start.13 = (bf16[128,1024]{1,0:T(8,128)(2,1)}, bf16[128,1024]{1,0:T(8,128)(2,1)S(1)}, u32[]{:S(2)}, u32[]{:S(2)}) collective-permute-start(bf16[128,1024]{1,0:T(8,128)(2,1)} %collective-permute-done.12.refs_14_), channel_id=1, source_target_pairs={{0,8},{1,121},{2,10},{3,123},{4,12},{5,125},{6,14},{7,127},{8,16},... | collective-permute-start | bytes 786440 | tf_op jit(solution)/shard_map/ppermute | solution.py:385
  100.6 12.3 %collective-permute-start.7 = (bf16[128,1024]{1,0:T(8,128)(2,1)S(1)}, bf16[128,1024]{1,0:T(8,128)(2,1)S(1)}, u32[]{:S(2)}, u32[]{:S(2)}) collective-permute-start(bf16[128,1024]{1,0:T(8,128)(2,1)S(1)} %collective-permute-done.6.refs_3_), channel_id=1, source_target_pairs={{0,8},{1,121},{2,10},{3,123},{4,12},{5,125},{6,14},{7,127},{8,16},... | collective-permute-start | bytes 786440 | tf_op jit(solution)/shard_map/ppermute | solution.py:385
  101.4 17.5 %collective-permute-start.15 = (bf16[128,1024]{1,0:T(8,128)(2,1)S(1)}, bf16[128,1024]{1,0:T(8,128)(2,1)S(1)}, u32[]{:S(2)}, u32[]{:S(2)}) collective-permute-start(bf16[128,1024]{1,0:T(8,128)(2,1)S(1)} %collective-permute-done.5.refs_13_), channel_id=1, source_target_pairs={{0,1},{1,0},{2,3},{3,2},{4,5},{5,4},{6,7},{7,6},{8,9},{9,8},{10,11... | collective-permute-start | bytes 786440 | tf_op jit(solution)/shard_map/ppermute | solution.py:391
  105.9 13.5 %collective-permute-start.20 = (bf16[128,1024]{1,0:T(8,128)(2,1)S(1)}, bf16[128,1024]{1,0:T(8,128)(2,1)S(1)}, u32[]{:S(2)}, u32[]{:S(2)}) collective-permute-start(bf16[128,1024]{1,0:T(8,128)(2,1)S(1)} %collective-permute-done.13.refs_4_), channel_id=1, source_target_pairs={{0,8},{1,121},{2,10},{3,123},{4,12},{5,125},{6,14},{7,127},{8,16},... | collective-permute-start | bytes 786440 | tf_op jit(solution)/shard_map/ppermute | solution.py:385
  108.9 13.2 %collective-permute-start.14 = (bf16[128,2048]{1,0:T(8,128)(2,1)}, bf16[128,2048]{1,0:T(8,128)(2,1)S(1)}, u32[]{:S(2)}, u32[]{:S(2)}) collective-permute-start(bf16[128,2048]{1,0:T(8,128)(2,1)} %collective-permute-done.4.refs_12_), channel_id=1, source_target_pairs={{0,1},{1,0},{2,3},{3,2},{4,5},{5,4},{6,7},{7,6},{8,9},{9,8},{10,11... | collective-permute-start | bytes 1572872 | tf_op jit(solution)/shard_map/ppermute | solution.py:391
  112.9 8.7 %collective-permute-start.16 = (bf16[128,1024]{1,0:T(8,128)(2,1)}, bf16[128,1024]{1,0:T(8,128)(2,1)S(1)}, u32[]{:S(2)}, u32[]{:S(2)}) collective-permute-start(bf16[128,1024]{1,0:T(8,128)(2,1)} %collective-permute-done.12.refs_14_), channel_id=1, source_target_pairs={{0,1},{1,0},{2,3},{3,2},{4,5},{5,4},{6,7},{7,6},{8,9},{9,8},{10,11... | collective-permute-start | bytes 786440 | tf_op jit(solution)/shard_map/ppermute | solution.py:391
  115.8 10.0 %collective-permute-start.9 = (bf16[2,2,272,128]{3,2,1,0:T(8,128)(2,1)S(1)}, bf16[2,2,272,128]{3,2,1,0:T(8,128)(2,1)S(1)}, u32[]{:S(2)}, u32[]{:S(2)}) collective-permute-start(bf16[2,2,272,128]{3,2,1,0:T(8,128)(2,1)S(1)} %get-tuple-element.59), channel_id=1, source_target_pairs={{0,4},{1,5},{2,6},{3,7},{4,0},{5,1},{6,2},{7,3},{8,12},{9,13},{10,... | collective-permute-start | bytes 835592 | tf_op jit(solution)/shard_map/ppermute | solution.py:499
  118.9 13.1 %collective-permute-start.10 = (bf16[2,2,272,128]{3,2,1,0:T(8,128)(2,1)S(1)}, bf16[2,2,272,128]{3,2,1,0:T(8,128)(2,1)S(1)}, u32[]{:S(2)}, u32[]{:S(2)}) collective-permute-start(bf16[2,2,272,128]{3,2,1,0:T(8,128)(2,1)S(1)} %get-tuple-element.60), channel_id=1, source_target_pairs={{0,2},{1,3},{2,4},{3,5},{4,6},{5,7},{6,0},{7,1},{8,10},{9,11},{10,... | collective-permute-start | bytes 835592 | tf_op jit(solution)/shard_map/ppermute | solution.py:499
  119.3 13.1 %collective-permute-start.11 = (bf16[2,2,272,128]{3,2,1,0:T(8,128)(2,1)S(1)}, bf16[2,2,272,128]{3,2,1,0:T(8,128)(2,1)S(1)}, u32[]{:S(2)}, u32[]{:S(2)}) collective-permute-start(bf16[2,2,272,128]{3,2,1,0:T(8,128)(2,1)S(1)} %get-tuple-element.61), channel_id=1, source_target_pairs={{0,6},{1,7},{2,0},{3,1},{4,2},{5,3},{6,4},{7,5},{8,14},{9,15},{10,... | collective-permute-start | bytes 835592 | tf_op jit(solution)/shard_map/ppermute | solution.py:499
  121.6 11.3 %collective-permute-start.25 = (bf16[128,1024]{1,0:T(8,128)(2,1)S(1)}, bf16[128,1024]{1,0:T(8,128)(2,1)S(1)}, u32[]{:S(2)}, u32[]{:S(2)}) collective-permute-start(bf16[128,1024]{1,0:T(8,128)(2,1)S(1)} %broadcast_select_fusion), channel_id=1, source_target_pairs={{0,8},{1,121},{2,10},{3,123},{4,12},{5,125},{6,14},{7,127},{8,16},... | collective-permute-start | bytes 786440 | tf_op jit(solution)/shard_map/ppermute | solution.py:385
  122.0 15.5 %collective-permute-start.21 = (bf16[128,1024]{1,0:T(8,128)(2,1)S(1)}, bf16[128,1024]{1,0:T(8,128)(2,1)S(1)}, u32[]{:S(2)}, u32[]{:S(2)}) collective-permute-start(bf16[128,1024]{1,0:T(8,128)(2,1)S(1)} %collective-permute-done.6.refs_3_), channel_id=1, source_target_pairs={{0,1},{1,0},{2,3},{3,2},{4,5},{5,4},{6,7},{7,6},{8,9},{9,8},{10,11... | collective-permute-start | bytes 786440 | tf_op jit(solution)/shard_map/ppermute | solution.py:391
  125.8 11.7 %collective-permute-start.22 = (bf16[128,1024]{1,0:T(8,128)(2,1)S(1)}, bf16[128,1024]{1,0:T(8,128)(2,1)S(1)}, u32[]{:S(2)}, u32[]{:S(2)}) collective-permute-start(bf16[128,1024]{1,0:T(8,128)(2,1)S(1)} %collective-permute-done.13.refs_4_), channel_id=1, source_target_pairs={{0,1},{1,0},{2,3},{3,2},{4,5},{5,4},{6,7},{7,6},{8,9},{9,8},{10,11... | collective-permute-start | bytes 786440 | tf_op jit(solution)/shard_map/ppermute | solution.py:391
  (16 other events, 284.3 us)

commit v7 on v6

--- a/solution.py
+++ b/solution.py
@@ -100,7 +100,7 @@
     ]
     for copy in small:
         copy.start()
-    for k in range(count):
+    for k in range(2):
         chunk_copy(tokens, kept, sems, k)[1].start()
     for copy in small:
         copy.wait()
@@ -109,6 +109,11 @@
     def part(k, _):
         at, copy = chunk_copy(tokens, kept, sems, k)
         copy.wait()
+
+        @pl.when(k + 2 < count)
+        def _():
+            chunk_copy(tokens, kept, sems, k + 2)[1].start()
+
         projected[at, :] = branch_product(kept[at, :], scaled[...])
         return 0
 
@@ -453,7 +458,7 @@
     (ends,) = advance([ends])
     all_ends = lax.all_to_all(ends, "sp", split_axis=0, concat_axis=0, tiled=True)
     late_tokens, _ = tie(tokens, ends)
-    (late_tokens,) = advance([late_tokens])
+    (late_tokens,) = advance([late_tokens], STREAMS)
     gate = pl.pallas_call(
         gate_kernel,
         in_specs=[hbm, fixed, fixed],
@@ -466,7 +471,7 @@
         compiler_params=limit(20),
         name="gate",
     )(in_hbm(late_tokens), gain_row, w_gate)
-    (gate,) = advance([gate], STREAMS)
+    (gate,) = advance([gate])
     chips = heads // 2
     order = [(dx, dc) for dc in (1, 0) for dx in range(chips)]
     part_shape = (2, BLOCK + EXTRA, head // 2)

time: 140 us -> 138 us (0.986)
  starting transfers between devices: 88.8 us -> 67.6 us
  blocking collectives: 0 us -> 15.6 us
  waiting for transfers between devices: 15.5 us -> 21.9 us
  local copies, waits for them, and re-layouts: 2.6 us -> 0.94 us
  Pallas kernels: 32.6 us -> 31 us
    all_to_all x0 -> x1, blocking collectives: none -> 15.6 us  [body(): lax.all_to_all(ends, 'sp', split_axis=0, concat_axis=0, tiled=True)]
    ppermute x11 -> x12, starting transfers between devices: 24 us -> 14.5 us  [across(): made.append(lax.ppermute(part, ('sp', 'tp'), swap))]
    ppermute x11 -> x12, starting transfers between devices: 44.4 us -> 35.7 us  [onward(): made.append(lax.ppermute(part, ('sp', 'tp'), around))]
    ppermute x11 -> x12, waiting for transfers between devices: 6.69 us -> 13.6 us  [onward(): made.append(lax.ppermute(part, ('sp', 'tp'), around))]
    all_to_all x1 -> x0, starting transfers between devices: 3.94 us -> none  [body(): lax.all_to_all(ends, 'sp', split_axis=0, concat_axis=0, tiled=True)]
  transfers between devices with their start and end apart: 28 -> 29, of which waited for: 5 -> 8; matrix products, arithmetic and copies ran while one was open for 1% -> 1% of each run, Pallas kernels for 22% -> 21%
where the time goes in v7:
time: 138 us; the launch traced here: 137 us
  starting transfers between devices  67.6 us (49%)
  Pallas kernels  31 us (22%)
  waiting for transfers between devices  21.9 us (16%)
  blocking collectives  15.6 us (11%)
    ppermute x12, starting transfers between devices, onward(): made.append(lax.ppermute(part, ('sp', 'tp'), around))  35.7 us
    all_to_all x1, blocking collectives, body(): lax.all_to_all(ends, 'sp', split_axis=0, concat_axis=0, tiled=True)  15.6 us
    ppermute x12, starting transfers between devices, across(): made.append(lax.ppermute(part, ('sp', 'tp'), swap))  14.5 us
    ppermute x12, waiting for transfers between devices, onward(): made.append(lax.ppermute(part, ('sp', 'tp'), around))  13.6 us
    ppermute x1, starting transfers between devices, body(): lax.ppermute(given, 'tp', [(t, neighbour(t, 0, 1, chips)) for t in range(...  10.4 us
    pallas_call x2, Pallas kernels, recur(): pl.pallas_call(functools.partial(recur_kernel, first=first), in_specs=[fi...  8.93 us
    ppermute x3, waiting for transfers between devices, body(): lax.ppermute(both, 'tp', [(t, neighbour(t, dx, 0, chips)) for t in range(...  6.33 us
    pallas_call x1, Pallas kernels, body(): pl.pallas_call(gate_kernel, in_specs=[hbm, fixed, fixed], out_specs=hbm,...  6.06 us
  transfers between devices with their start and end apart: 29, of which 8 were waited for; matrix products, arithmetic and copies ran while one was open for 1% of the time, Pallas kernels for 21%

profile of v7, /device:TPU:33, one launch (start us, length us, event | category | flops | bytes accessed | tf_op | source)
XLA Modules:
  0.0 137.3 jit_solution(14870041647741819683)
XLA Ops:
  0.0 22.9 %collective-permute-start = (bf16[128,2048]{1,0:T(8,128)(2,1)}, bf16[128,2048]{1,0:T(8,128)(2,1)S(1)}, u32[]{:S(2)}, u32[]{:S(2)}) collective-permute-start(bf16[128,2048]{1,0:T(8,128)(2,1)} %refs_9_.1), channel_id=1, source_target_pairs={{0,8},{1,121},{2,10},{3,123},{4,12},{5,125},{6,14},{7,127},{8,16},... | collective-permute-start | bytes 1572872 | tf_op jit(solution)/shard_map/ppermute | solution.py:390
  22.9 5.8 %input.1 = (bf16[2048,256]{1,0:T(8,128)(2,1)S(1)}, bf16[2048,256]{1,0:T(8,128)(2,1)S(1)}) custom-call(bf16[2048,2048]{1,0:T(8,128)(2,1)} %tokens.2, f32[1,2048]{1,0:T(1,128)} %bitcast.3, bf16[2048,256]{1,0:T(8,128)(2,1)} %w_input.1), custom_call_target="tpu_custom_call" | custom-call | tf_op jit(solution)/shard_map/input/pallas_call | solution.py:418
  29.4 3.0 %collective-permute-start.2 = (bf16[128,2048]{1,0:T(8,128)(2,1)S(1)}, bf16[128,2048]{1,0:T(8,128)(2,1)S(1)}, u32[]{:S(2)}, u32[]{:S(2)}) collective-permute-start(bf16[128,2048]{1,0:T(8,128)(2,1)S(1)} %collective-permute-done.refs_10_), channel_id=1, source_target_pairs={{0,8},{1,121},{2,10},{3,123},{4,12},{5,125},{6,14},{7,127},{8,16},... | collective-permute-start | bytes 1572872 | tf_op jit(solution)/shard_map/ppermute | solution.py:390
  34.5 1.9 %collective-permute-done.1.refs_0_ = bf16[16,2048]{1,0:T(8,128)(2,1)S(1)} collective-permute-done((bf16[16,2048]{1,0:T(8,128)(2,1)S(1)}, bf16[16,2048]{1,0:T(8,128)(2,1)S(1)}, u32[]{:S(2)}, u32[]{:S(2)}) %collective-permute-start.1) | collective-permute-done | bytes 65568 | tf_op jit(solution)/shard_map/ppermute | solution.py:414
  36.4 4.6 %recur.2 = (f32[2,2048,128]{2,1,0:T(8,128)}, f32[2,2048,128]{2,1,0:T(8,128)}, f32[1,8,256]{2,1,0:T(8,128)S(1)}) custom-call(bf16[2048,256]{1,0:T(8,128)(2,1)S(1)} %get-tuple-element.36.projected, f32[4,256]{1,0:T(4,128)S(1)} %copy-done.5, bf16[1,256,256]{2,1,0:T(8,128)(2,1)S(1)} %copy-done.1, bf16[1,256,256]{2,1,0:T(8,128)(2,1)S(1)} %copy-done.2, ...), custom_call_target="tpu_custom_call" | custom-call | tf_op jit(solution)/shard_map/recur/pallas_call | solution.py:436
  41.0 4.4 %recur.3 = (f32[2,2048,128]{2,1,0:T(8,128)}, f32[2,2048,128]{2,1,0:T(8,128)}, f32[16,2,256]{2,1,0:T(2,128)S(1)}) custom-call(bf16[2048,256]{1,0:T(8,128)(2,1)S(1)} %get-tuple-element.36.projected, f32[4,256]{1,0:T(4,128)S(1)} %copy-done.5, bf16[1,256,256]{2,1,0:T(8,128)(2,1)S(1)} %copy-done.1, ...), custom_call_target="tpu_custom_call", output_to_operand_aliasing={{0}: (7, {}), {1}: (8, {})} | custom-call | tf_op jit(solution)/shard_map/recur/pallas_call | solution.py:436
  45.4 3.0 %collective-permute-start.3 = (bf16[128,2048]{1,0:T(8,128)(2,1)S(1)}, bf16[128,2048]{1,0:T(8,128)(2,1)S(1)}, u32[]{:S(2)}, u32[]{:S(2)}) collective-permute-start(bf16[128,2048]{1,0:T(8,128)(2,1)S(1)} %collective-permute-done.2.refs_11_), channel_id=1, source_target_pairs={{0,8},{1,121},{2,10},{3,123},{4,12},{5,125},{6,14},{7,127},{8,16},... | collective-permute-start | bytes 1572872 | tf_op jit(solution)/shard_map/ppermute | solution.py:390
  48.4 6.2 %collective-permute-done.3.refs_12_ = bf16[128,2048]{1,0:T(8,128)(2,1)S(1)} collective-permute-done((bf16[128,2048]{1,0:T(8,128)(2,1)S(1)}, bf16[128,2048]{1,0:T(8,128)(2,1)S(1)}, u32[]{:S(2)}, u32[]{:S(2)}) %collective-permute-start.3) | collective-permute-done | bytes 524320 | tf_op jit(solution)/shard_map/ppermute | solution.py:390
  54.7 3.2 %collective-permute-start.4 = (bf16[128,1024]{1,0:T(8,128)(2,1)S(1)}, bf16[128,1024]{1,0:T(8,128)(2,1)}, u32[]{:S(2)}, u32[]{:S(2)}) collective-permute-start(bf16[128,1024]{1,0:T(8,128)(2,1)S(1)} %get-tuple-element.66), channel_id=1, source_target_pairs={{0,8},{1,121},{2,10},{3,123},{4,12},{5,125},{6,14},{7,127},{8,16},... | collective-permute-start | bytes 786440 | tf_op jit(solution)/shard_map/ppermute | solution.py:390
  58.0 6.1 %gate.1 = f32[2048,256]{1,0:T(8,128)} custom-call(bf16[2048,2048]{1,0:T(8,128)(2,1)} %tokens.2, f32[1,2048]{1,0:T(1,128)S(1)} %bitcast.4, bf16[2048,256]{1,0:T(8,128)(2,1)S(1)} %copy-done), custom_call_target="tpu_custom_call" | custom-call | tf_op jit(solution)/shard_map/gate/pallas_call | solution.py:462
  64.4 15.6 %all_to_all.5.ends = f32[16,2,256]{2,1,0:T(2,128)S(1)} all-to-all(f32[16,2,256]{2,1,0:T(2,128)S(1)} %get-tuple-element.45), channel_id=1, replica_groups=mesh['grp'=2,'sp'=16,'tp'=8] {'sp'}, dimensions={0} | all-to-all | bytes 65536 | tf_op jit(solution)/shard_map/all_to_all | solution.py:459
  80.0 3.5 %gated.1 = (bf16[4,2,272,128]{3,2,1,0:T(8,128)(2,1)S(1)}, bf16[4,2,272,128]{3,2,1,0:T(8,128)(2,1)S(1)}) custom-call(f32[2,2048,128]{2,1,0:T(8,128)} %get-tuple-element.41.state, f32[2,2048,128]{2,1,0:T(8,128)} %get-tuple-element.42.prod, f32[2048,256]{1,0:T(8,128)} %gate.1, f32[16,2,256]{2,1,0:T(2,128)S(1)} %all_to_all.5.ends, f32[1,256]{1,0:T(1,128)S(1)} %bitcast.7), custom_call_target="tpu_custom_call" | custom-call | tf_op jit(solution)/shard_map/gated/pallas_call | solution.py:478
  83.5 10.4 %collective-permute-start.8 = (bf16[4,2,272,128]{3,2,1,0:T(8,128)(2,1)S(1)}, bf16[4,2,272,128]{3,2,1,0:T(8,128)(2,1)S(1)}, u32[]{:S(2)}, u32[]{:S(2)}) collective-permute-start(bf16[4,2,272,128]{3,2,1,0:T(8,128)(2,1)S(1)} %get-tuple-element.58), channel_id=1, source_target_pairs={{0,1},{1,0},{2,3},{3,2},{4,5},{5,4},{6,7},{7,6},{8,9},{9,8},{10,11... | collective-permute-start | bytes 1671176 | tf_op jit(solution)/shard_map/ppermute | solution.py:492
  95.3 4.8 %collective-permute-done.13.refs_16_ = bf16[128,1024]{1,0:T(8,128)(2,1)S(1)} collective-permute-done((bf16[128,1024]{1,0:T(8,128)(2,1)}, bf16[128,1024]{1,0:T(8,128)(2,1)S(1)}, u32[]{:S(2)}, u32[]{:S(2)}) %collective-permute-start.13) | collective-permute-done | bytes 262176 | tf_op jit(solution)/shard_map/ppermute | solution.py:390
  102.9 2.4 %collective-permute-start.21 = (bf16[128,2048]{1,0:T(8,128)(2,1)S(1)}, bf16[128,2048]{1,0:T(8,128)(2,1)}, u32[]{:S(2)}, u32[]{:S(2)}) collective-permute-start(bf16[128,2048]{1,0:T(8,128)(2,1)S(1)} %collective-permute-done.3.refs_12_), channel_id=1, source_target_pairs={{0,1},{1,0},{2,3},{3,2},{4,5},{5,4},{6,7},{7,6},{8,9},{9,8},{10,11... | collective-permute-start | bytes 1572872 | tf_op jit(solution)/shard_map/ppermute | solution.py:396
  105.7 4.5 %collective-permute-start.16 = (bf16[128,1024]{1,0:T(8,128)(2,1)}, bf16[128,1024]{1,0:T(8,128)(2,1)S(1)}, u32[]{:S(2)}, u32[]{:S(2)}) collective-permute-start(bf16[128,1024]{1,0:T(8,128)(2,1)} %collective-permute-done.12.refs_14_), channel_id=1, source_target_pairs={{0,1},{1,0},{2,3},{3,2},{4,5},{5,4},{6,7},{7,6},{8,9},{9,8},{10,11... | collective-permute-start | bytes 786440 | tf_op jit(solution)/shard_map/ppermute | solution.py:396
  110.9 2.2 %collective-permute-start.17 = (bf16[128,1024]{1,0:T(8,128)(2,1)}, bf16[128,1024]{1,0:T(8,128)(2,1)S(1)}, u32[]{:S(2)}, u32[]{:S(2)}) collective-permute-start(bf16[128,1024]{1,0:T(8,128)(2,1)} %collective-permute-done.5.refs_15_), channel_id=1, source_target_pairs={{0,1},{1,0},{2,3},{3,2},{4,5},{5,4},{6,7},{7,6},{8,9},{9,8},{10,11... | collective-permute-start | bytes 786440 | tf_op jit(solution)/shard_map/ppermute | solution.py:396
  113.3 3.1 %collective-permute-start.9 = (bf16[2,2,272,128]{3,2,1,0:T(8,128)(2,1)S(1)}, bf16[2,2,272,128]{3,2,1,0:T(8,128)(2,1)S(1)}, u32[]{:S(2)}, u32[]{:S(2)}) collective-permute-start(bf16[2,2,272,128]{3,2,1,0:T(8,128)(2,1)S(1)} %get-tuple-element.59), channel_id=1, source_target_pairs={{0,4},{1,5},{2,6},{3,7},{4,0},{5,1},{6,2},{7,3},{8,12},{9,13},{10,... | collective-permute-start | bytes 835592 | tf_op jit(solution)/shard_map/ppermute | solution.py:504
  116.9 2.2 %collective-permute-start.11 = (bf16[2,2,272,128]{3,2,1,0:T(8,128)(2,1)S(1)}, bf16[2,2,272,128]{3,2,1,0:T(8,128)(2,1)S(1)}, u32[]{:S(2)}, u32[]{:S(2)}) collective-permute-start(bf16[2,2,272,128]{3,2,1,0:T(8,128)(2,1)S(1)} %get-tuple-element.61), channel_id=1, source_target_pairs={{0,6},{1,7},{2,0},{3,1},{4,2},{5,3},{6,4},{7,5},{8,14},{9,15},{10,... | collective-permute-start | bytes 835592 | tf_op jit(solution)/shard_map/ppermute | solution.py:504
  119.6 1.7 %collective-permute-start.23 = (bf16[128,1024]{1,0:T(8,128)(2,1)S(1)}, bf16[128,1024]{1,0:T(8,128)(2,1)S(1)}, u32[]{:S(2)}, u32[]{:S(2)}) collective-permute-start(bf16[128,1024]{1,0:T(8,128)(2,1)S(1)} %collective-permute-done.6.refs_3_), channel_id=1, source_target_pairs={{0,1},{1,0},{2,3},{3,2},{4,5},{5,4},{6,7},{7,6},{8,9},{9,8},{10,11... | collective-permute-start | bytes 786440 | tf_op jit(solution)/shard_map/ppermute | solution.py:396
  121.3 1.6 %collective-permute-done.9.refs_0_ = bf16[2,2,272,128]{3,2,1,0:T(8,128)(2,1)S(1)} collective-permute-done((bf16[2,2,272,128]{3,2,1,0:T(8,128)(2,1)S(1)}, bf16[2,2,272,128]{3,2,1,0:T(8,128)(2,1)S(1)}, u32[]{:S(2)}, u32[]{:S(2)}) %collective-permute-start.9) | collective-permute-done | bytes 278560 | tf_op jit(solution)/shard_map/ppermute | solution.py:504
  123.0 1.9 %collective-permute-start.24 = (bf16[128,1024]{1,0:T(8,128)(2,1)S(1)}, bf16[128,1024]{1,0:T(8,128)(2,1)S(1)}, u32[]{:S(2)}, u32[]{:S(2)}) collective-permute-start(bf16[128,1024]{1,0:T(8,128)(2,1)S(1)} %collective-permute-done.14.refs_4_), channel_id=1, source_target_pairs={{0,1},{1,0},{2,3},{3,2},{4,5},{5,4},{6,7},{7,6},{8,9},{9,8},{10,11... | collective-permute-start | bytes 786440 | tf_op jit(solution)/shard_map/ppermute | solution.py:396
  124.9 4.7 %collective-permute-done.10.refs_1_ = bf16[2,2,272,128]{3,2,1,0:T(8,128)(2,1)S(1)} collective-permute-done((bf16[2,2,272,128]{3,2,1,0:T(8,128)(2,1)S(1)}, bf16[2,2,272,128]{3,2,1,0:T(8,128)(2,1)S(1)}, u32[]{:S(2)}, u32[]{:S(2)}) %collective-permute-start.10) | collective-permute-done | bytes 278560 | tf_op jit(solution)/shard_map/ppermute | solution.py:504
  130.6 4.5 %early.1 = (f32[256,2048]{1,0:T(8,128)S(1)}, bf16[8,2,272,128]{3,2,1,0:T(8,128)(2,1)S(1)}) custom-call(bf16[4,2,272,128]{3,2,1,0:T(8,128)(2,1)S(1)} %get-tuple-element.57.kept, bf16[4,2,272,128]{3,2,1,0:T(8,128)(2,1)S(1)} %collective-permute-done.8.given, bf16[2,2,272,128]{3,2,1,0:T(8,128)(2,1)S(1)} %collective-permute-done.9.refs_0_, ...), custom_call_target="tpu_custom_call" | custom-call | tf_op jit(solution)/shard_map/early/pallas_call | solution.py:516
  (75 shorter events, 13.0 us)
Async XLA Ops:
  0.0 29.4 %collective-permute-start = (bf16[128,2048]{1,0:T(8,128)(2,1)}, bf16[128,2048]{1,0:T(8,128)(2,1)S(1)}, u32[]{:S(2)}, u32[]{:S(2)}) collective-permute-start(bf16[128,2048]{1,0:T(8,128)(2,1)} %refs_9_.1), channel_id=1, source_target_pairs={{0,8},{1,121},{2,10},{3,123},{4,12},{5,125},{6,14},{7,127},{8,16},... | collective-permute-start | bytes 1572872 | tf_op jit(solution)/shard_map/ppermute | solution.py:390
  29.4 16.0 %collective-permute-start.2 = (bf16[128,2048]{1,0:T(8,128)(2,1)S(1)}, bf16[128,2048]{1,0:T(8,128)(2,1)S(1)}, u32[]{:S(2)}, u32[]{:S(2)}) collective-permute-start(bf16[128,2048]{1,0:T(8,128)(2,1)S(1)} %collective-permute-done.refs_10_), channel_id=1, source_target_pairs={{0,8},{1,121},{2,10},{3,123},{4,12},{5,125},{6,14},{7,127},{8,16},... | collective-permute-start | bytes 1572872 | tf_op jit(solution)/shard_map/ppermute | solution.py:390
  45.4 9.2 %collective-permute-start.3 = (bf16[128,2048]{1,0:T(8,128)(2,1)S(1)}, bf16[128,2048]{1,0:T(8,128)(2,1)S(1)}, u32[]{:S(2)}, u32[]{:S(2)}) collective-permute-start(bf16[128,2048]{1,0:T(8,128)(2,1)S(1)} %collective-permute-done.2.refs_11_), channel_id=1, source_target_pairs={{0,8},{1,121},{2,10},{3,123},{4,12},{5,125},{6,14},{7,127},{8,16},... | collective-permute-start | bytes 1572872 | tf_op jit(solution)/shard_map/ppermute | solution.py:390
  54.7 9.4 %collective-permute-start.4 = (bf16[128,1024]{1,0:T(8,128)(2,1)S(1)}, bf16[128,1024]{1,0:T(8,128)(2,1)}, u32[]{:S(2)}, u32[]{:S(2)}) collective-permute-start(bf16[128,1024]{1,0:T(8,128)(2,1)S(1)} %get-tuple-element.66), channel_id=1, source_target_pairs={{0,8},{1,121},{2,10},{3,123},{4,12},{5,125},{6,14},{7,127},{8,16},... | collective-permute-start | bytes 786440 | tf_op jit(solution)/shard_map/ppermute | solution.py:390
  57.8 36.6 %collective-permute-start.12 = (bf16[128,1024]{1,0:T(8,128)(2,1)S(1)}, bf16[128,1024]{1,0:T(8,128)(2,1)}, u32[]{:S(2)}, u32[]{:S(2)}) collective-permute-start(bf16[128,1024]{1,0:T(8,128)(2,1)S(1)} %get-tuple-element.65), channel_id=1, source_target_pairs={{0,8},{1,121},{2,10},{3,123},{4,12},{5,125},{6,14},{7,127},{8,16},... | collective-permute-start | bytes 786440 | tf_op jit(solution)/shard_map/ppermute | solution.py:390
  64.1 31.1 %collective-permute-start.5 = (bf16[128,1024]{1,0:T(8,128)(2,1)}, bf16[128,1024]{1,0:T(8,128)(2,1)}, u32[]{:S(2)}, u32[]{:S(2)}) collective-permute-start(bf16[128,1024]{1,0:T(8,128)(2,1)} %collective-permute-done.4.refs_13_), channel_id=1, source_target_pairs={{0,8},{1,121},{2,10},{3,123},{4,12},{5,125},{6,14},{7,127},{8,16},... | collective-permute-start | bytes 786440 | tf_op jit(solution)/shard_map/ppermute | solution.py:390
  83.5 26.7 %collective-permute-start.8 = (bf16[4,2,272,128]{3,2,1,0:T(8,128)(2,1)S(1)}, bf16[4,2,272,128]{3,2,1,0:T(8,128)(2,1)S(1)}, u32[]{:S(2)}, u32[]{:S(2)}) collective-permute-start(bf16[4,2,272,128]{3,2,1,0:T(8,128)(2,1)S(1)} %get-tuple-element.58), channel_id=1, source_target_pairs={{0,1},{1,0},{2,3},{3,2},{4,5},{5,4},{6,7},{7,6},{8,9},{9,8},{10,11... | collective-permute-start | bytes 1671176 | tf_op jit(solution)/shard_map/ppermute | solution.py:492
  93.9 11.5 %collective-permute-start.19 = (bf16[128,2048]{1,0:T(8,128)(2,1)S(1)}, bf16[128,2048]{1,0:T(8,128)(2,1)S(1)}, u32[]{:S(2)}, u32[]{:S(2)}) collective-permute-start(bf16[128,2048]{1,0:T(8,128)(2,1)S(1)} %collective-permute-done.refs_10_), channel_id=1, source_target_pairs={{0,1},{1,0},{2,3},{3,2},{4,5},{5,4},{6,7},{7,6},{8,9},{9,8},{10,11... | collective-permute-start | bytes 1572872 | tf_op jit(solution)/shard_map/ppermute | solution.py:396
  94.2 11.3 %collective-permute-start.20 = (bf16[128,2048]{1,0:T(8,128)(2,1)S(1)}, bf16[128,2048]{1,0:T(8,128)(2,1)S(1)}, u32[]{:S(2)}, u32[]{:S(2)}) collective-permute-start(bf16[128,2048]{1,0:T(8,128)(2,1)S(1)} %collective-permute-done.2.refs_11_), channel_id=1, source_target_pairs={{0,1},{1,0},{2,3},{3,2},{4,5},{5,4},{6,7},{7,6},{8,9},{9,8},{10,11... | collective-permute-start | bytes 1572872 | tf_op jit(solution)/shard_map/ppermute | solution.py:396
  94.4 5.7 %collective-permute-start.13 = (bf16[128,1024]{1,0:T(8,128)(2,1)}, bf16[128,1024]{1,0:T(8,128)(2,1)S(1)}, u32[]{:S(2)}, u32[]{:S(2)}) collective-permute-start(bf16[128,1024]{1,0:T(8,128)(2,1)} %collective-permute-done.12.refs_14_), channel_id=1, source_target_pairs={{0,8},{1,121},{2,10},{3,123},{4,12},{5,125},{6,14},{7,127},{8,16},... | collective-permute-start | bytes 786440 | tf_op jit(solution)/shard_map/ppermute | solution.py:390
  95.1 7.8 %collective-permute-start.6 = (bf16[128,1024]{1,0:T(8,128)(2,1)}, bf16[128,1024]{1,0:T(8,128)(2,1)S(1)}, u32[]{:S(2)}, u32[]{:S(2)}) collective-permute-start(bf16[128,1024]{1,0:T(8,128)(2,1)} %collective-permute-done.5.refs_15_), channel_id=1, source_target_pairs={{0,8},{1,121},{2,10},{3,123},{4,12},{5,125},{6,14},{7,127},{8,16},... | collective-permute-start | bytes 786440 | tf_op jit(solution)/shard_map/ppermute | solution.py:390
  102.9 13.5 %collective-permute-start.21 = (bf16[128,2048]{1,0:T(8,128)(2,1)S(1)}, bf16[128,2048]{1,0:T(8,128)(2,1)}, u32[]{:S(2)}, u32[]{:S(2)}) collective-permute-start(bf16[128,2048]{1,0:T(8,128)(2,1)S(1)} %collective-permute-done.3.refs_12_), channel_id=1, source_target_pairs={{0,1},{1,0},{2,3},{3,2},{4,5},{5,4},{6,7},{7,6},{8,9},{9,8},{10,11... | collective-permute-start | bytes 1572872 | tf_op jit(solution)/shard_map/ppermute | solution.py:396
  105.5 7.6 %collective-permute-start.15 = (bf16[128,1024]{1,0:T(8,128)(2,1)}, bf16[128,1024]{1,0:T(8,128)(2,1)S(1)}, u32[]{:S(2)}, u32[]{:S(2)}) collective-permute-start(bf16[128,1024]{1,0:T(8,128)(2,1)} %collective-permute-done.4.refs_13_), channel_id=1, source_target_pairs={{0,1},{1,0},{2,3},{3,2},{4,5},{5,4},{6,7},{7,6},{8,9},{9,8},{10,11... | collective-permute-start | bytes 786440 | tf_op jit(solution)/shard_map/ppermute | solution.py:396
  105.7 7.6 %collective-permute-start.16 = (bf16[128,1024]{1,0:T(8,128)(2,1)}, bf16[128,1024]{1,0:T(8,128)(2,1)S(1)}, u32[]{:S(2)}, u32[]{:S(2)}) collective-permute-start(bf16[128,1024]{1,0:T(8,128)(2,1)} %collective-permute-done.12.refs_14_), channel_id=1, source_target_pairs={{0,1},{1,0},{2,3},{3,2},{4,5},{5,4},{6,7},{7,6},{8,9},{9,8},{10,11... | collective-permute-start | bytes 786440 | tf_op jit(solution)/shard_map/ppermute | solution.py:396
  110.1 6.8 %collective-permute-start.22 = (bf16[128,1024]{1,0:T(8,128)(2,1)S(1)}, bf16[128,1024]{1,0:T(8,128)(2,1)S(1)}, u32[]{:S(2)}, u32[]{:S(2)}) collective-permute-start(bf16[128,1024]{1,0:T(8,128)(2,1)S(1)} %collective-permute-done.14.refs_4_), channel_id=1, source_target_pairs={{0,8},{1,121},{2,10},{3,123},{4,12},{5,125},{6,14},{7,127},{8,16},... | collective-permute-start | bytes 786440 | tf_op jit(solution)/shard_map/ppermute | solution.py:390
  110.9 8.3 %collective-permute-start.17 = (bf16[128,1024]{1,0:T(8,128)(2,1)}, bf16[128,1024]{1,0:T(8,128)(2,1)S(1)}, u32[]{:S(2)}, u32[]{:S(2)}) collective-permute-start(bf16[128,1024]{1,0:T(8,128)(2,1)} %collective-permute-done.5.refs_15_), channel_id=1, source_target_pairs={{0,1},{1,0},{2,3},{3,2},{4,5},{5,4},{6,7},{7,6},{8,9},{9,8},{10,11... | collective-permute-start | bytes 786440 | tf_op jit(solution)/shard_map/ppermute | solution.py:396
  113.1 6.5 %collective-permute-start.18 = (bf16[128,1024]{1,0:T(8,128)(2,1)}, bf16[128,1024]{1,0:T(8,128)(2,1)S(1)}, u32[]{:S(2)}, u32[]{:S(2)}) collective-permute-start(bf16[128,1024]{1,0:T(8,128)(2,1)} %copy-done.13), channel_id=1, source_target_pairs={{0,1},{1,0},{2,3},{3,2},{4,5},{5,4},{6,7},{7,6},{8,9},{9,8},{10,11... | collective-permute-start | bytes 786440 | tf_op jit(solution)/shard_map/ppermute | solution.py:396
  113.3 9.7 %collective-permute-start.9 = (bf16[2,2,272,128]{3,2,1,0:T(8,128)(2,1)S(1)}, bf16[2,2,272,128]{3,2,1,0:T(8,128)(2,1)S(1)}, u32[]{:S(2)}, u32[]{:S(2)}) collective-permute-start(bf16[2,2,272,128]{3,2,1,0:T(8,128)(2,1)S(1)} %get-tuple-element.59), channel_id=1, source_target_pairs={{0,4},{1,5},{2,6},{3,7},{4,0},{5,1},{6,2},{7,3},{8,12},{9,13},{10,... | collective-permute-start | bytes 835592 | tf_op jit(solution)/shard_map/ppermute | solution.py:504
  116.4 13.1 %collective-permute-start.10 = (bf16[2,2,272,128]{3,2,1,0:T(8,128)(2,1)S(1)}, bf16[2,2,272,128]{3,2,1,0:T(8,128)(2,1)S(1)}, u32[]{:S(2)}, u32[]{:S(2)}) collective-permute-start(bf16[2,2,272,128]{3,2,1,0:T(8,128)(2,1)S(1)} %get-tuple-element.60), channel_id=1, source_target_pairs={{0,2},{1,3},{2,4},{3,5},{4,6},{5,7},{6,0},{7,1},{8,10},{9,11},{10,... | collective-permute-start | bytes 835592 | tf_op jit(solution)/shard_map/ppermute | solution.py:504
  116.9 13.1 %collective-permute-start.11 = (bf16[2,2,272,128]{3,2,1,0:T(8,128)(2,1)S(1)}, bf16[2,2,272,128]{3,2,1,0:T(8,128)(2,1)S(1)}, u32[]{:S(2)}, u32[]{:S(2)}) collective-permute-start(bf16[2,2,272,128]{3,2,1,0:T(8,128)(2,1)S(1)} %get-tuple-element.61), channel_id=1, source_target_pairs={{0,6},{1,7},{2,0},{3,1},{4,2},{5,3},{6,4},{7,5},{8,14},{9,15},{10,... | collective-permute-start | bytes 835592 | tf_op jit(solution)/shard_map/ppermute | solution.py:504
  119.2 11.3 %collective-permute-start.27 = (bf16[128,1024]{1,0:T(8,128)(2,1)S(1)}, bf16[128,1024]{1,0:T(8,128)(2,1)S(1)}, u32[]{:S(2)}, u32[]{:S(2)}) collective-permute-start(bf16[128,1024]{1,0:T(8,128)(2,1)S(1)} %broadcast_select_fusion), channel_id=1, source_target_pairs={{0,8},{1,121},{2,10},{3,123},{4,12},{5,125},{6,14},{7,127},{8,16},... | collective-permute-start | bytes 786440 | tf_op jit(solution)/shard_map/ppermute | solution.py:390
  119.6 15.4 %collective-permute-start.23 = (bf16[128,1024]{1,0:T(8,128)(2,1)S(1)}, bf16[128,1024]{1,0:T(8,128)(2,1)S(1)}, u32[]{:S(2)}, u32[]{:S(2)}) collective-permute-start(bf16[128,1024]{1,0:T(8,128)(2,1)S(1)} %collective-permute-done.6.refs_3_), channel_id=1, source_target_pairs={{0,1},{1,0},{2,3},{3,2},{4,5},{5,4},{6,7},{7,6},{8,9},{9,8},{10,11... | collective-permute-start | bytes 786440 | tf_op jit(solution)/shard_map/ppermute | solution.py:396
  123.0 12.1 %collective-permute-start.24 = (bf16[128,1024]{1,0:T(8,128)(2,1)S(1)}, bf16[128,1024]{1,0:T(8,128)(2,1)S(1)}, u32[]{:S(2)}, u32[]{:S(2)}) collective-permute-start(bf16[128,1024]{1,0:T(8,128)(2,1)S(1)} %collective-permute-done.14.refs_4_), channel_id=1, source_target_pairs={{0,1},{1,0},{2,3},{3,2},{4,5},{5,4},{6,7},{7,6},{8,9},{9,8},{10,11... | collective-permute-start | bytes 786440 | tf_op jit(solution)/shard_map/ppermute | solution.py:396
  129.5 5.5 %collective-permute-start.25 = (bf16[128,1024]{1,0:T(8,128)(2,1)S(1)}, bf16[128,1024]{1,0:T(8,128)(2,1)S(1)}, u32[]{:S(2)}, u32[]{:S(2)}) collective-permute-start(bf16[128,1024]{1,0:T(8,128)(2,1)S(1)} %collective-permute-done.7.refs_0_), channel_id=1, source_target_pairs={{0,1},{1,0},{2,3},{3,2},{4,5},{5,4},{6,7},{7,6},{8,9},{9,8},{10,11... | collective-permute-start | bytes 786440 | tf_op jit(solution)/shard_map/ppermute | solution.py:396
  (19 other events, 332.8 us)
